TPU v7x, 512 devices: a whole 4x8x8 slice. The times are simulated.
512 devices in a mesh: sp: 32 (over z, x), tp: 16 (over y, core).
Axes of the slice: x: 4, y: 8, z: 8, core: 2. Of those that a mesh axis runs over, the one named last changes fastest.
Arguments:
- queries: bfloat16 [8192, 1536], P('sp', 'tp'), may hold values from -500 to 500
- latent: bfloat16 [8192, 256], P('sp'), may hold values from -6 to 6
- rope_key: bfloat16 [8192, 32], P('sp'), may hold values from -6 to 6
- latent_gain: bfloat16 [256], replicated, may hold values from 0.099609375 to 1.8984375
- key_value_weight: bfloat16 [256, 2048], P(None, 'tp'), may hold values from -0.375 to 0.375
- out_weight: bfloat16 [1024, 2048], P(None, 'tp'), may hold values from -6 to 6
- residual: bfloat16 [8192, 2048], P('sp', 'tp'), may hold values from -150 to 150
- ffn_gain: bfloat16 [2048], replicated, may hold values from 0.099609375 to 1.8984375
- routes: int32 [8192, 2], P('sp'), may hold values from 0 to 31, all different within a row; in each aligned block of 256 rows (0 to 255, 256 to 511, ...) at most 32 rows name the same one
- route_prob: float32 [8192, 2], P('sp'), may hold values from 0.1 to 1
- group_weight: float32 [8192], P('sp'), may hold values from 0.25 to 1
- gate_weight: bfloat16 [32, 2048, 4096], P('sp', None, 'tp'), may hold values from -0.125 to 0.125
- up_weight: bfloat16 [32, 2048, 4096], P('sp', None, 'tp'), may hold values from -0.125 to 0.125
- down_weight: bfloat16 [32, 4096, 2048], P('sp', None, 'tp'), may hold values from -0.75 to 0.75
Outputs:
- final: bfloat16 [8192, 2048], P('sp', 'tp')
Inputs may be any that keep to these rules, and one draw needn't show every extreme that they name: `routes`: each row names 2 different experts; among the 256 rows of one index of sp no expert is named more than 32 times, a bound that some block reaches.
All inputs are finite; a program needn't handle non-finite values.
Results may differ from a plain program's by a relative error of at most 0.015.
The roundings to bfloat16 on the way count: a program that leaves them out, or rounds other values in their place, can miss the bound.
Values may be sent and summed in bfloat16 or wider, within the bound.
No kernel may reach another device: no remote copies, remote signals or barrier semaphores. Data moves between devices by JAX's collectives and lax.ppermute only.
A program may use at most 64 MiB of HBM per device.

v0:
```python
import jax
import jax.numpy as jnp
from jax import lax
from jax.sharding import PartitionSpec as P

D = 2048
NOPE = 64
ROPE = 32
VDIM = 64
TOP = 2
SPAN = 64
X = 4
Z = 8
Y = 8
SP = X * Z
TP = Y * 2

THETA = 500000.0
EPSILON = 1e-06

EARLY = (4, 1, 7, 2)
LATE = (6, 3, 5)


Z_GROUPS = [[z * X + x for z in range(Z)] for x in range(X)]
X_GROUPS = [[z * X + x for x in range(X)] for z in range(Z)]


def exchange(value, axis, groups=None):
    return lax.all_to_all(
        value, axis, split_axis=0, concat_axis=0, tiled=True, axis_index_groups=groups
    )


def swap(value):
    return lax.ppermute(value, "tp", [(t, t ^ 1) for t in range(TP)])


def x_shift(value, by):
    return lax.ppermute(
        value, "sp", [(s, s // X * X + (s + by) % X) for s in range(SP)]
    )


def y_step(value, by):
    return lax.ppermute(value, "tp", [(t, (t + 2 * by) % TP) for t in range(TP)])


def tables(positions):
    frequency = 1.0 / THETA ** (jnp.arange(0, ROPE, 2, dtype=jnp.float32) / ROPE)
    angles = positions.astype(jnp.float32)[:, None] * frequency[None, :]
    return jnp.cos(angles), jnp.sin(angles)


def rotate(values, positions):
    half_width = ROPE // 2
    cos_table, sin_table = tables(positions)
    wide = values.astype(jnp.float32)
    lower_half = wide[:, :half_width]
    upper_half = wide[:, half_width:]
    return jnp.concatenate(
        [
            lower_half * cos_table - upper_half * sin_table,
            upper_half * cos_table + lower_half * sin_table,
        ],
        axis=-1,
    ).astype(jnp.bfloat16)


def body(
    queries,
    latent,
    rope_key,
    latent_gain,
    key_value_weight,
    out_weight,
    residual,
    ffn_gain,
    routes,
    route_prob,
    group_weight,
    gate_weight,
    up_weight,
    down_weight,
):
    tokens = queries.shape[0]
    width = residual.shape[1]
    ff = gate_weight.shape[2]
    sp = lax.axis_index("sp")
    tp = lax.axis_index("tp")
    z, x = sp // X, sp % X
    y, core = tp // 2, tp % 2
    bf16, f32 = jnp.bfloat16, jnp.float32
    local = jnp.arange(tokens, dtype=jnp.int32)

    latent_wide = latent.astype(f32)
    normed = latent_wide * lax.rsqrt(
        jnp.mean(latent_wide * latent_wide, axis=-1, keepdims=True) + EPSILON
    )
    normed = (normed * latent_gain.astype(f32)).astype(bf16)
    key_value = lax.dot_general(
        key_value_weight, normed, (((0,), (1,)), ((), ())), preferred_element_type=f32
    ).astype(bf16)
    positions = sp * tokens + local
    rotated = rotate(rope_key, positions).T
    block = jnp.concatenate([key_value[:NOPE], rotated, key_value[NOPE:]], axis=0)
    query = jnp.concatenate([queries[:, :NOPE], rotate(queries[:, NOPE:], positions)], axis=1)
    copies, query = lax.optimization_barrier(
        (jnp.broadcast_to(block, (Z,) + block.shape), query)
    )
    blocks = exchange(copies, "sp", Z_GROUPS)

    query_parts = [query]
    for by in range(1, X):
        query_parts.append(x_shift(query, by))
    query_parts = jnp.stack(query_parts)
    at = lambda a, chip: lax.dynamic_index_in_dim(a, chip, 0, keepdims=False)
    query_all = jnp.concatenate([at(query_parts, (x - one) % X) for one in range(X)], axis=0)

    gate_up_weight = jnp.concatenate(
        [gate_weight.reshape(TP, width, ff), up_weight.reshape(TP, width, ff)], axis=2
    )
    gains = ffn_gain.astype(f32).reshape(TP, width)
    down = down_weight.reshape(Y, 2, ff, width)
    down = jnp.where(core == 0, down, down[:, ::-1]).reshape(Y, 2 * ff, width)
    down_parts = {0: at(down, y)}
    for by in EARLY:
        down_parts[by] = y_step(at(down, (y + by) % Y), by)
    late = {by: at(down, (y + by) % Y) for by in LATE}

    experts = SP
    capacity = 2 * tokens * TOP // experts
    slots = experts * capacity
    named = jnp.arange(experts, dtype=jnp.int32)[None, :]
    one_hot = [(routes[:, k : k + 1] == named).astype(f32) for k in range(TOP)]
    both = (one_hot[0] + one_hot[1]).astype(bf16)
    earlier = (local[None, :] < local[:, None]).astype(bf16)
    before = jnp.dot(earlier, both, preferred_element_type=f32)
    slot_row = jnp.arange(slots, dtype=jnp.int32)
    select = []
    for k in range(TOP):
        rank = jnp.sum(before * one_hot[k], axis=1).astype(jnp.int32)
        slot = routes[:, k] * capacity + rank
        select.append((slot[:, None] == slot_row[None, :]).astype(bf16))
    placed = select[0] + select[1]

    scores = jnp.einsum(
        "zdk,qd->zkq", blocks[:, : NOPE + ROPE], query_all, preferred_element_type=f32
    )
    scores = scores * (NOPE + ROPE) ** (-0.5)
    query_positions = z * X * tokens + jnp.arange(X * tokens, dtype=jnp.int32)
    key_starts = (jnp.arange(Z, dtype=jnp.int32) * X + x) * tokens
    key_blocks = (key_starts[:, None] + local[None, :]) // SPAN
    allowed = key_blocks[:, :, None] <= (query_positions // SPAN)[None, None, :]
    scores = jnp.where(allowed, scores, -jnp.inf)
    top = jnp.maximum(jnp.max(scores, axis=(0, 1)), -1e30)[None, :]
    expd = jnp.exp(scores - top[None])
    total = jnp.sum(expd, axis=(0, 1))[None, :]
    summed = jnp.einsum(
        "zvk,zkq->vq", blocks[:, NOPE + ROPE :], expd.astype(bf16), preferred_element_type=f32
    )
    packed = jnp.concatenate([summed, top, total, jnp.zeros((6, X * tokens), f32)], axis=0)
    packed = jnp.stack([packed[:, i * tokens : (i + 1) * tokens] for i in range(X)])
    packed = exchange(packed, "sp", X_GROUPS)
    tops = packed[:, VDIM]
    factors = jnp.exp(tops - jnp.max(tops, axis=0, keepdims=True))
    merged = jnp.sum(factors[:, None, :] * packed, axis=0)
    attended = (merged[:VDIM] / merged[VDIM + 1 : VDIM + 2]).astype(bf16)
    attended, gate_up_weight, down_parts, placed = lax.optimization_barrier(
        (attended, gate_up_weight, down_parts, placed)
    )

    attended_all = lax.all_gather(attended, "tp", axis=0, tiled=True)
    projected = lax.dot_general(
        attended_all, out_weight, (((0,), (0,)), ((), ())), preferred_element_type=f32
    )
    mixed = (residual.astype(f32) + projected).astype(bf16)

    sent = lax.dot_general(placed, mixed, (((0,), (0,)), ((), ())), preferred_element_type=f32)
    sent, late = lax.optimization_barrier((sent.astype(bf16), late))
    arrived = exchange(sent.reshape(SP, capacity, width), "sp").reshape(slots, width)
    for by in LATE:
        late[by] = y_step(late[by], by)
    arrived, late = lax.optimization_barrier((arrived, late))
    down_parts = {**down_parts, **late}

    def products(parts):
        scaled, weights, squares = [], [], 0.0
        for rows, chip, side in parts:
            wide = rows.astype(f32)
            device = (chip % Y) * 2 + side
            scaled.append((wide * at(gains, device)[None, :]).astype(bf16))
            weights.append(at(gate_up_weight, device))
            squares = squares + jnp.sum(wide * wide, axis=1, keepdims=True)
        product = jnp.dot(
            jnp.concatenate(scaled, axis=1),
            jnp.concatenate(weights, axis=0),
            preferred_element_type=f32,
        )
        return product, squares

    half = slots // 2

    def ring(above, below):
        above = y_step(above, 1)
        below = y_step(below, -1)
        return above, below

    above = below = arrived
    gate_up, squares = products([(arrived, y, core), (swap(arrived), y, 1 - core)])
    for k in range(1, 4):
        above, below = ring(above, below)
        crossed = swap(jnp.concatenate([above, below], axis=1))
        more, more_squares = products(
            [
                (above, y - k, core),
                (below, y + k, core),
                (crossed[:, :width], y - k, 1 - core),
                (crossed[:, width:], y + k, 1 - core),
            ]
        )
        gate_up, squares = gate_up + more, squares + more_squares
    last = jnp.concatenate(ring(above[:half], below[half:]), axis=0)
    more, more_squares = products([(last, y + 4, core), (swap(last), y + 4, 1 - core)])
    gate_up, squares = gate_up + more, squares + more_squares
    gate_up = gate_up * lax.rsqrt(squares / D + EPSILON)
    hidden = (jax.nn.silu(gate_up[:, :ff]) * gate_up[:, ff:]).astype(bf16)

    hidden = jnp.concatenate([hidden, swap(hidden)], axis=1)
    first = jnp.dot(hidden, down_parts[4], preferred_element_type=f32).astype(bf16)
    order = (3, 5, 2, 6, 1, 7, 0)
    rest = jnp.dot(
        hidden,
        jnp.concatenate([down_parts[by] for by in order], axis=1),
        preferred_element_type=f32,
    )
    rest = lax.optimization_barrier(rest)
    own = {by: rest[:, i * width : (i + 1) * width] for i, by in enumerate(order)}
    nothing = jnp.zeros((half, width), bf16)
    above = jnp.concatenate([y_step(first[:half], 1), nothing], axis=0)
    below = jnp.concatenate([nothing, y_step(first[half:], -1)], axis=0)
    for k in (3, 2, 1):
        above = y_step((above.astype(f32) + own[Y - k]).astype(bf16), 1)
        below = y_step((below.astype(f32) + own[k]).astype(bf16), -1)
    expert_out = own[0] + above.astype(f32) + below.astype(f32)
    expert_out = expert_out.astype(bf16).reshape(SP, capacity, width)

    returned = exchange(expert_out, "sp").reshape(slots, width)
    combine = group_weight[:, None] * route_prob / jnp.sum(route_prob, axis=-1, keepdims=True)
    final = mixed.astype(f32)
    for k in range(TOP):
        picked = jnp.dot(select[k], returned, preferred_element_type=f32)
        final = final + combine[:, k : k + 1] * picked
    return final.astype(bf16)


def solution(mesh):
    return jax.shard_map(
        body,
        mesh=mesh,
        in_specs=(
            P("sp", "tp"),
            P("sp", None),
            P("sp", None),
            P(),
            P(None, "tp"),
            P(None, "tp"),
            P("sp", "tp"),
            P(),
            P("sp", None),
            P("sp", None),
            P("sp"),
            P("sp", None, "tp"),
            P("sp", None, "tp"),
            P("sp", None, "tp"),
        ),
        out_specs=P("sp", "tp"),
        check_vma=False,
    )
```

profile of v0, /device:TPU:8, one launch (start us, length us, event | category | flops | bytes accessed | tf_op | source)
XLA Modules:
  0.0 262.1 jit_solution(11410558851968653652)
XLA Ops:
  6.9 3.4 %collective-permute-start = (bf16[256,96]{0,1:T(8,128)(2,1)}, bf16[256,96]{0,1:T(8,128)(2,1)}, u32[]{:S(2)}, u32[]{:S(2)}) collective-permute-start(bf16[256,96]{0,1:T(8,128)(2,1)} %pad_maximum_fusion.10), channel_id=1, source_target_pairs={{0,16},{16,32},{32,48},{48,0},{64,80},{80,96},{96,112},{112,64},{1... | collective-permute-start | bytes 147464 | tf_op jit(solution)/shard_map/ppermute | solution.py:40
  10.3 4.6 %collective-permute-start.1 = (bf16[256,96]{0,1:T(8,128)(2,1)}, bf16[256,96]{0,1:T(8,128)(2,1)}, u32[]{:S(2)}, u32[]{:S(2)}) collective-permute-start(bf16[256,96]{0,1:T(8,128)(2,1)} %pad_maximum_fusion.10), channel_id=1, source_target_pairs={{0,32},{16,48},{32,0},{48,16},{64,96},{80,112},{96,64},{112,80},{1... | collective-permute-start | bytes 147464 | tf_op jit(solution)/shard_map/ppermute | solution.py:40
  14.9 3.3 %collective-permute-start.2 = (bf16[256,96]{0,1:T(8,128)(2,1)}, bf16[256,96]{0,1:T(8,128)(2,1)}, u32[]{:S(2)}, u32[]{:S(2)}) collective-permute-start(bf16[256,96]{0,1:T(8,128)(2,1)} %pad_maximum_fusion.10), channel_id=1, source_target_pairs={{0,48},{16,0},{32,16},{48,32},{64,112},{80,64},{96,80},{112,96},{1... | collective-permute-start | bytes 147464 | tf_op jit(solution)/shard_map/ppermute | solution.py:40
  19.7 3.5 %collective-permute-start.3 = (bf16[512,128]{1,0:T(8,128)(2,1)}, bf16[512,128]{1,0:T(8,128)(2,1)}, u32[]{:S(2)}, u32[]{:S(2)}) collective-permute-start(bf16[512,128]{1,0:T(8,128)(2,1)} %get-tuple-element.77), channel_id=1, source_target_pairs={{0,2},{1,3},{2,4},{3,5},{4,6},{5,7},{6,8},{7,9},{8,10},{9,11},{10,... | collective-permute-start | bytes 393224 | tf_op jit(solution)/shard_map/ppermute | solution.py:46
  23.2 5.7 %collective-permute-start.4 = (bf16[512,128]{1,0:T(8,128)(2,1)}, bf16[512,128]{1,0:T(8,128)(2,1)}, u32[]{:S(2)}, u32[]{:S(2)}) collective-permute-start(bf16[512,128]{1,0:T(8,128)(2,1)} %get-tuple-element.76), channel_id=1, source_target_pairs={{0,4},{1,5},{2,6},{3,7},{4,8},{5,9},{6,10},{7,11},{8,12},{9,13},{1... | collective-permute-start | bytes 393224 | tf_op jit(solution)/shard_map/ppermute | solution.py:46
  28.9 10.3 %all-to-all-start = ((bf16[8,160,256]{2,1,0:T(8,128)(2,1)}), bf16[8,160,256]{2,1,0:T(8,128)(2,1)}, u32[]{:S(2)}, u32[]{:S(2)}) async-start(bf16[8,160,256]{2,1,0:T(8,128)(2,1)} %broadcast_in_dim.9), calls=%async_computation | async-start | bytes 1310720 | tf_op jit(solution)/shard_map/all_to_all | solution.py:30
  41.8 2.3 collective-permute-start.5
  44.1 3.9 %collective-permute-start.6 = (bf16[512,128]{1,0:T(8,128)(2,1)}, bf16[512,128]{1,0:T(8,128)(2,1)}, u32[]{:S(2)}, u32[]{:S(2)}) collective-permute-start(bf16[512,128]{1,0:T(8,128)(2,1)} %get-tuple-element.74), channel_id=1, source_target_pairs={{0,14},{1,15},{2,0},{3,1},{4,2},{5,3},{6,4},{7,5},{8,6},{9,7},{10,... | collective-permute-start | bytes 393224 | tf_op jit(solution)/shard_map/ppermute | solution.py:46
  48.9 9.3 %all-to-all-done = bf16[8,160,256]{2,1,0:T(8,128)(2,1)} async-done(((bf16[8,160,256]{2,1,0:T(8,128)(2,1)}), bf16[8,160,256]{2,1,0:T(8,128)(2,1)}, u32[]{:S(2)}, u32[]{:S(2)}) %all-to-all-start) | async-done | bytes 655392 | tf_op jit(solution)/shard_map/all_to_all | solution.py:30
  58.3 2.5 fusion.2
  60.8 2.1 fusion
  62.9 3.1 %fusion.5 = f32[64,1024]{1,0:T(8,128)S(1)} fusion(f32[8,256,1024]{2,1,0:T(8,128)S(1)} %get-tuple-element.146, f32[1024]{0:T(1024)S(1)} %broadcast_maximum_fusion, s32[1024]{0:T(1024)S(1)} %add_select_fusion.1, s32[8,256]{1,0:T(8,128)S(1)} %add_select_fusion, bf16[8,160,256]{2,1,0:T(8,128)(2,1)} %all-to-all-done), kind=kOutput, calls=%fused_computation.11 | convolution fusion | flops 278921216 | bytes 8929280 | tf_op jit(solution)/shard_map/zvk,zkq->vq/dot_general | solution.py:159
  66.9 3.5 %all-to-all-start.1 = ((f32[4,72,256]{2,1,0:T(8,128)}), f32[4,72,256]{2,1,0:T(8,128)S(1)}, u32[]{:S(2)}, u32[]{:S(2)}) async-start(f32[4,72,256]{2,1,0:T(8,128)} %pad_maximum_fusion.7), calls=%async_computation.1 | async-start | bytes 589824 | tf_op jit(solution)/shard_map/all_to_all | solution.py:30
  70.6 6.5 %all-to-all-done.1 = f32[4,72,256]{2,1,0:T(8,128)S(1)} async-done(((f32[4,72,256]{2,1,0:T(8,128)}), f32[4,72,256]{2,1,0:T(8,128)S(1)}, u32[]{:S(2)}, u32[]{:S(2)}) %all-to-all-start.1) | async-done | bytes 294944 | tf_op jit(solution)/shard_map/all_to_all | solution.py:30
  77.3 15.0 %all_gather.3 = bf16[1024,256]{1,0:T(8,128)(2,1)S(1)} all-gather(bf16[64,256]{1,0:T(8,128)(2,1)S(1)} %fusion.134), channel_id=1, replica_groups=mesh['sp'=32,'tp'=16] {'tp'}, dimensions={0}, use_global_device_ids=true | all-gather | bytes 557056 | tf_op jit(solution)/shard_map/all_gather | solution.py:173
  93.8 3.9 %all-to-all-start.2 = ((bf16[32,32,128]{2,1,0:T(8,128)(2,1)}), bf16[32,32,128]{2,1,0:T(8,128)(2,1)S(1)}, u32[]{:S(2)}, u32[]{:S(2)}) async-start(bf16[32,32,128]{2,1,0:T(8,128)(2,1)} %bitcast.38), calls=%async_computation.2 | async-start | bytes 524288 | tf_op jit(solution)/shard_map/all_to_all | solution.py:30
  98.5 5.9 %collective-permute-start.7 = (bf16[512,128]{1,0:T(8,128)(2,1)}, bf16[512,128]{1,0:T(8,128)(2,1)S(1)}, u32[]{:S(2)}, u32[]{:S(2)}) collective-permute-start(bf16[512,128]{1,0:T(8,128)(2,1)} %get-tuple-element.28), channel_id=1, source_target_pairs={{0,6},{1,7},{2,8},{3,9},{4,10},{5,11},{6,12},{7,13},{8,14},{9,15},... | collective-permute-start | bytes 393224 | tf_op jit(solution)/shard_map/ppermute | solution.py:46
  104.4 2.9 %collective-permute-start.8 = (bf16[512,128]{1,0:T(8,128)(2,1)}, bf16[512,128]{1,0:T(8,128)(2,1)S(1)}, u32[]{:S(2)}, u32[]{:S(2)}) collective-permute-start(bf16[512,128]{1,0:T(8,128)(2,1)} %get-tuple-element.29), channel_id=1, source_target_pairs={{0,10},{1,11},{2,12},{3,13},{4,14},{5,15},{6,0},{7,1},{8,2},{9,3},... | collective-permute-start | bytes 393224 | tf_op jit(solution)/shard_map/ppermute | solution.py:46
  107.4 2.3 collective-permute-start.9
  111.8 11.9 %collective-permute-done.8 = bf16[512,128]{1,0:T(8,128)(2,1)S(1)} collective-permute-done((bf16[512,128]{1,0:T(8,128)(2,1)}, bf16[512,128]{1,0:T(8,128)(2,1)S(1)}, u32[]{:S(2)}, u32[]{:S(2)}) %collective-permute-start.8) | collective-permute-done | bytes 131104 | tf_op jit(solution)/shard_map/ppermute | solution.py:46
  124.4 4.4 %collective-permute-start.11 = (bf16[1024,128]{1,0:T(8,128)(2,1)S(1)}, bf16[1024,128]{1,0:T(8,128)(2,1)S(1)}, u32[]{:S(2)}, u32[]{:S(2)}) collective-permute-start(bf16[1024,128]{1,0:T(8,128)(2,1)S(1)} %bitcast.147), channel_id=1, source_target_pairs={{0,2},{1,3},{2,4},{3,5},{4,6},{5,7},{6,8},{7,9},{8,10},{9,11},{10,... | collective-permute-start | bytes 786440 | tf_op jit(solution)/shard_map/ppermute | solution.py:46
  135.4 2.5 collective-permute-done.12
  139.9 2.2 collective-permute-start.14
  142.2 3.6 %collective-permute-start.15 = (bf16[1024,128]{1,0:T(8,128)(2,1)S(1)}, bf16[1024,128]{1,0:T(8,128)(2,1)S(1)}, u32[]{:S(2)}, u32[]{:S(2)}) collective-permute-start(bf16[1024,128]{1,0:T(8,128)(2,1)S(1)} %collective-permute-done.12), channel_id=1, source_target_pairs={{0,14},{1,15},{2,0},{3,1},{4,2},{5,3},{6,4},{7,5},{8,6},{9,7},{10,... | collective-permute-start | bytes 786440 | tf_op jit(solution)/shard_map/ppermute | solution.py:46
  147.0 3.5 %collective-permute-done.14 = bf16[1024,128]{1,0:T(8,128)(2,1)S(1)} collective-permute-done((bf16[1024,128]{1,0:T(8,128)(2,1)S(1)}, bf16[1024,128]{1,0:T(8,128)(2,1)S(1)}, u32[]{:S(2)}, u32[]{:S(2)}) %collective-permute-start.14) | collective-permute-done | bytes 262176 | tf_op jit(solution)/shard_map/ppermute | solution.py:46
  154.5 2.9 %collective-permute-start.17 = (bf16[1024,128]{1,0:T(8,128)(2,1)S(1)}, bf16[1024,128]{1,0:T(8,128)(2,1)S(1)}, u32[]{:S(2)}, u32[]{:S(2)}) collective-permute-start(bf16[1024,128]{1,0:T(8,128)(2,1)S(1)} %collective-permute-done.14), channel_id=1, source_target_pairs={{0,2},{1,3},{2,4},{3,5},{4,6},{5,7},{6,8},{7,9},{8,10},{9,11},{10,... | collective-permute-start | bytes 786440 | tf_op jit(solution)/shard_map/ppermute | solution.py:46
  157.4 3.1 %collective-permute-start.18 = (bf16[1024,128]{1,0:T(8,128)(2,1)S(1)}, bf16[1024,128]{1,0:T(8,128)(2,1)S(1)}, u32[]{:S(2)}, u32[]{:S(2)}) collective-permute-start(bf16[1024,128]{1,0:T(8,128)(2,1)S(1)} %collective-permute-done.15), channel_id=1, source_target_pairs={{0,14},{1,15},{2,0},{3,1},{4,2},{5,3},{6,4},{7,5},{8,6},{9,7},{10,... | collective-permute-start | bytes 786440 | tf_op jit(solution)/shard_map/ppermute | solution.py:46
  161.0 4.1 %collective-permute-done.17 = bf16[1024,128]{1,0:T(8,128)(2,1)S(1)} collective-permute-done((bf16[1024,128]{1,0:T(8,128)(2,1)S(1)}, bf16[1024,128]{1,0:T(8,128)(2,1)S(1)}, u32[]{:S(2)}, u32[]{:S(2)}) %collective-permute-start.17) | collective-permute-done | bytes 262176 | tf_op jit(solution)/shard_map/ppermute | solution.py:46
  165.1 3.3 %collective-permute-start.20 = (bf16[512,128]{1,0:T(8,128)(2,1)S(1)}, bf16[512,128]{1,0:T(8,128)(2,1)S(1)}, u32[]{:S(2)}, u32[]{:S(2)}) collective-permute-start(bf16[512,128]{1,0:T(8,128)(2,1)S(1)} %slice.184), channel_id=1, source_target_pairs={{0,2},{1,3},{2,4},{3,5},{4,6},{5,7},{6,8},{7,9},{8,10},{9,11},{10,... | collective-permute-start | bytes 393224 | tf_op jit(solution)/shard_map/ppermute | solution.py:46
  168.9 3.1 %collective-permute-start.21 = (bf16[512,128]{1,0:T(8,128)(2,1)S(1)}, bf16[512,128]{1,0:T(8,128)(2,1)S(1)}, u32[]{:S(2)}, u32[]{:S(2)}) collective-permute-start(bf16[512,128]{1,0:T(8,128)(2,1)S(1)} %slice.185), channel_id=1, source_target_pairs={{0,14},{1,15},{2,0},{3,1},{4,2},{5,3},{6,4},{7,5},{8,6},{9,7},{10,... | collective-permute-start | bytes 393224 | tf_op jit(solution)/shard_map/ppermute | solution.py:46
  175.8 2.4 collective-permute-start.22
  189.3 3.8 %collective-permute-start.24 = (bf16[512,128]{1,0:T(8,128)(2,1)S(1)}, bf16[512,128]{1,0:T(8,128)(2,1)S(1)}, u32[]{:S(2)}, u32[]{:S(2)}) collective-permute-start(bf16[512,128]{1,0:T(8,128)(2,1)S(1)} %get-tuple-element.89), channel_id=1, source_target_pairs={{0,2},{1,3},{2,4},{3,5},{4,6},{5,7},{6,8},{7,9},{8,10},{9,11},{10,... | collective-permute-start | bytes 393224 | tf_op jit(solution)/shard_map/ppermute | solution.py:46
  193.2 3.2 %collective-permute-start.28 = (bf16[512,128]{1,0:T(8,128)(2,1)S(1)}, bf16[512,128]{1,0:T(8,128)(2,1)S(1)}, u32[]{:S(2)}, u32[]{:S(2)}) collective-permute-start(bf16[512,128]{1,0:T(8,128)(2,1)S(1)} %get-tuple-element.90), channel_id=1, source_target_pairs={{0,14},{1,15},{2,0},{3,1},{4,2},{5,3},{6,4},{7,5},{8,6},{9,7},{10,... | collective-permute-start | bytes 393224 | tf_op jit(solution)/shard_map/ppermute | solution.py:46
  198.6 2.8 %collective-permute-done.28 = bf16[512,128]{1,0:T(8,128)(2,1)S(1)} collective-permute-done((bf16[512,128]{1,0:T(8,128)(2,1)S(1)}, bf16[512,128]{1,0:T(8,128)(2,1)S(1)}, u32[]{:S(2)}, u32[]{:S(2)}) %collective-permute-start.28) | collective-permute-done | bytes 131104 | tf_op jit(solution)/shard_map/ppermute | solution.py:46
  201.6 3.6 %collective-permute-start.25 = (bf16[1024,128]{1,0:T(8,128)(2,1)S(1)}, bf16[1024,128]{1,0:T(8,128)(2,1)S(1)}, u32[]{:S(2)}, u32[]{:S(2)}) collective-permute-start(bf16[1024,128]{1,0:T(8,128)(2,1)S(1)} %get-tuple-element.53), channel_id=1, source_target_pairs={{0,2},{1,3},{2,4},{3,5},{4,6},{5,7},{6,8},{7,9},{8,10},{9,11},{10,... | collective-permute-start | bytes 786440 | tf_op jit(solution)/shard_map/ppermute | solution.py:46
  205.2 2.2 collective-permute-start.29
  207.4 3.4 %collective-permute-done.25 = bf16[1024,128]{1,0:T(8,128)(2,1)S(1)} collective-permute-done((bf16[1024,128]{1,0:T(8,128)(2,1)S(1)}, bf16[1024,128]{1,0:T(8,128)(2,1)S(1)}, u32[]{:S(2)}, u32[]{:S(2)}) %collective-permute-start.25) | collective-permute-done | bytes 262176 | tf_op jit(solution)/shard_map/ppermute | solution.py:46
  210.8 4.4 %collective-permute-done.29 = bf16[1024,128]{1,0:T(8,128)(2,1)S(1)} collective-permute-done((bf16[1024,128]{1,0:T(8,128)(2,1)S(1)}, bf16[1024,128]{1,0:T(8,128)(2,1)S(1)}, u32[]{:S(2)}, u32[]{:S(2)}) %collective-permute-start.29) | collective-permute-done | bytes 262176 | tf_op jit(solution)/shard_map/ppermute | solution.py:46
  215.4 3.8 %collective-permute-start.26 = (bf16[1024,128]{1,0:T(8,128)(2,1)S(1)}, bf16[1024,128]{1,0:T(8,128)(2,1)S(1)}, u32[]{:S(2)}, u32[]{:S(2)}) collective-permute-start(bf16[1024,128]{1,0:T(8,128)(2,1)S(1)} %get-tuple-element.51), channel_id=1, source_target_pairs={{0,2},{1,3},{2,4},{3,5},{4,6},{5,7},{6,8},{7,9},{8,10},{9,11},{10,... | collective-permute-start | bytes 786440 | tf_op jit(solution)/shard_map/ppermute | solution.py:46
  219.2 2.2 collective-permute-start.30
  221.4 2.7 %collective-permute-done.26 = bf16[1024,128]{1,0:T(8,128)(2,1)S(1)} collective-permute-done((bf16[1024,128]{1,0:T(8,128)(2,1)S(1)}, bf16[1024,128]{1,0:T(8,128)(2,1)S(1)}, u32[]{:S(2)}, u32[]{:S(2)}) %collective-permute-start.26) | collective-permute-done | bytes 262176 | tf_op jit(solution)/shard_map/ppermute | solution.py:46
  224.2 3.3 %collective-permute-done.30 = bf16[1024,128]{1,0:T(8,128)(2,1)S(1)} collective-permute-done((bf16[1024,128]{1,0:T(8,128)(2,1)S(1)}, bf16[1024,128]{1,0:T(8,128)(2,1)S(1)}, u32[]{:S(2)}, u32[]{:S(2)}) %collective-permute-start.30) | collective-permute-done | bytes 262176 | tf_op jit(solution)/shard_map/ppermute | solution.py:46
  227.6 3.5 %collective-permute-start.27 = (bf16[1024,128]{1,0:T(8,128)(2,1)S(1)}, bf16[1024,128]{1,0:T(8,128)(2,1)S(1)}, u32[]{:S(2)}, u32[]{:S(2)}) collective-permute-start(bf16[1024,128]{1,0:T(8,128)(2,1)S(1)} %get-tuple-element.49), channel_id=1, source_target_pairs={{0,2},{1,3},{2,4},{3,5},{4,6},{5,7},{6,8},{7,9},{8,10},{9,11},{10,... | collective-permute-start | bytes 786440 | tf_op jit(solution)/shard_map/ppermute | solution.py:46
  231.1 2.4 collective-permute-start.31
  233.5 2.4 collective-permute-done.27
  235.9 3.5 %collective-permute-done.31 = bf16[1024,128]{1,0:T(8,128)(2,1)S(1)} collective-permute-done((bf16[1024,128]{1,0:T(8,128)(2,1)S(1)}, bf16[1024,128]{1,0:T(8,128)(2,1)S(1)}, u32[]{:S(2)}, u32[]{:S(2)}) %collective-permute-start.31) | collective-permute-done | bytes 262176 | tf_op jit(solution)/shard_map/ppermute | solution.py:46
  240.1 9.2 %all-to-all-start.3 = ((bf16[32,32,128]{2,1,0:T(8,128)(2,1)}), bf16[32,32,128]{2,1,0:T(8,128)(2,1)S(1)}, u32[]{:S(2)}, u32[]{:S(2)}) async-start(bf16[32,32,128]{2,1,0:T(8,128)(2,1)} %bitcast.74), calls=%async_computation.3 | async-start | bytes 524288 | tf_op jit(solution)/shard_map/all_to_all | solution.py:30
  249.4 11.3 %all-to-all-done.3 = bf16[32,32,128]{2,1,0:T(8,128)(2,1)S(1)} async-done(((bf16[32,32,128]{2,1,0:T(8,128)(2,1)}), bf16[32,32,128]{2,1,0:T(8,128)(2,1)S(1)}, u32[]{:S(2)}, u32[]{:S(2)}) %all-to-all-start.3) | async-done | bytes 262176 | tf_op jit(solution)/shard_map/all_to_all | solution.py:30
  (196 shorter events, 51.2 us)
Async XLA Ops:
  0.0 92.4 %copy-start = (bf16[1024,128]{1,0:T(8,128)(2,1)S(1)}, bf16[1024,128]{1,0:T(8,128)(2,1)}, u32[]{:S(2)}) copy-start(bf16[1024,128]{1,0:T(8,128)(2,1)} %param.19) | copy-start | bytes 786436
  6.9 34.9 %collective-permute-start = (bf16[256,96]{0,1:T(8,128)(2,1)}, bf16[256,96]{0,1:T(8,128)(2,1)}, u32[]{:S(2)}, u32[]{:S(2)}) collective-permute-start(bf16[256,96]{0,1:T(8,128)(2,1)} %pad_maximum_fusion.10), channel_id=1, source_target_pairs={{0,16},{16,32},{32,48},{48,0},{64,80},{80,96},{96,112},{112,64},{1... | collective-permute-start | bytes 147464 | tf_op jit(solution)/shard_map/ppermute | solution.py:40
  10.3 33.8 %collective-permute-start.1 = (bf16[256,96]{0,1:T(8,128)(2,1)}, bf16[256,96]{0,1:T(8,128)(2,1)}, u32[]{:S(2)}, u32[]{:S(2)}) collective-permute-start(bf16[256,96]{0,1:T(8,128)(2,1)} %pad_maximum_fusion.10), channel_id=1, source_target_pairs={{0,32},{16,48},{32,0},{48,16},{64,96},{80,112},{96,64},{112,80},{1... | collective-permute-start | bytes 147464 | tf_op jit(solution)/shard_map/ppermute | solution.py:40
  14.9 33.0 %collective-permute-start.2 = (bf16[256,96]{0,1:T(8,128)(2,1)}, bf16[256,96]{0,1:T(8,128)(2,1)}, u32[]{:S(2)}, u32[]{:S(2)}) collective-permute-start(bf16[256,96]{0,1:T(8,128)(2,1)} %pad_maximum_fusion.10), channel_id=1, source_target_pairs={{0,48},{16,0},{32,16},{48,32},{64,112},{80,64},{96,80},{112,96},{1... | collective-permute-start | bytes 147464 | tf_op jit(solution)/shard_map/ppermute | solution.py:40
  19.7 57.5 %collective-permute-start.3 = (bf16[512,128]{1,0:T(8,128)(2,1)}, bf16[512,128]{1,0:T(8,128)(2,1)}, u32[]{:S(2)}, u32[]{:S(2)}) collective-permute-start(bf16[512,128]{1,0:T(8,128)(2,1)} %get-tuple-element.77), channel_id=1, source_target_pairs={{0,2},{1,3},{2,4},{3,5},{4,6},{5,7},{6,8},{7,9},{8,10},{9,11},{10,... | collective-permute-start | bytes 393224 | tf_op jit(solution)/shard_map/ppermute | solution.py:46
  23.2 54.1 %collective-permute-start.4 = (bf16[512,128]{1,0:T(8,128)(2,1)}, bf16[512,128]{1,0:T(8,128)(2,1)}, u32[]{:S(2)}, u32[]{:S(2)}) collective-permute-start(bf16[512,128]{1,0:T(8,128)(2,1)} %get-tuple-element.76), channel_id=1, source_target_pairs={{0,4},{1,5},{2,6},{3,7},{4,8},{5,9},{6,10},{7,11},{8,12},{9,13},{1... | collective-permute-start | bytes 393224 | tf_op jit(solution)/shard_map/ppermute | solution.py:46
  28.9 29.3 %all-to-all-start = ((bf16[8,160,256]{2,1,0:T(8,128)(2,1)}), bf16[8,160,256]{2,1,0:T(8,128)(2,1)}, u32[]{:S(2)}, u32[]{:S(2)}) async-start(bf16[8,160,256]{2,1,0:T(8,128)(2,1)} %broadcast_in_dim.9), calls=%async_computation | async-start | bytes 1310720 | tf_op jit(solution)/shard_map/all_to_all | solution.py:30
  41.8 35.5 %collective-permute-start.5 = (bf16[512,128]{1,0:T(8,128)(2,1)}, bf16[512,128]{1,0:T(8,128)(2,1)}, u32[]{:S(2)}, u32[]{:S(2)}) collective-permute-start(bf16[512,128]{1,0:T(8,128)(2,1)} %get-tuple-element.75), channel_id=1, source_target_pairs={{0,8},{1,9},{2,10},{3,11},{4,12},{5,13},{6,14},{7,15},{8,0},{9,1},... | collective-permute-start | bytes 393224 | tf_op jit(solution)/shard_map/ppermute | solution.py:46
  44.1 33.3 %collective-permute-start.6 = (bf16[512,128]{1,0:T(8,128)(2,1)}, bf16[512,128]{1,0:T(8,128)(2,1)}, u32[]{:S(2)}, u32[]{:S(2)}) collective-permute-start(bf16[512,128]{1,0:T(8,128)(2,1)} %get-tuple-element.74), channel_id=1, source_target_pairs={{0,14},{1,15},{2,0},{3,1},{4,2},{5,3},{6,4},{7,5},{8,6},{9,7},{10,... | collective-permute-start | bytes 393224 | tf_op jit(solution)/shard_map/ppermute | solution.py:46
  66.0 26.3 %copy-start.19 = (bf16[256,128]{1,0:T(8,128)(2,1)S(1)}, bf16[256,128]{1,0:T(8,128)(2,1)}, u32[]{:S(2)}) copy-start(bf16[256,128]{1,0:T(8,128)(2,1)} %param.20) | copy-start | bytes 196612
  66.9 10.3 %all-to-all-start.1 = ((f32[4,72,256]{2,1,0:T(8,128)}), f32[4,72,256]{2,1,0:T(8,128)S(1)}, u32[]{:S(2)}, u32[]{:S(2)}) async-start(f32[4,72,256]{2,1,0:T(8,128)} %pad_maximum_fusion.7), calls=%async_computation.1 | async-start | bytes 589824 | tf_op jit(solution)/shard_map/all_to_all | solution.py:30
  70.3 27.5 %copy-start.22 = (bf16[2048]{0:T(1024)(128)(2,1)S(1)}, bf16[2048]{0:T(1024)(128)(2,1)}, u32[]{:S(2)}) copy-start(bf16[2048]{0:T(1024)(128)(2,1)} %param.21) | copy-start | bytes 12292
  70.4 37.1 %copy-start.5 = (bf16[512,128]{1,0:T(8,128)(2,1)S(1)}, bf16[512,128]{1,0:T(8,128)(2,1)}, u32[]{:S(2)}) copy-start(bf16[512,128]{1,0:T(8,128)(2,1)} %get-tuple-element.30) | copy-start | bytes 393220
  93.8 30.6 %all-to-all-start.2 = ((bf16[32,32,128]{2,1,0:T(8,128)(2,1)}), bf16[32,32,128]{2,1,0:T(8,128)(2,1)S(1)}, u32[]{:S(2)}, u32[]{:S(2)}) async-start(bf16[32,32,128]{2,1,0:T(8,128)(2,1)} %bitcast.38), calls=%async_computation.2 | async-start | bytes 524288 | tf_op jit(solution)/shard_map/all_to_all | solution.py:30
  98.5 13.2 %collective-permute-start.7 = (bf16[512,128]{1,0:T(8,128)(2,1)}, bf16[512,128]{1,0:T(8,128)(2,1)S(1)}, u32[]{:S(2)}, u32[]{:S(2)}) collective-permute-start(bf16[512,128]{1,0:T(8,128)(2,1)} %get-tuple-element.28), channel_id=1, source_target_pairs={{0,6},{1,7},{2,8},{3,9},{4,10},{5,11},{6,12},{7,13},{8,14},{9,15},... | collective-permute-start | bytes 393224 | tf_op jit(solution)/shard_map/ppermute | solution.py:46
  104.4 19.3 %collective-permute-start.8 = (bf16[512,128]{1,0:T(8,128)(2,1)}, bf16[512,128]{1,0:T(8,128)(2,1)S(1)}, u32[]{:S(2)}, u32[]{:S(2)}) collective-permute-start(bf16[512,128]{1,0:T(8,128)(2,1)} %get-tuple-element.29), channel_id=1, source_target_pairs={{0,10},{1,11},{2,12},{3,13},{4,14},{5,15},{6,0},{7,1},{8,2},{9,3},... | collective-permute-start | bytes 393224 | tf_op jit(solution)/shard_map/ppermute | solution.py:46
  107.4 16.9 %collective-permute-start.9 = (bf16[512,128]{1,0:T(8,128)(2,1)S(1)}, bf16[512,128]{1,0:T(8,128)(2,1)}, u32[]{:S(2)}, u32[]{:S(2)}) collective-permute-start(bf16[512,128]{1,0:T(8,128)(2,1)S(1)} %copy-done.5), channel_id=1, source_target_pairs={{0,12},{1,13},{2,14},{3,15},{4,0},{5,1},{6,2},{7,3},{8,4},{9,5},{1... | collective-permute-start | bytes 393224 | tf_op jit(solution)/shard_map/ppermute | solution.py:46
  111.0 34.8 %copy-start.36 = (f32[128]{0:T(128)S(1)}, f32[128]{0:T(128)}, u32[]{:S(2)}) copy-start(f32[128]{0:T(128)} %get-tuple-element.134) | copy-start | bytes 1540
  111.0 35.1 %copy-start.35 = (f32[128]{0:T(128)S(1)}, f32[128]{0:T(128)}, u32[]{:S(2)}) copy-start(f32[128]{0:T(128)} %get-tuple-element.135) | copy-start | bytes 1540
  124.4 11.0 %collective-permute-start.11 = (bf16[1024,128]{1,0:T(8,128)(2,1)S(1)}, bf16[1024,128]{1,0:T(8,128)(2,1)S(1)}, u32[]{:S(2)}, u32[]{:S(2)}) collective-permute-start(bf16[1024,128]{1,0:T(8,128)(2,1)S(1)} %bitcast.147), channel_id=1, source_target_pairs={{0,2},{1,3},{2,4},{3,5},{4,6},{5,7},{6,8},{7,9},{8,10},{9,11},{10,... | collective-permute-start | bytes 786440 | tf_op jit(solution)/shard_map/ppermute | solution.py:46
  128.8 9.2 %collective-permute-start.12 = (bf16[1024,128]{1,0:T(8,128)(2,1)S(1)}, bf16[1024,128]{1,0:T(8,128)(2,1)S(1)}, u32[]{:S(2)}, u32[]{:S(2)}) collective-permute-start(bf16[1024,128]{1,0:T(8,128)(2,1)S(1)} %bitcast.148), channel_id=1, source_target_pairs={{0,14},{1,15},{2,0},{3,1},{4,2},{5,3},{6,4},{7,5},{8,6},{9,7},{10,... | collective-permute-start | bytes 786440 | tf_op jit(solution)/shard_map/ppermute | solution.py:46
  130.7 15.3 %collective-permute-start.10 = (bf16[1024,128]{1,0:T(8,128)(2,1)S(1)}, bf16[1024,128]{1,0:T(8,128)(2,1)S(1)}, u32[]{:S(2)}, u32[]{:S(2)}) collective-permute-start(bf16[1024,128]{1,0:T(8,128)(2,1)S(1)} %bitcast.149), channel_id=1, source_target_pairs={{0,1},{1,0},{2,3},{3,2},{4,5},{5,4},{6,7},{7,6},{8,9},{9,8},{10,11... | collective-permute-start | bytes 786440 | tf_op jit(solution)/shard_map/ppermute | solution.py:36
  138.0 36.4 %collective-permute-start.13 = (bf16[1024,256]{1,0:T(8,128)(2,1)S(1)}, bf16[1024,256]{1,0:T(8,128)(2,1)S(1)}, u32[]{:S(2)}, u32[]{:S(2)}) collective-permute-start(bf16[1024,256]{1,0:T(8,128)(2,1)S(1)} %pad_maximum_fusion.4), channel_id=1, source_target_pairs={{0,1},{1,0},{2,3},{3,2},{4,5},{5,4},{6,7},{7,6},{8,9},{9,8},{10,11... | collective-permute-start | bytes 1572872 | tf_op jit(solution)/shard_map/ppermute | solution.py:36
  139.9 10.6 %collective-permute-start.14 = (bf16[1024,128]{1,0:T(8,128)(2,1)S(1)}, bf16[1024,128]{1,0:T(8,128)(2,1)S(1)}, u32[]{:S(2)}, u32[]{:S(2)}) collective-permute-start(bf16[1024,128]{1,0:T(8,128)(2,1)S(1)} %collective-permute-done.11), channel_id=1, source_target_pairs={{0,2},{1,3},{2,4},{3,5},{4,6},{5,7},{6,8},{7,9},{8,10},{9,11},{10,... | collective-permute-start | bytes 786440 | tf_op jit(solution)/shard_map/ppermute | solution.py:46
  142.2 10.3 %collective-permute-start.15 = (bf16[1024,128]{1,0:T(8,128)(2,1)S(1)}, bf16[1024,128]{1,0:T(8,128)(2,1)S(1)}, u32[]{:S(2)}, u32[]{:S(2)}) collective-permute-start(bf16[1024,128]{1,0:T(8,128)(2,1)S(1)} %collective-permute-done.12), channel_id=1, source_target_pairs={{0,14},{1,15},{2,0},{3,1},{4,2},{5,3},{6,4},{7,5},{8,6},{9,7},{10,... | collective-permute-start | bytes 786440 | tf_op jit(solution)/shard_map/ppermute | solution.py:46
  146.8 27.1 %copy-start.31 = (f32[128]{0:T(128)S(1)}, f32[128]{0:T(128)}, u32[]{:S(2)}) copy-start(f32[128]{0:T(128)} %get-tuple-element.126) | copy-start | bytes 1540
  147.0 27.1 %copy-start.30 = (f32[128]{0:T(128)S(1)}, f32[128]{0:T(128)}, u32[]{:S(2)}) copy-start(f32[128]{0:T(128)} %get-tuple-element.125) | copy-start | bytes 1540
  152.5 21.8 %copy-start.26 = (f32[128]{0:T(128)S(1)}, f32[128]{0:T(128)}, u32[]{:S(2)}) copy-start(f32[128]{0:T(128)} %get-tuple-element.131) | copy-start | bytes 1540
  152.6 25.9 %collective-permute-start.16 = (bf16[1024,256]{1,0:T(8,128)(2,1)S(1)}, bf16[1024,256]{1,0:T(8,128)(2,1)S(1)}, u32[]{:S(2)}, u32[]{:S(2)}) collective-permute-start(bf16[1024,256]{1,0:T(8,128)(2,1)S(1)} %pad_maximum_fusion.5), channel_id=1, source_target_pairs={{0,1},{1,0},{2,3},{3,2},{4,5},{5,4},{6,7},{7,6},{8,9},{9,8},{10,11... | collective-permute-start | bytes 1572872 | tf_op jit(solution)/shard_map/ppermute | solution.py:36
  154.5 10.6 %collective-permute-start.17 = (bf16[1024,128]{1,0:T(8,128)(2,1)S(1)}, bf16[1024,128]{1,0:T(8,128)(2,1)S(1)}, u32[]{:S(2)}, u32[]{:S(2)}) collective-permute-start(bf16[1024,128]{1,0:T(8,128)(2,1)S(1)} %collective-permute-done.14), channel_id=1, source_target_pairs={{0,2},{1,3},{2,4},{3,5},{4,6},{5,7},{6,8},{7,9},{8,10},{9,11},{10,... | collective-permute-start | bytes 786440 | tf_op jit(solution)/shard_map/ppermute | solution.py:46
  157.4 11.4 %collective-permute-start.18 = (bf16[1024,128]{1,0:T(8,128)(2,1)S(1)}, bf16[1024,128]{1,0:T(8,128)(2,1)S(1)}, u32[]{:S(2)}, u32[]{:S(2)}) collective-permute-start(bf16[1024,128]{1,0:T(8,128)(2,1)S(1)} %collective-permute-done.15), channel_id=1, source_target_pairs={{0,14},{1,15},{2,0},{3,1},{4,2},{5,3},{6,4},{7,5},{8,6},{9,7},{10,... | collective-permute-start | bytes 786440 | tf_op jit(solution)/shard_map/ppermute | solution.py:46
  165.1 10.5 %collective-permute-start.20 = (bf16[512,128]{1,0:T(8,128)(2,1)S(1)}, bf16[512,128]{1,0:T(8,128)(2,1)S(1)}, u32[]{:S(2)}, u32[]{:S(2)}) collective-permute-start(bf16[512,128]{1,0:T(8,128)(2,1)S(1)} %slice.184), channel_id=1, source_target_pairs={{0,2},{1,3},{2,4},{3,5},{4,6},{5,7},{6,8},{7,9},{8,10},{9,11},{10,... | collective-permute-start | bytes 393224 | tf_op jit(solution)/shard_map/ppermute | solution.py:46
  168.9 7.0 %collective-permute-start.21 = (bf16[512,128]{1,0:T(8,128)(2,1)S(1)}, bf16[512,128]{1,0:T(8,128)(2,1)S(1)}, u32[]{:S(2)}, u32[]{:S(2)}) collective-permute-start(bf16[512,128]{1,0:T(8,128)(2,1)S(1)} %slice.185), channel_id=1, source_target_pairs={{0,14},{1,15},{2,0},{3,1},{4,2},{5,3},{6,4},{7,5},{8,6},{9,7},{10,... | collective-permute-start | bytes 393224 | tf_op jit(solution)/shard_map/ppermute | solution.py:46
  172.0 8.0 %collective-permute-start.19 = (bf16[1024,256]{1,0:T(8,128)(2,1)S(1)}, bf16[1024,256]{1,0:T(8,128)(2,1)S(1)}, u32[]{:S(2)}, u32[]{:S(2)}) collective-permute-start(bf16[1024,256]{1,0:T(8,128)(2,1)S(1)} %pad_maximum_fusion.6), channel_id=1, source_target_pairs={{0,1},{1,0},{2,3},{3,2},{4,5},{5,4},{6,7},{7,6},{8,9},{9,8},{10,11... | collective-permute-start | bytes 1572872 | tf_op jit(solution)/shard_map/ppermute | solution.py:36
  175.8 3.9 %collective-permute-start.22 = (bf16[1024,128]{1,0:T(8,128)(2,1)S(1)}, bf16[1024,128]{1,0:T(8,128)(2,1)S(1)}, u32[]{:S(2)}, u32[]{:S(2)}) collective-permute-start(bf16[1024,128]{1,0:T(8,128)(2,1)S(1)} %constant_dynamic-update-slice_fusion), channel_id=1, source_target_pairs={{0,1},{1,0},{2,3},{3,2},{4,5},{5,4},{6,7},{7,6},{8,9},{9,8},{10,11... | collective-permute-start | bytes 786440 | tf_op jit(solution)/shard_map/ppermute | solution.py:36
  182.2 5.8 %collective-permute-start.23 = (bf16[1024,256]{0,1:T(8,128)(2,1)S(1)}, bf16[1024,256]{0,1:T(8,128)(2,1)S(1)}, u32[]{:S(2)}, u32[]{:S(2)}) collective-permute-start(bf16[1024,256]{0,1:T(8,128)(2,1)S(1)} %fusion.13), channel_id=1, source_target_pairs={{0,1},{1,0},{2,3},{3,2},{4,5},{5,4},{6,7},{7,6},{8,9},{9,8},{10,11... | collective-permute-start | bytes 1572872 | tf_op jit(solution)/shard_map/ppermute | solution.py:36
  189.3 9.3 %collective-permute-start.24 = (bf16[512,128]{1,0:T(8,128)(2,1)S(1)}, bf16[512,128]{1,0:T(8,128)(2,1)S(1)}, u32[]{:S(2)}, u32[]{:S(2)}) collective-permute-start(bf16[512,128]{1,0:T(8,128)(2,1)S(1)} %get-tuple-element.89), channel_id=1, source_target_pairs={{0,2},{1,3},{2,4},{3,5},{4,6},{5,7},{6,8},{7,9},{8,10},{9,11},{10,... | collective-permute-start | bytes 393224 | tf_op jit(solution)/shard_map/ppermute | solution.py:46
  193.2 8.3 %collective-permute-start.28 = (bf16[512,128]{1,0:T(8,128)(2,1)S(1)}, bf16[512,128]{1,0:T(8,128)(2,1)S(1)}, u32[]{:S(2)}, u32[]{:S(2)}) collective-permute-start(bf16[512,128]{1,0:T(8,128)(2,1)S(1)} %get-tuple-element.90), channel_id=1, source_target_pairs={{0,14},{1,15},{2,0},{3,1},{4,2},{5,3},{6,4},{7,5},{8,6},{9,7},{10,... | collective-permute-start | bytes 393224 | tf_op jit(solution)/shard_map/ppermute | solution.py:46
  201.6 9.3 %collective-permute-start.25 = (bf16[1024,128]{1,0:T(8,128)(2,1)S(1)}, bf16[1024,128]{1,0:T(8,128)(2,1)S(1)}, u32[]{:S(2)}, u32[]{:S(2)}) collective-permute-start(bf16[1024,128]{1,0:T(8,128)(2,1)S(1)} %get-tuple-element.53), channel_id=1, source_target_pairs={{0,2},{1,3},{2,4},{3,5},{4,6},{5,7},{6,8},{7,9},{8,10},{9,11},{10,... | collective-permute-start | bytes 786440 | tf_op jit(solution)/shard_map/ppermute | solution.py:46
  205.2 10.1 %collective-permute-start.29 = (bf16[1024,128]{1,0:T(8,128)(2,1)S(1)}, bf16[1024,128]{1,0:T(8,128)(2,1)S(1)}, u32[]{:S(2)}, u32[]{:S(2)}) collective-permute-start(bf16[1024,128]{1,0:T(8,128)(2,1)S(1)} %get-tuple-element.54), channel_id=1, source_target_pairs={{0,14},{1,15},{2,0},{3,1},{4,2},{5,3},{6,4},{7,5},{8,6},{9,7},{10,... | collective-permute-start | bytes 786440 | tf_op jit(solution)/shard_map/ppermute | solution.py:46
  215.4 34.0 %copy-start.20 = (f32[256,2]{0,1:T(2,128)S(1)}, f32[256,2]{0,1:T(2,128)}, u32[]{:S(2)}) copy-start(f32[256,2]{0,1:T(2,128)} %param.23) | copy-start | bytes 6148
  215.4 34.0 %copy-start.37 = (f32[256]{0:T(256)S(1)}, f32[256]{0:T(256)}, u32[]{:S(2)}) copy-start(f32[256]{0:T(256)} %param.24) | copy-start | bytes 3076
  215.4 45.3 %copy-start.4 = (bf16[256,128]{1,0:T(8,128)(2,1)S(1)}, bf16[256,128]{1,0:T(8,128)(2,1)}, u32[]{:S(2)}) copy-start(bf16[256,128]{1,0:T(8,128)(2,1)} %copy-done.3) | copy-start | bytes 196612
  215.4 8.7 %collective-permute-start.26 = (bf16[1024,128]{1,0:T(8,128)(2,1)S(1)}, bf16[1024,128]{1,0:T(8,128)(2,1)S(1)}, u32[]{:S(2)}, u32[]{:S(2)}) collective-permute-start(bf16[1024,128]{1,0:T(8,128)(2,1)S(1)} %get-tuple-element.51), channel_id=1, source_target_pairs={{0,2},{1,3},{2,4},{3,5},{4,6},{5,7},{6,8},{7,9},{8,10},{9,11},{10,... | collective-permute-start | bytes 786440 | tf_op jit(solution)/shard_map/ppermute | solution.py:46
  219.2 8.3 %collective-permute-start.30 = (bf16[1024,128]{1,0:T(8,128)(2,1)S(1)}, bf16[1024,128]{1,0:T(8,128)(2,1)S(1)}, u32[]{:S(2)}, u32[]{:S(2)}) collective-permute-start(bf16[1024,128]{1,0:T(8,128)(2,1)S(1)} %get-tuple-element.52), channel_id=1, source_target_pairs={{0,14},{1,15},{2,0},{3,1},{4,2},{5,3},{6,4},{7,5},{8,6},{9,7},{10,... | collective-permute-start | bytes 786440 | tf_op jit(solution)/shard_map/ppermute | solution.py:46
  227.6 8.3 %collective-permute-start.27 = (bf16[1024,128]{1,0:T(8,128)(2,1)S(1)}, bf16[1024,128]{1,0:T(8,128)(2,1)S(1)}, u32[]{:S(2)}, u32[]{:S(2)}) collective-permute-start(bf16[1024,128]{1,0:T(8,128)(2,1)S(1)} %get-tuple-element.49), channel_id=1, source_target_pairs={{0,2},{1,3},{2,4},{3,5},{4,6},{5,7},{6,8},{7,9},{8,10},{9,11},{10,... | collective-permute-start | bytes 786440 | tf_op jit(solution)/shard_map/ppermute | solution.py:46
  231.1 8.3 %collective-permute-start.31 = (bf16[1024,128]{1,0:T(8,128)(2,1)S(1)}, bf16[1024,128]{1,0:T(8,128)(2,1)S(1)}, u32[]{:S(2)}, u32[]{:S(2)}) collective-permute-start(bf16[1024,128]{1,0:T(8,128)(2,1)S(1)} %get-tuple-element.50), channel_id=1, source_target_pairs={{0,14},{1,15},{2,0},{3,1},{4,2},{5,3},{6,4},{7,5},{8,6},{9,7},{10,... | collective-permute-start | bytes 786440 | tf_op jit(solution)/shard_map/ppermute | solution.py:46
  240.1 20.6 %all-to-all-start.3 = ((bf16[32,32,128]{2,1,0:T(8,128)(2,1)}), bf16[32,32,128]{2,1,0:T(8,128)(2,1)S(1)}, u32[]{:S(2)}, u32[]{:S(2)}) async-start(bf16[32,32,128]{2,1,0:T(8,128)(2,1)} %bitcast.74), calls=%async_computation.3 | async-start | bytes 524288 | tf_op jit(solution)/shard_map/all_to_all | solution.py:30
  (26 other events, 233.2 us)
where the time goes:
time: 264 us; the launch traced here: 262 us
  starting transfers between devices  126 us (48%)
  waiting for transfers between devices  76.1 us (29%)
  other arithmetic  16.1 us (6%)
  matrix products  15.9 us (6%)
  blocking collectives  15 us (6%)
  local copies, waits for them, and re-layouts  11.2 us (4%)
    ppermute x23, starting transfers between devices, y_step(): lax.ppermute(value, 'tp', [(t, (t + 2 * by) % TP) for t in range(TP)])  75.8 us
    ppermute x23, waiting for transfers between devices, y_step(): lax.ppermute(value, 'tp', [(t, (t + 2 * by) % TP) for t in range(TP)])  48.9 us
    all_to_all x4, waiting for transfers between devices, exchange(): lax.all_to_all(value, axis, split_axis=0, concat_axis=0, tiled=True, axis...  27.2 us
    all_to_all x4, starting transfers between devices, exchange(): lax.all_to_all(value, axis, split_axis=0, concat_axis=0, tiled=True, axis...  26.9 us
    all_gather x1, blocking collectives, body(): attended_all = lax.all_gather(attended, 'tp', axis=0, tiled=True)  15 us
    ppermute x6, starting transfers between devices, swap(): return lax.ppermute(value, 'tp', [(t, t ^ 1) for t in range(TP)])  12 us
    ppermute x3, starting transfers between devices, x_shift(): lax.ppermute(value, 'sp', [(s, s // X * X + (s + by) % X) for s in range(...  11.4 us
    unnamed x84, local copies, waits for them, and re-layouts  6.44 us
  transfers between devices with their start and end apart: 36, of which 19 were waited for; matrix products, arithmetic and copies ran while one was open for 11% of the time, Pallas kernels for 0%

commit v1 on v0

--- a/solution.py
+++ b/solution.py
@@ -18,12 +18,10 @@
 THETA = 500000.0
 EPSILON = 1e-06
 
-EARLY = (4, 1, 7, 2)
-LATE = (6, 3, 5)
-
 
 Z_GROUPS = [[z * X + x for z in range(Z)] for x in range(X)]
 X_GROUPS = [[z * X + x for x in range(X)] for z in range(Z)]
+Y_GROUPS = [[y * 2 + c for y in range(Y)] for c in range(2)]
 
 
 def exchange(value, axis, groups=None):
@@ -105,10 +103,7 @@
     rotated = rotate(rope_key, positions).T
     block = jnp.concatenate([key_value[:NOPE], rotated, key_value[NOPE:]], axis=0)
     query = jnp.concatenate([queries[:, :NOPE], rotate(queries[:, NOPE:], positions)], axis=1)
-    copies, query = lax.optimization_barrier(
-        (jnp.broadcast_to(block, (Z,) + block.shape), query)
-    )
-    blocks = exchange(copies, "sp", Z_GROUPS)
+    blocks = lax.all_gather(block, "sp", axis=0, tiled=False, axis_index_groups=Z_GROUPS)
 
     query_parts = [query]
     for by in range(1, X):
@@ -121,12 +116,7 @@
         [gate_weight.reshape(TP, width, ff), up_weight.reshape(TP, width, ff)], axis=2
     )
     gains = ffn_gain.astype(f32).reshape(TP, width)
-    down = down_weight.reshape(Y, 2, ff, width)
-    down = jnp.where(core == 0, down, down[:, ::-1]).reshape(Y, 2 * ff, width)
-    down_parts = {0: at(down, y)}
-    for by in EARLY:
-        down_parts[by] = y_step(at(down, (y + by) % Y), by)
-    late = {by: at(down, (y + by) % Y) for by in LATE}
+    down = exchange(down_weight.reshape(Y, 2 * ff, width), "tp", Y_GROUPS)
 
     experts = SP
     capacity = 2 * tokens * TOP // experts
@@ -161,13 +151,14 @@
     )
     packed = jnp.concatenate([summed, top, total, jnp.zeros((6, X * tokens), f32)], axis=0)
     packed = jnp.stack([packed[:, i * tokens : (i + 1) * tokens] for i in range(X)])
+    packed, down = lax.optimization_barrier((packed, down))
     packed = exchange(packed, "sp", X_GROUPS)
     tops = packed[:, VDIM]
     factors = jnp.exp(tops - jnp.max(tops, axis=0, keepdims=True))
     merged = jnp.sum(factors[:, None, :] * packed, axis=0)
     attended = (merged[:VDIM] / merged[VDIM + 1 : VDIM + 2]).astype(bf16)
-    attended, gate_up_weight, down_parts, placed = lax.optimization_barrier(
-        (attended, gate_up_weight, down_parts, placed)
+    attended, gate_up_weight, placed = lax.optimization_barrier(
+        (attended, gate_up_weight, placed)
     )
 
     attended_all = lax.all_gather(attended, "tp", axis=0, tiled=True)
@@ -177,12 +168,14 @@
     mixed = (residual.astype(f32) + projected).astype(bf16)
 
     sent = lax.dot_general(placed, mixed, (((0,), (0,)), ((), ())), preferred_element_type=f32)
-    sent, late = lax.optimization_barrier((sent.astype(bf16), late))
-    arrived = exchange(sent.reshape(SP, capacity, width), "sp").reshape(slots, width)
-    for by in LATE:
-        late[by] = y_step(late[by], by)
-    arrived, late = lax.optimization_barrier((arrived, late))
-    down_parts = {**down_parts, **late}
+    arrived = exchange(sent.astype(bf16).reshape(SP, capacity, width), "sp")
+    down = down.reshape(Y, 2, ff, width)
+    down = jnp.where(core == 0, down, down[:, ::-1]).reshape(Y, 2 * ff, width)
+    features = lambda steps: jnp.concatenate([at(down, (y + k) % Y) for k in steps], axis=1)
+    down_first, down_above, down_below = features([4]), features([3, 2, 1]), features([-3, -2, -1, 0])
+    arrived, down_first, down_above, down_below = lax.optimization_barrier(
+        (arrived.reshape(slots, width), down_first, down_above, down_below)
+    )
 
     def products(parts):
         scaled, weights, squares = [], [], 0.0
@@ -227,22 +220,17 @@
     hidden = (jax.nn.silu(gate_up[:, :ff]) * gate_up[:, ff:]).astype(bf16)
 
     hidden = jnp.concatenate([hidden, swap(hidden)], axis=1)
-    first = jnp.dot(hidden, down_parts[4], preferred_element_type=f32).astype(bf16)
-    order = (3, 5, 2, 6, 1, 7, 0)
-    rest = jnp.dot(
-        hidden,
-        jnp.concatenate([down_parts[by] for by in order], axis=1),
-        preferred_element_type=f32,
-    )
-    rest = lax.optimization_barrier(rest)
-    own = {by: rest[:, i * width : (i + 1) * width] for i, by in enumerate(order)}
+    first = jnp.dot(hidden, down_first, preferred_element_type=f32).astype(bf16)
+    part_above = lax.optimization_barrier(jnp.dot(hidden, down_above, preferred_element_type=f32))
+    part_below = lax.optimization_barrier(jnp.dot(hidden, down_below, preferred_element_type=f32))
+    column = lambda a, i: a[:, i * width : (i + 1) * width]
     nothing = jnp.zeros((half, width), bf16)
     above = jnp.concatenate([y_step(first[:half], 1), nothing], axis=0)
     below = jnp.concatenate([nothing, y_step(first[half:], -1)], axis=0)
-    for k in (3, 2, 1):
-        above = y_step((above.astype(f32) + own[Y - k]).astype(bf16), 1)
-        below = y_step((below.astype(f32) + own[k]).astype(bf16), -1)
-    expert_out = own[0] + above.astype(f32) + below.astype(f32)
+    for i in range(3):
+        above = y_step((above.astype(f32) + column(part_above, i)).astype(bf16), 1)
+        below = y_step((below.astype(f32) + column(part_below, i)).astype(bf16), -1)
+    expert_out = column(part_below, 3) + above.astype(f32) + below.astype(f32)
     expert_out = expert_out.astype(bf16).reshape(SP, capacity, width)
 
     returned = exchange(expert_out, "sp").reshape(slots, width)

time: 264 us -> 249 us (0.943)
  the two profiles are of different devices: /device:TPU:8 before, /device:TPU:24 now
where the time goes in v1:
time: 249 us; the launch traced here: 248 us
  starting transfers between devices  94.5 us (38%)
  waiting for transfers between devices  60.4 us (24%)
  blocking collectives  51.3 us (21%)
  other arithmetic  21.8 us (9%)
  matrix products  14.3 us (6%)
  local copies, waits for them, and re-layouts  4.28 us (2%)
    ppermute x16, starting transfers between devices, y_step(): lax.ppermute(value, 'tp', [(t, (t + 2 * by) % TP) for t in range(TP)])  49.8 us
    all_gather x1, blocking collectives, body(): lax.all_gather(block, 'sp', axis=0, tiled=False, axis_index_groups=Z_GROUPS)  34.3 us
    ppermute x16, waiting for transfers between devices, y_step(): lax.ppermute(value, 'tp', [(t, (t + 2 * by) % TP) for t in range(TP)])  30.8 us
    all_to_all x4, waiting for transfers between devices, exchange(): lax.all_to_all(value, axis, split_axis=0, concat_axis=0, tiled=True, axis...  27.9 us
    all_to_all x4, starting transfers between devices, exchange(): lax.all_to_all(value, axis, split_axis=0, concat_axis=0, tiled=True, axis...  21 us
    all_gather x1, blocking collectives, body(): attended_all = lax.all_gather(attended, 'tp', axis=0, tiled=True)  17 us
    ppermute x6, starting transfers between devices, swap(): return lax.ppermute(value, 'tp', [(t, t ^ 1) for t in range(TP)])  12.1 us
    ppermute x3, starting transfers between devices, x_shift(): lax.ppermute(value, 'sp', [(s, s // X * X + (s + by) % X) for s in range(...  11.5 us
  transfers between devices with their start and end apart: 29, of which 17 were waited for; matrix products, arithmetic and copies ran while one was open for 11% of the time, Pallas kernels for 0%

profile of v1, /device:TPU:24, one launch (start us, length us, event | category | flops | bytes accessed | tf_op | source)
XLA Modules:
  0.0 247.9 jit_solution(8723266511018414352)
XLA Ops:
  3.1 3.5 %collective-permute-start = (bf16[256,96]{0,1:T(8,128)(2,1)}, bf16[256,96]{0,1:T(8,128)(2,1)S(1)}, u32[]{:S(2)}, u32[]{:S(2)}) collective-permute-start(bf16[256,96]{0,1:T(8,128)(2,1)} %get-tuple-element.94), channel_id=1, source_target_pairs={{0,16},{16,32},{32,48},{48,0},{64,80},{80,96},{96,112},{112,64},{1... | collective-permute-start | bytes 147464 | tf_op jit(solution)/shard_map/ppermute | solution.py:38
  6.6 4.6 %collective-permute-start.1 = (bf16[256,96]{0,1:T(8,128)(2,1)}, bf16[256,96]{0,1:T(8,128)(2,1)S(1)}, u32[]{:S(2)}, u32[]{:S(2)}) collective-permute-start(bf16[256,96]{0,1:T(8,128)(2,1)} %get-tuple-element.94), channel_id=1, source_target_pairs={{0,32},{16,48},{32,0},{48,16},{64,96},{80,112},{96,64},{112,80},{1... | collective-permute-start | bytes 147464 | tf_op jit(solution)/shard_map/ppermute | solution.py:38
  11.3 3.3 %collective-permute-start.2 = (bf16[256,96]{0,1:T(8,128)(2,1)}, bf16[256,96]{0,1:T(8,128)(2,1)}, u32[]{:S(2)}, u32[]{:S(2)}) collective-permute-start(bf16[256,96]{0,1:T(8,128)(2,1)} %get-tuple-element.94), channel_id=1, source_target_pairs={{0,48},{16,0},{32,16},{48,32},{64,112},{80,64},{96,80},{112,96},{1... | collective-permute-start | bytes 147464 | tf_op jit(solution)/shard_map/ppermute | solution.py:38
  14.6 7.3 %all-to-all-start = ((bf16[8,512,128]{2,1,0:T(8,128)(2,1)}), bf16[8,512,128]{2,1,0:T(8,128)(2,1)S(1)}, u32[]{:S(2)}, u32[]{:S(2)}) async-start(bf16[8,512,128]{2,1,0:T(8,128)(2,1)} %bitcast.151), calls=%async_computation | async-start | bytes 2097152 | tf_op jit(solution)/shard_map/all_to_all | solution.py:28
  23.1 34.3 %all-gather = bf16[1280,256]{1,0:T(8,128)(2,1)} all-gather(bf16[160,256]{1,0:T(8,128)(2,1)S(1)} %pad_maximum_fusion.12), channel_id=2, replica_groups={{0,64,128,192,256,320,384,448},{16,80,144,208,272,336,400,464},{32,96,1..., dimensions={0}, use_global_device_ids=true | all-gather | bytes 737280 | tf_op jit(solution)/shard_map/all_gather | solution.py:106
  58.8 1.7 pad_maximum_fusion
  60.6 1.7 fusion.174
  64.4 2.5 %fusion.2 = (f32[1024]{0:T(1024)S(1)}, f32[8,256,1024]{2,1,0:T(8,128)S(1)}) fusion(s32[1024]{0:T(1024)} %add_select_fusion.1, s32[8,256]{1,0:T(8,128)} %add_select_fusion, bf16[256,96]{0,1:T(8,128)(2,1)S(1)} %get-tuple-element.88, bf16[256,96]{0,1:T(8,128)(2,1)S(1)} %get-tuple-element.89, bf16[256,96]{0,1:T(8,128)(2,1)S(1)} %get-tuple-element.90, ...), kind=kOutput, calls=%fused_computation.4 | convolution fusion | flops 411827200 | bytes 8994816 | tf_op jit(solution)/shard_map/zdk,qd->zkq/dot_general | solution.py:137
  66.9 3.1 %fusion.5 = f32[64,1024]{1,0:T(8,128)S(1)} fusion(f32[8,256,1024]{2,1,0:T(8,128)S(1)} %get-tuple-element.124, f32[1024]{0:T(1024)S(1)} %broadcast_maximum_fusion, s32[1024]{0:T(1024)S(1)} %copy-done.8, s32[8,256]{1,0:T(8,128)S(1)} %copy-done.7, bf16[8,160,256]{2,1,0:T(8,128)(2,1)} %bitcast.156), kind=kOutput, calls=%fused_computation.11 | convolution fusion | flops 278921216 | bytes 8929280 | tf_op jit(solution)/shard_map/zvk,zkq->vq/dot_general | solution.py:149
  70.0 2.1 fusion
  73.1 4.1 %all-to-all-start.1 = ((f32[4,72,256]{2,1,0:T(8,128)}), f32[4,72,256]{2,1,0:T(8,128)}, u32[]{:S(2)}, u32[]{:S(2)}) async-start(f32[4,72,256]{2,1,0:T(8,128)} %pad_maximum_fusion.10), calls=%async_computation.1 | async-start | bytes 589824 | tf_op jit(solution)/shard_map/all_to_all | solution.py:28
  78.3 5.8 %all-to-all-done.1 = f32[4,72,256]{2,1,0:T(8,128)} async-done(((f32[4,72,256]{2,1,0:T(8,128)}), f32[4,72,256]{2,1,0:T(8,128)}, u32[]{:S(2)}, u32[]{:S(2)}) %all-to-all-start.1) | async-done | bytes 294944 | tf_op jit(solution)/shard_map/all_to_all | solution.py:28
  86.7 17.0 %all_gather.11 = bf16[1024,256]{1,0:T(8,128)(2,1)S(1)} all-gather(bf16[64,256]{1,0:T(8,128)(2,1)S(1)} %fusion.135), channel_id=1, replica_groups=mesh['sp'=32,'tp'=16] {'tp'}, dimensions={0}, use_global_device_ids=true | all-gather | bytes 557056 | tf_op jit(solution)/shard_map/all_gather | solution.py:164
  105.2 5.0 %all-to-all-start.2 = ((bf16[32,32,128]{2,1,0:T(8,128)(2,1)}), bf16[32,32,128]{2,1,0:T(8,128)(2,1)}, u32[]{:S(2)}, u32[]{:S(2)}) async-start(bf16[32,32,128]{2,1,0:T(8,128)(2,1)} %bitcast.152), calls=%async_computation.2 | async-start | bytes 524288 | tf_op jit(solution)/shard_map/all_to_all | solution.py:28
  112.9 10.8 %all-to-all-done.2 = bf16[32,32,128]{2,1,0:T(8,128)(2,1)} async-done(((bf16[32,32,128]{2,1,0:T(8,128)(2,1)}), bf16[32,32,128]{2,1,0:T(8,128)(2,1)}, u32[]{:S(2)}, u32[]{:S(2)}) %all-to-all-start.2) | async-done | bytes 262176 | tf_op jit(solution)/shard_map/all_to_all | solution.py:28
  123.8 3.8 %collective-permute-start.4 = (bf16[1024,128]{1,0:T(8,128)(2,1)}, bf16[1024,128]{1,0:T(8,128)(2,1)S(1)}, u32[]{:S(2)}, u32[]{:S(2)}) collective-permute-start(bf16[1024,128]{1,0:T(8,128)(2,1)} %bitcast.31), channel_id=1, source_target_pairs={{0,2},{1,3},{2,4},{3,5},{4,6},{5,7},{6,8},{7,9},{8,10},{9,11},{10,... | collective-permute-start | bytes 786440 | tf_op jit(solution)/shard_map/ppermute | solution.py:44
  127.6 2.2 collective-permute-start.5
  130.0 1.9 collective-permute-start.3
  133.1 4.1 %collective-permute-done.5 = bf16[1024,128]{1,0:T(8,128)(2,1)S(1)} collective-permute-done((bf16[1024,128]{1,0:T(8,128)(2,1)}, bf16[1024,128]{1,0:T(8,128)(2,1)S(1)}, u32[]{:S(2)}, u32[]{:S(2)}) %collective-permute-start.5) | collective-permute-done | bytes 262176 | tf_op jit(solution)/shard_map/ppermute | solution.py:44
  137.3 1.9 collective-permute-start.6
  139.2 2.2 collective-permute-start.7
  141.4 3.7 %collective-permute-start.8 = (bf16[1024,128]{1,0:T(8,128)(2,1)S(1)}, bf16[1024,128]{1,0:T(8,128)(2,1)S(1)}, u32[]{:S(2)}, u32[]{:S(2)}) collective-permute-start(bf16[1024,128]{1,0:T(8,128)(2,1)S(1)} %collective-permute-done.5), channel_id=1, source_target_pairs={{0,14},{1,15},{2,0},{3,1},{4,2},{5,3},{6,4},{7,5},{8,6},{9,7},{10,... | collective-permute-start | bytes 786440 | tf_op jit(solution)/shard_map/ppermute | solution.py:44
  146.3 3.5 %collective-permute-done.7 = bf16[1024,128]{1,0:T(8,128)(2,1)S(1)} collective-permute-done((bf16[1024,128]{1,0:T(8,128)(2,1)S(1)}, bf16[1024,128]{1,0:T(8,128)(2,1)S(1)}, u32[]{:S(2)}, u32[]{:S(2)}) %collective-permute-start.7) | collective-permute-done | bytes 262176 | tf_op jit(solution)/shard_map/ppermute | solution.py:44
  149.8 3.1 %collective-permute-done.8 = bf16[1024,128]{1,0:T(8,128)(2,1)S(1)} collective-permute-done((bf16[1024,128]{1,0:T(8,128)(2,1)S(1)}, bf16[1024,128]{1,0:T(8,128)(2,1)S(1)}, u32[]{:S(2)}, u32[]{:S(2)}) %collective-permute-start.8) | collective-permute-done | bytes 262176 | tf_op jit(solution)/shard_map/ppermute | solution.py:44
  153.1 1.9 collective-permute-start.9
  155.0 1.9 collective-permute-start.10
  156.9 3.9 %collective-permute-start.11 = (bf16[1024,128]{1,0:T(8,128)(2,1)S(1)}, bf16[1024,128]{1,0:T(8,128)(2,1)S(1)}, u32[]{:S(2)}, u32[]{:S(2)}) collective-permute-start(bf16[1024,128]{1,0:T(8,128)(2,1)S(1)} %collective-permute-done.8), channel_id=1, source_target_pairs={{0,14},{1,15},{2,0},{3,1},{4,2},{5,3},{6,4},{7,5},{8,6},{9,7},{10,... | collective-permute-start | bytes 786440 | tf_op jit(solution)/shard_map/ppermute | solution.py:44
  161.3 4.3 %collective-permute-done.10 = bf16[1024,128]{1,0:T(8,128)(2,1)S(1)} collective-permute-done((bf16[1024,128]{1,0:T(8,128)(2,1)S(1)}, bf16[1024,128]{1,0:T(8,128)(2,1)S(1)}, u32[]{:S(2)}, u32[]{:S(2)}) %collective-permute-start.10) | collective-permute-done | bytes 262176 | tf_op jit(solution)/shard_map/ppermute | solution.py:44
  165.6 3.4 %collective-permute-start.13 = (bf16[512,128]{1,0:T(8,128)(2,1)S(1)}, bf16[512,128]{1,0:T(8,128)(2,1)S(1)}, u32[]{:S(2)}, u32[]{:S(2)}) collective-permute-start(bf16[512,128]{1,0:T(8,128)(2,1)S(1)} %slice.184), channel_id=1, source_target_pairs={{0,2},{1,3},{2,4},{3,5},{4,6},{5,7},{6,8},{7,9},{8,10},{9,11},{10,... | collective-permute-start | bytes 393224 | tf_op jit(solution)/shard_map/ppermute | solution.py:44
  169.1 2.4 collective-permute-start.14
  171.6 2.1 collective-permute-start.12
  175.3 1.9 collective-permute-done.14
  177.2 1.9 collective-permute-start.15
  183.1 2.3 collective-permute-start.16
  187.5 3.1 %collective-permute-start.17 = (bf16[512,128]{1,0:T(8,128)(2,1)S(1)}, bf16[512,128]{1,0:T(8,128)(2,1)S(1)}, u32[]{:S(2)}, u32[]{:S(2)}) collective-permute-start(bf16[512,128]{1,0:T(8,128)(2,1)S(1)} %get-tuple-element.65), channel_id=1, source_target_pairs={{0,2},{1,3},{2,4},{3,5},{4,6},{5,7},{6,8},{7,9},{8,10},{9,11},{10,... | collective-permute-start | bytes 393224 | tf_op jit(solution)/shard_map/ppermute | solution.py:44
  191.3 2.9 %collective-permute-start.21 = (bf16[512,128]{1,0:T(8,128)(2,1)S(1)}, bf16[512,128]{1,0:T(8,128)(2,1)S(1)}, u32[]{:S(2)}, u32[]{:S(2)}) collective-permute-start(bf16[512,128]{1,0:T(8,128)(2,1)S(1)} %get-tuple-element.66), channel_id=1, source_target_pairs={{0,14},{1,15},{2,0},{3,1},{4,2},{5,3},{6,4},{7,5},{8,6},{9,7},{10,... | collective-permute-start | bytes 393224 | tf_op jit(solution)/shard_map/ppermute | solution.py:44
  195.3 4.0 %collective-permute-start.18 = (bf16[1024,128]{1,0:T(8,128)(2,1)S(1)}, bf16[1024,128]{1,0:T(8,128)(2,1)S(1)}, u32[]{:S(2)}, u32[]{:S(2)}) collective-permute-start(bf16[1024,128]{1,0:T(8,128)(2,1)S(1)} %fusion.78), channel_id=1, source_target_pairs={{0,2},{1,3},{2,4},{3,5},{4,6},{5,7},{6,8},{7,9},{8,10},{9,11},{10,... | collective-permute-start | bytes 786440 | tf_op jit(solution)/shard_map/ppermute | solution.py:44
  200.2 1.9 collective-permute-start.22
  202.1 2.8 %collective-permute-done.18 = bf16[1024,128]{1,0:T(8,128)(2,1)S(1)} collective-permute-done((bf16[1024,128]{1,0:T(8,128)(2,1)S(1)}, bf16[1024,128]{1,0:T(8,128)(2,1)S(1)}, u32[]{:S(2)}, u32[]{:S(2)}) %collective-permute-start.18) | collective-permute-done | bytes 262176 | tf_op jit(solution)/shard_map/ppermute | solution.py:44
  205.0 5.0 %collective-permute-start.19 = (bf16[1024,128]{1,0:T(8,128)(2,1)S(1)}, bf16[1024,128]{1,0:T(8,128)(2,1)S(1)}, u32[]{:S(2)}, u32[]{:S(2)}) collective-permute-start(bf16[1024,128]{1,0:T(8,128)(2,1)S(1)} %fusion.77), channel_id=1, source_target_pairs={{0,2},{1,3},{2,4},{3,5},{4,6},{5,7},{6,8},{7,9},{8,10},{9,11},{10,... | collective-permute-start | bytes 786440 | tf_op jit(solution)/shard_map/ppermute | solution.py:44
  210.7 1.9 collective-permute-start.23
  212.6 1.6 collective-permute-done.19
  214.3 5.6 %collective-permute-start.20 = (bf16[1024,128]{1,0:T(8,128)(2,1)S(1)}, bf16[1024,128]{1,0:T(8,128)(2,1)S(1)}, u32[]{:S(2)}, u32[]{:S(2)}) collective-permute-start(bf16[1024,128]{1,0:T(8,128)(2,1)S(1)} %fusion.76), channel_id=1, source_target_pairs={{0,2},{1,3},{2,4},{3,5},{4,6},{5,7},{6,8},{7,9},{8,10},{9,11},{10,... | collective-permute-start | bytes 786440 | tf_op jit(solution)/shard_map/ppermute | solution.py:44
  220.3 1.9 collective-permute-start.24
  222.2 1.6 collective-permute-done.20
  223.8 6.0 %collective-permute-done.24 = bf16[1024,128]{1,0:T(8,128)(2,1)S(1)} collective-permute-done((bf16[1024,128]{1,0:T(8,128)(2,1)S(1)}, bf16[1024,128]{1,0:T(8,128)(2,1)S(1)}, u32[]{:S(2)}, u32[]{:S(2)}) %collective-permute-start.24) | collective-permute-done | bytes 262176 | tf_op jit(solution)/shard_map/ppermute | solution.py:44
  230.6 4.6 %all-to-all-start.3 = ((bf16[32,32,128]{2,1,0:T(8,128)(2,1)}), bf16[32,32,128]{2,1,0:T(8,128)(2,1)S(1)}, u32[]{:S(2)}, u32[]{:S(2)}) async-start(bf16[32,32,128]{2,1,0:T(8,128)(2,1)} %bitcast.76), calls=%async_computation.3 | async-start | bytes 524288 | tf_op jit(solution)/shard_map/all_to_all | solution.py:28
  235.2 11.3 %all-to-all-done.3 = bf16[32,32,128]{2,1,0:T(8,128)(2,1)S(1)} async-done(((bf16[32,32,128]{2,1,0:T(8,128)(2,1)}), bf16[32,32,128]{2,1,0:T(8,128)(2,1)S(1)}, u32[]{:S(2)}, u32[]{:S(2)}) %all-to-all-start.3) | async-done | bytes 262176 | tf_op jit(solution)/shard_map/all_to_all | solution.py:28
  (173 shorter events, 32.8 us)
Async XLA Ops:
  0.0 103.8 %copy-start = (bf16[1024,128]{1,0:T(8,128)(2,1)S(1)}, bf16[1024,128]{1,0:T(8,128)(2,1)}, u32[]{:S(2)}) copy-start(bf16[1024,128]{1,0:T(8,128)(2,1)} %param.19) | copy-start | bytes 786436
  0.0 22.6 %copy-start.5 = (bf16[256,256]{1,0:T(8,128)(2,1)S(1)}, bf16[256,256]{1,0:T(8,128)(2,1)}, u32[]{:S(2)}) copy-start(bf16[256,256]{1,0:T(8,128)(2,1)} %param.15) | copy-start | bytes 393220
  0.0 22.7 %copy-start.33 = (bf16[256]{0:T(256)(128)(2,1)S(1)}, bf16[256]{0:T(256)(128)(2,1)}, u32[]{:S(2)}) copy-start(bf16[256]{0:T(256)(128)(2,1)} %param.17) | copy-start | bytes 1540
  0.0 22.8 %copy-start.32 = (bf16[256,128]{1,0:T(8,128)(2,1)S(1)}, bf16[256,128]{1,0:T(8,128)(2,1)}, u32[]{:S(2)}) copy-start(bf16[256,128]{1,0:T(8,128)(2,1)} %param.18) | copy-start | bytes 196612
  2.3 55.1 %copy-start.10 = (s32[256,2]{0,1:T(2,128)S(1)}, s32[256,2]{0,1:T(2,128)}, u32[]{:S(2)}) copy-start(s32[256,2]{0,1:T(2,128)} %param.22) | copy-start | bytes 6148
  3.1 54.5 %copy-start.13 = (bf16[2048]{0:T(1024)(128)(2,1)S(1)}, bf16[2048]{0:T(1024)(128)(2,1)}, u32[]{:S(2)}) copy-start(bf16[2048]{0:T(1024)(128)(2,1)} %param.21) | copy-start | bytes 12292
  3.1 60.4 %collective-permute-start = (bf16[256,96]{0,1:T(8,128)(2,1)}, bf16[256,96]{0,1:T(8,128)(2,1)S(1)}, u32[]{:S(2)}, u32[]{:S(2)}) collective-permute-start(bf16[256,96]{0,1:T(8,128)(2,1)} %get-tuple-element.94), channel_id=1, source_target_pairs={{0,16},{16,32},{32,48},{48,0},{64,80},{80,96},{96,112},{112,64},{1... | collective-permute-start | bytes 147464 | tf_op jit(solution)/shard_map/ppermute | solution.py:38
  6.6 56.9 %collective-permute-start.1 = (bf16[256,96]{0,1:T(8,128)(2,1)}, bf16[256,96]{0,1:T(8,128)(2,1)S(1)}, u32[]{:S(2)}, u32[]{:S(2)}) collective-permute-start(bf16[256,96]{0,1:T(8,128)(2,1)} %get-tuple-element.94), channel_id=1, source_target_pairs={{0,32},{16,48},{32,0},{48,16},{64,96},{80,112},{96,64},{112,80},{1... | collective-permute-start | bytes 147464 | tf_op jit(solution)/shard_map/ppermute | solution.py:38
  11.3 52.2 %collective-permute-start.2 = (bf16[256,96]{0,1:T(8,128)(2,1)}, bf16[256,96]{0,1:T(8,128)(2,1)}, u32[]{:S(2)}, u32[]{:S(2)}) collective-permute-start(bf16[256,96]{0,1:T(8,128)(2,1)} %get-tuple-element.94), channel_id=1, source_target_pairs={{0,48},{16,0},{32,16},{48,32},{64,112},{80,64},{96,80},{112,96},{1... | collective-permute-start | bytes 147464 | tf_op jit(solution)/shard_map/ppermute | solution.py:38
  14.6 58.5 %all-to-all-start = ((bf16[8,512,128]{2,1,0:T(8,128)(2,1)}), bf16[8,512,128]{2,1,0:T(8,128)(2,1)S(1)}, u32[]{:S(2)}, u32[]{:S(2)}) async-start(bf16[8,512,128]{2,1,0:T(8,128)(2,1)} %bitcast.151), calls=%async_computation | async-start | bytes 2097152 | tf_op jit(solution)/shard_map/all_to_all | solution.py:28
  72.2 31.6 %copy-start.6 = (bf16[256,128]{1,0:T(8,128)(2,1)S(1)}, bf16[256,128]{1,0:T(8,128)(2,1)}, u32[]{:S(2)}) copy-start(bf16[256,128]{1,0:T(8,128)(2,1)} %param.20) | copy-start | bytes 196612
  73.1 11.0 %all-to-all-start.1 = ((f32[4,72,256]{2,1,0:T(8,128)}), f32[4,72,256]{2,1,0:T(8,128)}, u32[]{:S(2)}, u32[]{:S(2)}) async-start(f32[4,72,256]{2,1,0:T(8,128)} %pad_maximum_fusion.10), calls=%async_computation.1 | async-start | bytes 589824 | tf_op jit(solution)/shard_map/all_to_all | solution.py:28
  84.1 20.0 %copy-start.1 = (bf16[256,1024]{1,0:T(8,128)(2,1)S(1)}, bf16[256,1024]{1,0:T(8,128)(2,1)}, u32[]{:S(2)}) copy-start(bf16[256,1024]{1,0:T(8,128)(2,1)} %fusion.72) | copy-start | bytes 1572868
  105.2 18.6 %all-to-all-start.2 = ((bf16[32,32,128]{2,1,0:T(8,128)(2,1)}), bf16[32,32,128]{2,1,0:T(8,128)(2,1)}, u32[]{:S(2)}, u32[]{:S(2)}) async-start(bf16[32,32,128]{2,1,0:T(8,128)(2,1)} %bitcast.152), calls=%async_computation.2 | async-start | bytes 524288 | tf_op jit(solution)/shard_map/all_to_all | solution.py:28
  123.8 21.4 %copy-start.28 = (f32[128]{0:T(128)S(1)}, f32[128]{0:T(128)}, u32[]{:S(2)}) copy-start(f32[128]{0:T(128)} %get-tuple-element.112) | copy-start | bytes 1540
  123.8 9.4 %collective-permute-start.4 = (bf16[1024,128]{1,0:T(8,128)(2,1)}, bf16[1024,128]{1,0:T(8,128)(2,1)S(1)}, u32[]{:S(2)}, u32[]{:S(2)}) collective-permute-start(bf16[1024,128]{1,0:T(8,128)(2,1)} %bitcast.31), channel_id=1, source_target_pairs={{0,2},{1,3},{2,4},{3,5},{4,6},{5,7},{6,8},{7,9},{8,10},{9,11},{10,... | collective-permute-start | bytes 786440 | tf_op jit(solution)/shard_map/ppermute | solution.py:44
  127.6 9.7 %collective-permute-start.5 = (bf16[1024,128]{1,0:T(8,128)(2,1)}, bf16[1024,128]{1,0:T(8,128)(2,1)S(1)}, u32[]{:S(2)}, u32[]{:S(2)}) collective-permute-start(bf16[1024,128]{1,0:T(8,128)(2,1)} %bitcast.31), channel_id=1, source_target_pairs={{0,14},{1,15},{2,0},{3,1},{4,2},{5,3},{6,4},{7,5},{8,6},{9,7},{10,... | collective-permute-start | bytes 786440 | tf_op jit(solution)/shard_map/ppermute | solution.py:44
  130.0 15.3 %copy-start.27 = (f32[128]{0:T(128)S(1)}, f32[128]{0:T(128)}, u32[]{:S(2)}) copy-start(f32[128]{0:T(128)} %get-tuple-element.113) | copy-start | bytes 1540
  130.0 15.3 %collective-permute-start.3 = (bf16[1024,128]{1,0:T(8,128)(2,1)}, bf16[1024,128]{1,0:T(8,128)(2,1)S(1)}, u32[]{:S(2)}, u32[]{:S(2)}) collective-permute-start(bf16[1024,128]{1,0:T(8,128)(2,1)} %bitcast.31), channel_id=1, source_target_pairs={{0,1},{1,0},{2,3},{3,2},{4,5},{5,4},{6,7},{7,6},{8,9},{9,8},{10,11... | collective-permute-start | bytes 786440 | tf_op jit(solution)/shard_map/ppermute | solution.py:34
  137.3 36.8 %collective-permute-start.6 = (bf16[1024,256]{1,0:T(8,128)(2,1)S(1)}, bf16[1024,256]{1,0:T(8,128)(2,1)S(1)}, u32[]{:S(2)}, u32[]{:S(2)}) collective-permute-start(bf16[1024,256]{1,0:T(8,128)(2,1)S(1)} %pad_maximum_fusion.3), channel_id=1, source_target_pairs={{0,1},{1,0},{2,3},{3,2},{4,5},{5,4},{6,7},{7,6},{8,9},{9,8},{10,11... | collective-permute-start | bytes 1572872 | tf_op jit(solution)/shard_map/ppermute | solution.py:34
  139.2 10.6 %collective-permute-start.7 = (bf16[1024,128]{1,0:T(8,128)(2,1)S(1)}, bf16[1024,128]{1,0:T(8,128)(2,1)S(1)}, u32[]{:S(2)}, u32[]{:S(2)}) collective-permute-start(bf16[1024,128]{1,0:T(8,128)(2,1)S(1)} %collective-permute-done.4), channel_id=1, source_target_pairs={{0,2},{1,3},{2,4},{3,5},{4,6},{5,7},{6,8},{7,9},{8,10},{9,11},{10,... | collective-permute-start | bytes 786440 | tf_op jit(solution)/shard_map/ppermute | solution.py:44
  141.4 11.6 %collective-permute-start.8 = (bf16[1024,128]{1,0:T(8,128)(2,1)S(1)}, bf16[1024,128]{1,0:T(8,128)(2,1)S(1)}, u32[]{:S(2)}, u32[]{:S(2)}) collective-permute-start(bf16[1024,128]{1,0:T(8,128)(2,1)S(1)} %collective-permute-done.5), channel_id=1, source_target_pairs={{0,14},{1,15},{2,0},{3,1},{4,2},{5,3},{6,4},{7,5},{8,6},{9,7},{10,... | collective-permute-start | bytes 786440 | tf_op jit(solution)/shard_map/ppermute | solution.py:44
  145.6 15.3 %copy-start.25 = (f32[128]{0:T(128)S(1)}, f32[128]{0:T(128)}, u32[]{:S(2)}) copy-start(f32[128]{0:T(128)} %get-tuple-element.108) | copy-start | bytes 1540
  145.6 15.5 %copy-start.24 = (f32[128]{0:T(128)S(1)}, f32[128]{0:T(128)}, u32[]{:S(2)}) copy-start(f32[128]{0:T(128)} %get-tuple-element.107) | copy-start | bytes 1540
  146.1 27.6 %copy-start.23 = (f32[128]{0:T(128)S(1)}, f32[128]{0:T(128)}, u32[]{:S(2)}) copy-start(f32[128]{0:T(128)} %get-tuple-element.104) | copy-start | bytes 1540
  146.3 27.6 %copy-start.22 = (f32[128]{0:T(128)S(1)}, f32[128]{0:T(128)}, u32[]{:S(2)}) copy-start(f32[128]{0:T(128)} %get-tuple-element.103) | copy-start | bytes 1540
  153.0 21.1 %copy-start.18 = (f32[128]{0:T(128)S(1)}, f32[128]{0:T(128)}, u32[]{:S(2)}) copy-start(f32[128]{0:T(128)} %get-tuple-element.109) | copy-start | bytes 1540
  153.1 21.1 %copy-start.19 = (f32[128]{0:T(128)S(1)}, f32[128]{0:T(128)}, u32[]{:S(2)}) copy-start(f32[128]{0:T(128)} %get-tuple-element.110) | copy-start | bytes 1540
  153.1 26.3 %collective-permute-start.9 = (bf16[1024,256]{1,0:T(8,128)(2,1)S(1)}, bf16[1024,256]{1,0:T(8,128)(2,1)S(1)}, u32[]{:S(2)}, u32[]{:S(2)}) collective-permute-start(bf16[1024,256]{1,0:T(8,128)(2,1)S(1)} %pad_maximum_fusion.4), channel_id=1, source_target_pairs={{0,1},{1,0},{2,3},{3,2},{4,5},{5,4},{6,7},{7,6},{8,9},{9,8},{10,11... | collective-permute-start | bytes 1572872 | tf_op jit(solution)/shard_map/ppermute | solution.py:34
  155.0 10.6 %collective-permute-start.10 = (bf16[1024,128]{1,0:T(8,128)(2,1)S(1)}, bf16[1024,128]{1,0:T(8,128)(2,1)S(1)}, u32[]{:S(2)}, u32[]{:S(2)}) collective-permute-start(bf16[1024,128]{1,0:T(8,128)(2,1)S(1)} %collective-permute-done.7), channel_id=1, source_target_pairs={{0,2},{1,3},{2,4},{3,5},{4,6},{5,7},{6,8},{7,9},{8,10},{9,11},{10,... | collective-permute-start | bytes 786440 | tf_op jit(solution)/shard_map/ppermute | solution.py:44
  156.9 12.1 %collective-permute-start.11 = (bf16[1024,128]{1,0:T(8,128)(2,1)S(1)}, bf16[1024,128]{1,0:T(8,128)(2,1)S(1)}, u32[]{:S(2)}, u32[]{:S(2)}) collective-permute-start(bf16[1024,128]{1,0:T(8,128)(2,1)S(1)} %collective-permute-done.8), channel_id=1, source_target_pairs={{0,14},{1,15},{2,0},{3,1},{4,2},{5,3},{6,4},{7,5},{8,6},{9,7},{10,... | collective-permute-start | bytes 786440 | tf_op jit(solution)/shard_map/ppermute | solution.py:44
  165.6 9.7 %collective-permute-start.13 = (bf16[512,128]{1,0:T(8,128)(2,1)S(1)}, bf16[512,128]{1,0:T(8,128)(2,1)S(1)}, u32[]{:S(2)}, u32[]{:S(2)}) collective-permute-start(bf16[512,128]{1,0:T(8,128)(2,1)S(1)} %slice.184), channel_id=1, source_target_pairs={{0,2},{1,3},{2,4},{3,5},{4,6},{5,7},{6,8},{7,9},{8,10},{9,11},{10,... | collective-permute-start | bytes 393224 | tf_op jit(solution)/shard_map/ppermute | solution.py:44
  169.1 8.1 %collective-permute-start.14 = (bf16[512,128]{1,0:T(8,128)(2,1)S(1)}, bf16[512,128]{1,0:T(8,128)(2,1)S(1)}, u32[]{:S(2)}, u32[]{:S(2)}) collective-permute-start(bf16[512,128]{1,0:T(8,128)(2,1)S(1)} %slice.185), channel_id=1, source_target_pairs={{0,14},{1,15},{2,0},{3,1},{4,2},{5,3},{6,4},{7,5},{8,6},{9,7},{10,... | collective-permute-start | bytes 393224 | tf_op jit(solution)/shard_map/ppermute | solution.py:44
  171.6 9.3 %collective-permute-start.12 = (bf16[1024,256]{1,0:T(8,128)(2,1)S(1)}, bf16[1024,256]{1,0:T(8,128)(2,1)S(1)}, u32[]{:S(2)}, u32[]{:S(2)}) collective-permute-start(bf16[1024,256]{1,0:T(8,128)(2,1)S(1)} %pad_maximum_fusion.5), channel_id=1, source_target_pairs={{0,1},{1,0},{2,3},{3,2},{4,5},{5,4},{6,7},{7,6},{8,9},{9,8},{10,11... | collective-permute-start | bytes 1572872 | tf_op jit(solution)/shard_map/ppermute | solution.py:34
  177.2 3.4 %collective-permute-start.15 = (bf16[1024,128]{1,0:T(8,128)(2,1)S(1)}, bf16[1024,128]{1,0:T(8,128)(2,1)S(1)}, u32[]{:S(2)}, u32[]{:S(2)}) collective-permute-start(bf16[1024,128]{1,0:T(8,128)(2,1)S(1)} %constant_dynamic-update-slice_fusion), channel_id=1, source_target_pairs={{0,1},{1,0},{2,3},{3,2},{4,5},{5,4},{6,7},{7,6},{8,9},{9,8},{10,11... | collective-permute-start | bytes 786440 | tf_op jit(solution)/shard_map/ppermute | solution.py:34
  183.1 3.8 %collective-permute-start.16 = (bf16[1024,256]{0,1:T(8,128)(2,1)S(1)}, bf16[1024,256]{0,1:T(8,128)(2,1)S(1)}, u32[]{:S(2)}, u32[]{:S(2)}) collective-permute-start(bf16[1024,256]{0,1:T(8,128)(2,1)S(1)} %fusion.13), channel_id=1, source_target_pairs={{0,1},{1,0},{2,3},{3,2},{4,5},{5,4},{6,7},{7,6},{8,9},{9,8},{10,11... | collective-permute-start | bytes 1572872 | tf_op jit(solution)/shard_map/ppermute | solution.py:34
  187.5 11.9 %copy-start.2 = (bf16[512,512]{1,0:T(8,128)(2,1)S(1)}, bf16[512,512]{1,0:T(8,128)(2,1)}, u32[]{:S(2)}) copy-start(bf16[512,512]{1,0:T(8,128)(2,1)} %pad_maximum_fusion.2) | copy-start | bytes 1572868
  187.5 7.8 %collective-permute-start.17 = (bf16[512,128]{1,0:T(8,128)(2,1)S(1)}, bf16[512,128]{1,0:T(8,128)(2,1)S(1)}, u32[]{:S(2)}, u32[]{:S(2)}) collective-permute-start(bf16[512,128]{1,0:T(8,128)(2,1)S(1)} %get-tuple-element.65), channel_id=1, source_target_pairs={{0,2},{1,3},{2,4},{3,5},{4,6},{5,7},{6,8},{7,9},{8,10},{9,11},{10,... | collective-permute-start | bytes 393224 | tf_op jit(solution)/shard_map/ppermute | solution.py:44
  191.3 8.8 %collective-permute-start.21 = (bf16[512,128]{1,0:T(8,128)(2,1)S(1)}, bf16[512,128]{1,0:T(8,128)(2,1)S(1)}, u32[]{:S(2)}, u32[]{:S(2)}) collective-permute-start(bf16[512,128]{1,0:T(8,128)(2,1)S(1)} %get-tuple-element.66), channel_id=1, source_target_pairs={{0,14},{1,15},{2,0},{3,1},{4,2},{5,3},{6,4},{7,5},{8,6},{9,7},{10,... | collective-permute-start | bytes 393224 | tf_op jit(solution)/shard_map/ppermute | solution.py:44
  195.3 9.6 %collective-permute-start.18 = (bf16[1024,128]{1,0:T(8,128)(2,1)S(1)}, bf16[1024,128]{1,0:T(8,128)(2,1)S(1)}, u32[]{:S(2)}, u32[]{:S(2)}) collective-permute-start(bf16[1024,128]{1,0:T(8,128)(2,1)S(1)} %fusion.78), channel_id=1, source_target_pairs={{0,2},{1,3},{2,4},{3,5},{4,6},{5,7},{6,8},{7,9},{8,10},{9,11},{10,... | collective-permute-start | bytes 786440 | tf_op jit(solution)/shard_map/ppermute | solution.py:44
  200.2 10.4 %collective-permute-start.22 = (bf16[1024,128]{1,0:T(8,128)(2,1)S(1)}, bf16[1024,128]{1,0:T(8,128)(2,1)S(1)}, u32[]{:S(2)}, u32[]{:S(2)}) collective-permute-start(bf16[1024,128]{1,0:T(8,128)(2,1)S(1)} %fusion.75), channel_id=1, source_target_pairs={{0,14},{1,15},{2,0},{3,1},{4,2},{5,3},{6,4},{7,5},{8,6},{9,7},{10,... | collective-permute-start | bytes 786440 | tf_op jit(solution)/shard_map/ppermute | solution.py:44
  205.0 9.2 %collective-permute-start.19 = (bf16[1024,128]{1,0:T(8,128)(2,1)S(1)}, bf16[1024,128]{1,0:T(8,128)(2,1)S(1)}, u32[]{:S(2)}, u32[]{:S(2)}) collective-permute-start(bf16[1024,128]{1,0:T(8,128)(2,1)S(1)} %fusion.77), channel_id=1, source_target_pairs={{0,2},{1,3},{2,4},{3,5},{4,6},{5,7},{6,8},{7,9},{8,10},{9,11},{10,... | collective-permute-start | bytes 786440 | tf_op jit(solution)/shard_map/ppermute | solution.py:44
  210.7 24.5 %copy-start.9 = (f32[256,2]{0,1:T(2,128)S(1)}, f32[256,2]{0,1:T(2,128)}, u32[]{:S(2)}) copy-start(f32[256,2]{0,1:T(2,128)} %param.23) | copy-start | bytes 6148
  210.7 24.5 %copy-start.30 = (f32[256]{0:T(256)S(1)}, f32[256]{0:T(256)}, u32[]{:S(2)}) copy-start(f32[256]{0:T(256)} %param.24) | copy-start | bytes 3076
  210.7 9.5 %collective-permute-start.23 = (bf16[1024,128]{1,0:T(8,128)(2,1)S(1)}, bf16[1024,128]{1,0:T(8,128)(2,1)S(1)}, u32[]{:S(2)}, u32[]{:S(2)}) collective-permute-start(bf16[1024,128]{1,0:T(8,128)(2,1)S(1)} %fusion.74), channel_id=1, source_target_pairs={{0,14},{1,15},{2,0},{3,1},{4,2},{5,3},{6,4},{7,5},{8,6},{9,7},{10,... | collective-permute-start | bytes 786440 | tf_op jit(solution)/shard_map/ppermute | solution.py:44
  214.3 9.5 %collective-permute-start.20 = (bf16[1024,128]{1,0:T(8,128)(2,1)S(1)}, bf16[1024,128]{1,0:T(8,128)(2,1)S(1)}, u32[]{:S(2)}, u32[]{:S(2)}) collective-permute-start(bf16[1024,128]{1,0:T(8,128)(2,1)S(1)} %fusion.76), channel_id=1, source_target_pairs={{0,2},{1,3},{2,4},{3,5},{4,6},{5,7},{6,8},{7,9},{8,10},{9,11},{10,... | collective-permute-start | bytes 786440 | tf_op jit(solution)/shard_map/ppermute | solution.py:44
  220.3 9.5 %collective-permute-start.24 = (bf16[1024,128]{1,0:T(8,128)(2,1)S(1)}, bf16[1024,128]{1,0:T(8,128)(2,1)S(1)}, u32[]{:S(2)}, u32[]{:S(2)}) collective-permute-start(bf16[1024,128]{1,0:T(8,128)(2,1)S(1)} %fusion.73), channel_id=1, source_target_pairs={{0,14},{1,15},{2,0},{3,1},{4,2},{5,3},{6,4},{7,5},{8,6},{9,7},{10,... | collective-permute-start | bytes 786440 | tf_op jit(solution)/shard_map/ppermute | solution.py:44
  230.6 16.0 %all-to-all-start.3 = ((bf16[32,32,128]{2,1,0:T(8,128)(2,1)}), bf16[32,32,128]{2,1,0:T(8,128)(2,1)S(1)}, u32[]{:S(2)}, u32[]{:S(2)}) async-start(bf16[32,32,128]{2,1,0:T(8,128)(2,1)} %bitcast.76), calls=%async_computation.3 | async-start | bytes 524288 | tf_op jit(solution)/shard_map/all_to_all | solution.py:28
  (15 other events, 63.7 us)

commit v2 on v1

--- a/solution.py
+++ b/solution.py
@@ -21,7 +21,6 @@
 
 Z_GROUPS = [[z * X + x for z in range(Z)] for x in range(X)]
 X_GROUPS = [[z * X + x for x in range(X)] for z in range(Z)]
-Y_GROUPS = [[y * 2 + c for y in range(Y)] for c in range(2)]
 
 
 def exchange(value, axis, groups=None):
@@ -103,7 +102,7 @@
     rotated = rotate(rope_key, positions).T
     block = jnp.concatenate([key_value[:NOPE], rotated, key_value[NOPE:]], axis=0)
     query = jnp.concatenate([queries[:, :NOPE], rotate(queries[:, NOPE:], positions)], axis=1)
-    blocks = lax.all_gather(block, "sp", axis=0, tiled=False, axis_index_groups=Z_GROUPS)
+    blocks = exchange(jnp.broadcast_to(block, (Z,) + block.shape), "sp", Z_GROUPS)
 
     query_parts = [query]
     for by in range(1, X):
@@ -116,7 +115,15 @@
         [gate_weight.reshape(TP, width, ff), up_weight.reshape(TP, width, ff)], axis=2
     )
     gains = ffn_gain.astype(f32).reshape(TP, width)
-    down = exchange(down_weight.reshape(Y, 2 * ff, width), "tp", Y_GROUPS)
+    down = down_weight.reshape(Y // 2, 2, 2 * ff, width)
+    odd = y % 2
+    parity = lambda one: lax.dynamic_index_in_dim(down, one, 1, keepdims=False)
+    kept = parity(odd)
+    got = lax.ppermute(parity(1 - odd), "tp", [(t, t ^ 2) for t in range(TP)])
+    both = jnp.stack([jnp.where(odd == 0, kept, got), jnp.where(odd == 0, got, kept)], axis=1)
+    down = [at(both, y // 2)]
+    for by in (1, 2, 3):
+        down.append(y_step(at(both, (y // 2 + by) % (Y // 2)), 2 * by))
 
     experts = SP
     capacity = 2 * tokens * TOP // experts
@@ -151,7 +158,6 @@
     )
     packed = jnp.concatenate([summed, top, total, jnp.zeros((6, X * tokens), f32)], axis=0)
     packed = jnp.stack([packed[:, i * tokens : (i + 1) * tokens] for i in range(X)])
-    packed, down = lax.optimization_barrier((packed, down))
     packed = exchange(packed, "sp", X_GROUPS)
     tops = packed[:, VDIM]
     factors = jnp.exp(tops - jnp.max(tops, axis=0, keepdims=True))
@@ -169,9 +175,16 @@
 
     sent = lax.dot_general(placed, mixed, (((0,), (0,)), ((), ())), preferred_element_type=f32)
     arrived = exchange(sent.astype(bf16).reshape(SP, capacity, width), "sp")
-    down = down.reshape(Y, 2, ff, width)
+    down = jnp.stack(down).reshape(Y, 2, ff, width)
     down = jnp.where(core == 0, down, down[:, ::-1]).reshape(Y, 2 * ff, width)
-    features = lambda steps: jnp.concatenate([at(down, (y + k) % Y) for k in steps], axis=1)
+
+    def features(steps):
+        parts = []
+        for k in steps:
+            chip = (y + k) % Y
+            parts.append(at(down, (y // 2 - chip // 2) % (Y // 2) * 2 + chip % 2))
+        return jnp.concatenate(parts, axis=1)
+
     down_first, down_above, down_below = features([4]), features([3, 2, 1]), features([-3, -2, -1, 0])
     arrived, down_first, down_above, down_below = lax.optimization_barrier(
         (arrived.reshape(slots, width), down_first, down_above, down_below)

time: 249 us -> 245 us (0.984)
  the two profiles are of different devices: /device:TPU:24 before, /device:TPU:56 now
where the time goes in v2:
time: 245 us; the launch traced here: 243 us
  starting transfers between devices  115 us (47%)
  waiting for transfers between devices  60 us (24%)
  other arithmetic  26.2 us (11%)
  blocking collectives  18.5 us (8%)
  matrix products  15.3 us (6%)
  local copies, waits for them, and re-layouts  6.77 us (3%)
    ppermute x19, starting transfers between devices, y_step(): lax.ppermute(value, 'tp', [(t, (t + 2 * by) % TP) for t in range(TP)])  61.8 us
    ppermute x19, waiting for transfers between devices, y_step(): lax.ppermute(value, 'tp', [(t, (t + 2 * by) % TP) for t in range(TP)])  32.2 us
    all_to_all x4, starting transfers between devices, exchange(): lax.all_to_all(value, axis, split_axis=0, concat_axis=0, tiled=True, axis...  26.5 us
    all_to_all x4, waiting for transfers between devices, exchange(): lax.all_to_all(value, axis, split_axis=0, concat_axis=0, tiled=True, axis...  26.1 us
    all_gather x1, blocking collectives, body(): attended_all = lax.all_gather(attended, 'tp', axis=0, tiled=True)  18.5 us
    ppermute x6, starting transfers between devices, swap(): return lax.ppermute(value, 'tp', [(t, t ^ 1) for t in range(TP)])  11.9 us
    ppermute x3, starting transfers between devices, x_shift(): lax.ppermute(value, 'sp', [(s, s // X * X + (s + by) % X) for s in range(...  11.5 us
  transfers between devices with their start and end apart: 33, of which 18 were waited for; matrix products, arithmetic and copies ran while one was open for 15% of the time, Pallas kernels for 0%

profile of v2, /device:TPU:56, one launch (start us, length us, event | category | flops | bytes accessed | tf_op | source)
XLA Modules:
  0.0 243.1 jit_solution(11476996473718657055)
XLA Ops:
  3.1 3.5 %collective-permute-start = (bf16[256,96]{0,1:T(8,128)(2,1)}, bf16[256,96]{0,1:T(8,128)(2,1)S(1)}, u32[]{:S(2)}, u32[]{:S(2)}) collective-permute-start(bf16[256,96]{0,1:T(8,128)(2,1)} %get-tuple-element.96), channel_id=1, source_target_pairs={{0,16},{16,32},{32,48},{48,0},{64,80},{80,96},{96,112},{112,64},{1... | collective-permute-start | bytes 147464 | tf_op jit(solution)/shard_map/ppermute | solution.py:37
  6.6 4.6 %collective-permute-start.1 = (bf16[256,96]{0,1:T(8,128)(2,1)}, bf16[256,96]{0,1:T(8,128)(2,1)S(1)}, u32[]{:S(2)}, u32[]{:S(2)}) collective-permute-start(bf16[256,96]{0,1:T(8,128)(2,1)} %get-tuple-element.96), channel_id=1, source_target_pairs={{0,32},{16,48},{32,0},{48,16},{64,96},{80,112},{96,64},{112,80},{1... | collective-permute-start | bytes 147464 | tf_op jit(solution)/shard_map/ppermute | solution.py:37
  11.2 3.3 %collective-permute-start.2 = (bf16[256,96]{0,1:T(8,128)(2,1)}, bf16[256,96]{0,1:T(8,128)(2,1)}, u32[]{:S(2)}, u32[]{:S(2)}) collective-permute-start(bf16[256,96]{0,1:T(8,128)(2,1)} %get-tuple-element.96), channel_id=1, source_target_pairs={{0,48},{16,0},{32,16},{48,32},{64,112},{80,64},{96,80},{112,96},{1... | collective-permute-start | bytes 147464 | tf_op jit(solution)/shard_map/ppermute | solution.py:37
  14.6 1.9 dynamic-slice_bitcast_fusion
  16.5 3.2 %collective-permute-start.3 = (bf16[4,512,128]{2,1,0:T(8,128)(2,1)}, bf16[4,512,128]{2,1,0:T(8,128)(2,1)}, u32[]{:S(2)}, u32[]{:S(2)}) collective-permute-start(bf16[4,512,128]{2,1,0:T(8,128)(2,1)} %dynamic-slice_bitcast_fusion), channel_id=1, source_target_pairs={{0,2},{1,3},{2,0},{3,1},{4,6},{5,7},{6,4},{7,5},{8,10},{9,11},{10,... | collective-permute-start | bytes 1572872 | tf_op jit(solution)/shard_map/ppermute | solution.py:122
  23.6 10.3 %all-to-all-start = ((bf16[8,160,256]{2,1,0:T(8,128)(2,1)}), bf16[8,160,256]{2,1,0:T(8,128)(2,1)}, u32[]{:S(2)}, u32[]{:S(2)}) async-start(bf16[8,160,256]{2,1,0:T(8,128)(2,1)} %broadcast_in_dim.9), calls=%async_computation | async-start | bytes 1310720 | tf_op jit(solution)/shard_map/all_to_all | solution.py:27
  43.3 1.9 collective-permute-start.4
  45.2 7.6 %collective-permute-start.5 = (bf16[2,512,128]{2,1,0:T(8,128)(2,1)}, bf16[2,512,128]{2,1,0:T(8,128)(2,1)}, u32[]{:S(2)}, u32[]{:S(2)}) collective-permute-start(bf16[2,512,128]{2,1,0:T(8,128)(2,1)} %get-tuple-element.55), channel_id=1, source_target_pairs={{0,8},{1,9},{2,10},{3,11},{4,12},{5,13},{6,14},{7,15},{8,0},{9,1},... | collective-permute-start | bytes 786440 | tf_op jit(solution)/shard_map/ppermute | solution.py:43
  52.9 1.9 collective-permute-start.6
  54.8 2.5 %fusion.2 = (f32[1024]{0:T(1024)S(1)}, f32[8,256,1024]{2,1,0:T(8,128)S(1)}) fusion(s32[1024]{0:T(1024)} %add_select_fusion.1, s32[8,256]{1,0:T(8,128)} %add_select_fusion, bf16[256,96]{0,1:T(8,128)(2,1)S(1)} %get-tuple-element.90, bf16[256,96]{0,1:T(8,128)(2,1)S(1)} %get-tuple-element.91, bf16[256,96]{0,1:T(8,128)(2,1)S(1)} %copy-done.7, ...), kind=kOutput, calls=%fused_computation.4 | convolution fusion | flops 411827200 | bytes 8994816 | tf_op jit(solution)/shard_map/zdk,qd->zkq/dot_general | solution.py:144
  57.3 2.1 fusion
  59.5 3.1 %fusion.5 = f32[64,1024]{1,0:T(8,128)S(1)} fusion(f32[8,256,1024]{2,1,0:T(8,128)S(1)} %get-tuple-element.126, f32[1024]{0:T(1024)S(1)} %broadcast_maximum_fusion, s32[1024]{0:T(1024)S(1)} %copy-done.10, s32[8,256]{1,0:T(8,128)S(1)} %copy-done.9, bf16[8,160,256]{2,1,0:T(8,128)(2,1)} %all-to-all-done), kind=kOutput, calls=%fused_computation.19 | convolution fusion | flops 278921216 | bytes 8929280 | tf_op jit(solution)/shard_map/zvk,zkq->vq/dot_general | solution.py:156
  63.5 4.1 %all-to-all-start.1 = ((f32[4,72,256]{2,1,0:T(8,128)}), f32[4,72,256]{2,1,0:T(8,128)}, u32[]{:S(2)}, u32[]{:S(2)}) async-start(f32[4,72,256]{2,1,0:T(8,128)} %pad_maximum_fusion.11), calls=%async_computation.1 | async-start | bytes 589824 | tf_op jit(solution)/shard_map/all_to_all | solution.py:27
  70.8 3.8 %all-to-all-done.1 = f32[4,72,256]{2,1,0:T(8,128)} async-done(((f32[4,72,256]{2,1,0:T(8,128)}), f32[4,72,256]{2,1,0:T(8,128)}, u32[]{:S(2)}, u32[]{:S(2)}) %all-to-all-start.1) | async-done | bytes 294944 | tf_op jit(solution)/shard_map/all_to_all | solution.py:27
  77.2 18.5 %all_gather.3 = bf16[1024,256]{1,0:T(8,128)(2,1)S(1)} all-gather(bf16[64,256]{1,0:T(8,128)(2,1)S(1)} %fusion.144), channel_id=1, replica_groups=mesh['sp'=32,'tp'=16] {'tp'}, dimensions={0}, use_global_device_ids=true | all-gather | bytes 557056 | tf_op jit(solution)/shard_map/all_gather | solution.py:170
  97.1 7.5 %all-to-all-start.2 = ((bf16[32,32,128]{2,1,0:T(8,128)(2,1)}), bf16[32,32,128]{2,1,0:T(8,128)(2,1)}, u32[]{:S(2)}, u32[]{:S(2)}) async-start(bf16[32,32,128]{2,1,0:T(8,128)(2,1)} %bitcast.178), calls=%async_computation.2 | async-start | bytes 524288 | tf_op jit(solution)/shard_map/all_to_all | solution.py:27
  107.3 10.8 %all-to-all-done.2 = bf16[32,32,128]{2,1,0:T(8,128)(2,1)} async-done(((bf16[32,32,128]{2,1,0:T(8,128)(2,1)}), bf16[32,32,128]{2,1,0:T(8,128)(2,1)}, u32[]{:S(2)}, u32[]{:S(2)}) %all-to-all-start.2) | async-done | bytes 262176 | tf_op jit(solution)/shard_map/all_to_all | solution.py:27
  118.1 4.6 %collective-permute-start.8 = (bf16[1024,128]{1,0:T(8,128)(2,1)}, bf16[1024,128]{1,0:T(8,128)(2,1)S(1)}, u32[]{:S(2)}, u32[]{:S(2)}) collective-permute-start(bf16[1024,128]{1,0:T(8,128)(2,1)} %bitcast.29), channel_id=1, source_target_pairs={{0,2},{1,3},{2,4},{3,5},{4,6},{5,7},{6,8},{7,9},{8,10},{9,11},{10,... | collective-permute-start | bytes 786440 | tf_op jit(solution)/shard_map/ppermute | solution.py:43
  122.7 1.9 collective-permute-start.9
  124.9 1.9 collective-permute-start.7
  128.0 4.4 %collective-permute-done.9 = bf16[1024,128]{1,0:T(8,128)(2,1)S(1)} collective-permute-done((bf16[1024,128]{1,0:T(8,128)(2,1)}, bf16[1024,128]{1,0:T(8,128)(2,1)S(1)}, u32[]{:S(2)}, u32[]{:S(2)}) %collective-permute-start.9) | collective-permute-done | bytes 262176 | tf_op jit(solution)/shard_map/ppermute | solution.py:43
  132.5 1.9 collective-permute-start.10
  134.4 1.9 collective-permute-start.11
  136.3 4.1 %collective-permute-start.12 = (bf16[1024,128]{1,0:T(8,128)(2,1)S(1)}, bf16[1024,128]{1,0:T(8,128)(2,1)S(1)}, u32[]{:S(2)}, u32[]{:S(2)}) collective-permute-start(bf16[1024,128]{1,0:T(8,128)(2,1)S(1)} %collective-permute-done.9), channel_id=1, source_target_pairs={{0,14},{1,15},{2,0},{3,1},{4,2},{5,3},{6,4},{7,5},{8,6},{9,7},{10,... | collective-permute-start | bytes 786440 | tf_op jit(solution)/shard_map/ppermute | solution.py:43
  141.7 3.3 %collective-permute-done.11 = bf16[1024,128]{1,0:T(8,128)(2,1)S(1)} collective-permute-done((bf16[1024,128]{1,0:T(8,128)(2,1)S(1)}, bf16[1024,128]{1,0:T(8,128)(2,1)S(1)}, u32[]{:S(2)}, u32[]{:S(2)}) %collective-permute-start.11) | collective-permute-done | bytes 262176 | tf_op jit(solution)/shard_map/ppermute | solution.py:43
  145.0 3.1 %collective-permute-done.12 = bf16[1024,128]{1,0:T(8,128)(2,1)S(1)} collective-permute-done((bf16[1024,128]{1,0:T(8,128)(2,1)S(1)}, bf16[1024,128]{1,0:T(8,128)(2,1)S(1)}, u32[]{:S(2)}, u32[]{:S(2)}) %collective-permute-start.12) | collective-permute-done | bytes 262176 | tf_op jit(solution)/shard_map/ppermute | solution.py:43
  148.2 1.9 collective-permute-start.13
  150.1 1.9 collective-permute-start.14
  152.1 3.9 %collective-permute-start.15 = (bf16[1024,128]{1,0:T(8,128)(2,1)S(1)}, bf16[1024,128]{1,0:T(8,128)(2,1)S(1)}, u32[]{:S(2)}, u32[]{:S(2)}) collective-permute-start(bf16[1024,128]{1,0:T(8,128)(2,1)S(1)} %collective-permute-done.12), channel_id=1, source_target_pairs={{0,14},{1,15},{2,0},{3,1},{4,2},{5,3},{6,4},{7,5},{8,6},{9,7},{10,... | collective-permute-start | bytes 786440 | tf_op jit(solution)/shard_map/ppermute | solution.py:43
  156.5 4.3 %collective-permute-done.14 = bf16[1024,128]{1,0:T(8,128)(2,1)S(1)} collective-permute-done((bf16[1024,128]{1,0:T(8,128)(2,1)S(1)}, bf16[1024,128]{1,0:T(8,128)(2,1)S(1)}, u32[]{:S(2)}, u32[]{:S(2)}) %collective-permute-start.14) | collective-permute-done | bytes 262176 | tf_op jit(solution)/shard_map/ppermute | solution.py:43
  160.8 3.4 %collective-permute-start.17 = (bf16[512,128]{1,0:T(8,128)(2,1)S(1)}, bf16[512,128]{1,0:T(8,128)(2,1)S(1)}, u32[]{:S(2)}, u32[]{:S(2)}) collective-permute-start(bf16[512,128]{1,0:T(8,128)(2,1)S(1)} %slice.184), channel_id=1, source_target_pairs={{0,2},{1,3},{2,4},{3,5},{4,6},{5,7},{6,8},{7,9},{8,10},{9,11},{10,... | collective-permute-start | bytes 393224 | tf_op jit(solution)/shard_map/ppermute | solution.py:43
  164.2 2.4 %collective-permute-start.18 = (bf16[512,128]{1,0:T(8,128)(2,1)S(1)}, bf16[512,128]{1,0:T(8,128)(2,1)S(1)}, u32[]{:S(2)}, u32[]{:S(2)}) collective-permute-start(bf16[512,128]{1,0:T(8,128)(2,1)S(1)} %slice.185), channel_id=1, source_target_pairs={{0,14},{1,15},{2,0},{3,1},{4,2},{5,3},{6,4},{7,5},{8,6},{9,7},{10,... | collective-permute-start | bytes 393224 | tf_op jit(solution)/shard_map/ppermute | solution.py:43
  166.7 1.9 collective-permute-start.16
  170.3 2.1 collective-permute-done.18
  172.4 1.9 collective-permute-start.19
  178.3 2.3 collective-permute-start.20
  182.7 3.1 %collective-permute-start.21 = (bf16[512,128]{1,0:T(8,128)(2,1)S(1)}, bf16[512,128]{1,0:T(8,128)(2,1)S(1)}, u32[]{:S(2)}, u32[]{:S(2)}) collective-permute-start(bf16[512,128]{1,0:T(8,128)(2,1)S(1)} %get-tuple-element.67), channel_id=1, source_target_pairs={{0,2},{1,3},{2,4},{3,5},{4,6},{5,7},{6,8},{7,9},{8,10},{9,11},{10,... | collective-permute-start | bytes 393224 | tf_op jit(solution)/shard_map/ppermute | solution.py:43
  186.5 2.9 %collective-permute-start.25 = (bf16[512,128]{1,0:T(8,128)(2,1)S(1)}, bf16[512,128]{1,0:T(8,128)(2,1)S(1)}, u32[]{:S(2)}, u32[]{:S(2)}) collective-permute-start(bf16[512,128]{1,0:T(8,128)(2,1)S(1)} %get-tuple-element.68), channel_id=1, source_target_pairs={{0,14},{1,15},{2,0},{3,1},{4,2},{5,3},{6,4},{7,5},{8,6},{9,7},{10,... | collective-permute-start | bytes 393224 | tf_op jit(solution)/shard_map/ppermute | solution.py:43
  190.5 3.9 %collective-permute-start.22 = (bf16[1024,128]{1,0:T(8,128)(2,1)S(1)}, bf16[1024,128]{1,0:T(8,128)(2,1)S(1)}, u32[]{:S(2)}, u32[]{:S(2)}) collective-permute-start(bf16[1024,128]{1,0:T(8,128)(2,1)S(1)} %fusion.78), channel_id=1, source_target_pairs={{0,2},{1,3},{2,4},{3,5},{4,6},{5,7},{6,8},{7,9},{8,10},{9,11},{10,... | collective-permute-start | bytes 786440 | tf_op jit(solution)/shard_map/ppermute | solution.py:43
  195.3 1.9 collective-permute-start.26
  197.3 2.9 %collective-permute-done.22 = bf16[1024,128]{1,0:T(8,128)(2,1)S(1)} collective-permute-done((bf16[1024,128]{1,0:T(8,128)(2,1)S(1)}, bf16[1024,128]{1,0:T(8,128)(2,1)S(1)}, u32[]{:S(2)}, u32[]{:S(2)}) %collective-permute-start.22) | collective-permute-done | bytes 262176 | tf_op jit(solution)/shard_map/ppermute | solution.py:43
  200.2 4.9 %collective-permute-start.23 = (bf16[1024,128]{1,0:T(8,128)(2,1)S(1)}, bf16[1024,128]{1,0:T(8,128)(2,1)S(1)}, u32[]{:S(2)}, u32[]{:S(2)}) collective-permute-start(bf16[1024,128]{1,0:T(8,128)(2,1)S(1)} %fusion.77), channel_id=1, source_target_pairs={{0,2},{1,3},{2,4},{3,5},{4,6},{5,7},{6,8},{7,9},{8,10},{9,11},{10,... | collective-permute-start | bytes 786440 | tf_op jit(solution)/shard_map/ppermute | solution.py:43
  205.8 1.9 collective-permute-start.27
  209.3 5.6 %collective-permute-start.24 = (bf16[1024,128]{1,0:T(8,128)(2,1)S(1)}, bf16[1024,128]{1,0:T(8,128)(2,1)S(1)}, u32[]{:S(2)}, u32[]{:S(2)}) collective-permute-start(bf16[1024,128]{1,0:T(8,128)(2,1)S(1)} %fusion.76), channel_id=1, source_target_pairs={{0,2},{1,3},{2,4},{3,5},{4,6},{5,7},{6,8},{7,9},{8,10},{9,11},{10,... | collective-permute-start | bytes 786440 | tf_op jit(solution)/shard_map/ppermute | solution.py:43
  215.3 1.9 collective-permute-start.28
  218.8 6.0 %collective-permute-done.28 = bf16[1024,128]{1,0:T(8,128)(2,1)S(1)} collective-permute-done((bf16[1024,128]{1,0:T(8,128)(2,1)S(1)}, bf16[1024,128]{1,0:T(8,128)(2,1)S(1)}, u32[]{:S(2)}, u32[]{:S(2)}) %collective-permute-start.28) | collective-permute-done | bytes 262176 | tf_op jit(solution)/shard_map/ppermute | solution.py:43
  225.6 4.6 %all-to-all-start.3 = ((bf16[32,32,128]{2,1,0:T(8,128)(2,1)}), bf16[32,32,128]{2,1,0:T(8,128)(2,1)S(1)}, u32[]{:S(2)}, u32[]{:S(2)}) async-start(bf16[32,32,128]{2,1,0:T(8,128)(2,1)} %bitcast.86), calls=%async_computation.3 | async-start | bytes 524288 | tf_op jit(solution)/shard_map/all_to_all | solution.py:27
  230.2 11.5 %all-to-all-done.3 = bf16[32,32,128]{2,1,0:T(8,128)(2,1)S(1)} async-done(((bf16[32,32,128]{2,1,0:T(8,128)(2,1)}), bf16[32,32,128]{2,1,0:T(8,128)(2,1)S(1)}, u32[]{:S(2)}, u32[]{:S(2)}) %all-to-all-start.3) | async-done | bytes 262176 | tf_op jit(solution)/shard_map/all_to_all | solution.py:27
  (181 shorter events, 46.5 us)
Async XLA Ops:
  0.0 95.7 %copy-start = (bf16[1024,128]{1,0:T(8,128)(2,1)S(1)}, bf16[1024,128]{1,0:T(8,128)(2,1)}, u32[]{:S(2)}) copy-start(bf16[1024,128]{1,0:T(8,128)(2,1)} %param.19) | copy-start | bytes 786436
  2.3 31.7 %copy-start.12 = (s32[256,2]{0,1:T(2,128)S(1)}, s32[256,2]{0,1:T(2,128)}, u32[]{:S(2)}) copy-start(s32[256,2]{0,1:T(2,128)} %param.22) | copy-start | bytes 6148
  3.0 31.1 %copy-start.17 = (bf16[2048]{0:T(1024)(128)(2,1)S(1)}, bf16[2048]{0:T(1024)(128)(2,1)}, u32[]{:S(2)}) copy-start(bf16[2048]{0:T(1024)(128)(2,1)} %param.21) | copy-start | bytes 12292
  3.1 36.7 %collective-permute-start = (bf16[256,96]{0,1:T(8,128)(2,1)}, bf16[256,96]{0,1:T(8,128)(2,1)S(1)}, u32[]{:S(2)}, u32[]{:S(2)}) collective-permute-start(bf16[256,96]{0,1:T(8,128)(2,1)} %get-tuple-element.96), channel_id=1, source_target_pairs={{0,16},{16,32},{32,48},{48,0},{64,80},{80,96},{96,112},{112,64},{1... | collective-permute-start | bytes 147464 | tf_op jit(solution)/shard_map/ppermute | solution.py:37
  6.6 33.2 %collective-permute-start.1 = (bf16[256,96]{0,1:T(8,128)(2,1)}, bf16[256,96]{0,1:T(8,128)(2,1)S(1)}, u32[]{:S(2)}, u32[]{:S(2)}) collective-permute-start(bf16[256,96]{0,1:T(8,128)(2,1)} %get-tuple-element.96), channel_id=1, source_target_pairs={{0,32},{16,48},{32,0},{48,16},{64,96},{80,112},{96,64},{112,80},{1... | collective-permute-start | bytes 147464 | tf_op jit(solution)/shard_map/ppermute | solution.py:37
  11.2 28.6 %collective-permute-start.2 = (bf16[256,96]{0,1:T(8,128)(2,1)}, bf16[256,96]{0,1:T(8,128)(2,1)}, u32[]{:S(2)}, u32[]{:S(2)}) collective-permute-start(bf16[256,96]{0,1:T(8,128)(2,1)} %get-tuple-element.96), channel_id=1, source_target_pairs={{0,48},{16,0},{32,16},{48,32},{64,112},{80,64},{96,80},{112,96},{1... | collective-permute-start | bytes 147464 | tf_op jit(solution)/shard_map/ppermute | solution.py:37
  16.5 24.8 %collective-permute-start.3 = (bf16[4,512,128]{2,1,0:T(8,128)(2,1)}, bf16[4,512,128]{2,1,0:T(8,128)(2,1)}, u32[]{:S(2)}, u32[]{:S(2)}) collective-permute-start(bf16[4,512,128]{2,1,0:T(8,128)(2,1)} %dynamic-slice_bitcast_fusion), channel_id=1, source_target_pairs={{0,2},{1,3},{2,0},{3,1},{4,6},{5,7},{6,4},{7,5},{8,10},{9,11},{10,... | collective-permute-start | bytes 1572872 | tf_op jit(solution)/shard_map/ppermute | solution.py:122
  23.6 31.2 %all-to-all-start = ((bf16[8,160,256]{2,1,0:T(8,128)(2,1)}), bf16[8,160,256]{2,1,0:T(8,128)(2,1)}, u32[]{:S(2)}, u32[]{:S(2)}) async-start(bf16[8,160,256]{2,1,0:T(8,128)(2,1)} %broadcast_in_dim.9), calls=%async_computation | async-start | bytes 1310720 | tf_op jit(solution)/shard_map/all_to_all | solution.py:27
  43.3 25.0 %collective-permute-start.4 = (bf16[2,512,128]{2,1,0:T(8,128)(2,1)}, bf16[2,512,128]{2,1,0:T(8,128)(2,1)}, u32[]{:S(2)}, u32[]{:S(2)}) collective-permute-start(bf16[2,512,128]{2,1,0:T(8,128)(2,1)} %get-tuple-element.54), channel_id=1, source_target_pairs={{0,4},{1,5},{2,6},{3,7},{4,8},{5,9},{6,10},{7,11},{8,12},{9,13},{1... | collective-permute-start | bytes 786440 | tf_op jit(solution)/shard_map/ppermute | solution.py:43
  45.2 23.1 %collective-permute-start.5 = (bf16[2,512,128]{2,1,0:T(8,128)(2,1)}, bf16[2,512,128]{2,1,0:T(8,128)(2,1)}, u32[]{:S(2)}, u32[]{:S(2)}) collective-permute-start(bf16[2,512,128]{2,1,0:T(8,128)(2,1)} %get-tuple-element.55), channel_id=1, source_target_pairs={{0,8},{1,9},{2,10},{3,11},{4,12},{5,13},{6,14},{7,15},{8,0},{9,1},... | collective-permute-start | bytes 786440 | tf_op jit(solution)/shard_map/ppermute | solution.py:43
  52.9 16.6 %collective-permute-start.6 = (bf16[2,512,128]{2,1,0:T(8,128)(2,1)S(1)}, bf16[2,512,128]{2,1,0:T(8,128)(2,1)}, u32[]{:S(2)}, u32[]{:S(2)}) collective-permute-start(bf16[2,512,128]{2,1,0:T(8,128)(2,1)S(1)} %get-tuple-element.56), channel_id=1, source_target_pairs={{0,12},{1,13},{2,14},{3,15},{4,0},{5,1},{6,2},{7,3},{8,4},{9,5},{1... | collective-permute-start | bytes 786440 | tf_op jit(solution)/shard_map/ppermute | solution.py:43
  62.7 32.9 %copy-start.6 = (bf16[256,128]{1,0:T(8,128)(2,1)S(1)}, bf16[256,128]{1,0:T(8,128)(2,1)}, u32[]{:S(2)}) copy-start(bf16[256,128]{1,0:T(8,128)(2,1)} %param.20) | copy-start | bytes 196612
  63.5 11.0 %all-to-all-start.1 = ((f32[4,72,256]{2,1,0:T(8,128)}), f32[4,72,256]{2,1,0:T(8,128)}, u32[]{:S(2)}, u32[]{:S(2)}) async-start(f32[4,72,256]{2,1,0:T(8,128)} %pad_maximum_fusion.11), calls=%async_computation.1 | async-start | bytes 589824 | tf_op jit(solution)/shard_map/all_to_all | solution.py:27
  74.5 21.5 %copy-start.1 = (bf16[256,1024]{1,0:T(8,128)(2,1)S(1)}, bf16[256,1024]{1,0:T(8,128)(2,1)}, u32[]{:S(2)}) copy-start(bf16[256,1024]{1,0:T(8,128)(2,1)} %fusion.72) | copy-start | bytes 1572868
  97.1 21.0 %all-to-all-start.2 = ((bf16[32,32,128]{2,1,0:T(8,128)(2,1)}), bf16[32,32,128]{2,1,0:T(8,128)(2,1)}, u32[]{:S(2)}, u32[]{:S(2)}) async-start(bf16[32,32,128]{2,1,0:T(8,128)(2,1)} %bitcast.178), calls=%async_computation.2 | async-start | bytes 524288 | tf_op jit(solution)/shard_map/all_to_all | solution.py:27
  118.1 22.3 %copy-start.28 = (f32[128]{0:T(128)S(1)}, f32[128]{0:T(128)}, u32[]{:S(2)}) copy-start(f32[128]{0:T(128)} %get-tuple-element.114) | copy-start | bytes 1540
  118.1 9.9 %collective-permute-start.8 = (bf16[1024,128]{1,0:T(8,128)(2,1)}, bf16[1024,128]{1,0:T(8,128)(2,1)S(1)}, u32[]{:S(2)}, u32[]{:S(2)}) collective-permute-start(bf16[1024,128]{1,0:T(8,128)(2,1)} %bitcast.29), channel_id=1, source_target_pairs={{0,2},{1,3},{2,4},{3,5},{4,6},{5,7},{6,8},{7,9},{8,10},{9,11},{10,... | collective-permute-start | bytes 786440 | tf_op jit(solution)/shard_map/ppermute | solution.py:43
  122.7 9.7 %collective-permute-start.9 = (bf16[1024,128]{1,0:T(8,128)(2,1)}, bf16[1024,128]{1,0:T(8,128)(2,1)S(1)}, u32[]{:S(2)}, u32[]{:S(2)}) collective-permute-start(bf16[1024,128]{1,0:T(8,128)(2,1)} %bitcast.29), channel_id=1, source_target_pairs={{0,14},{1,15},{2,0},{3,1},{4,2},{5,3},{6,4},{7,5},{8,6},{9,7},{10,... | collective-permute-start | bytes 786440 | tf_op jit(solution)/shard_map/ppermute | solution.py:43
  124.9 15.8 %copy-start.27 = (f32[128]{0:T(128)S(1)}, f32[128]{0:T(128)}, u32[]{:S(2)}) copy-start(f32[128]{0:T(128)} %get-tuple-element.115) | copy-start | bytes 1540
  124.9 15.8 %collective-permute-start.7 = (bf16[1024,128]{1,0:T(8,128)(2,1)}, bf16[1024,128]{1,0:T(8,128)(2,1)S(1)}, u32[]{:S(2)}, u32[]{:S(2)}) collective-permute-start(bf16[1024,128]{1,0:T(8,128)(2,1)} %bitcast.29), channel_id=1, source_target_pairs={{0,1},{1,0},{2,3},{3,2},{4,5},{5,4},{6,7},{7,6},{8,9},{9,8},{10,11... | collective-permute-start | bytes 786440 | tf_op jit(solution)/shard_map/ppermute | solution.py:33
  132.5 36.6 %collective-permute-start.10 = (bf16[1024,256]{1,0:T(8,128)(2,1)S(1)}, bf16[1024,256]{1,0:T(8,128)(2,1)S(1)}, u32[]{:S(2)}, u32[]{:S(2)}) collective-permute-start(bf16[1024,256]{1,0:T(8,128)(2,1)S(1)} %pad_maximum_fusion.4), channel_id=1, source_target_pairs={{0,1},{1,0},{2,3},{3,2},{4,5},{5,4},{6,7},{7,6},{8,9},{9,8},{10,11... | collective-permute-start | bytes 1572872 | tf_op jit(solution)/shard_map/ppermute | solution.py:33
  134.4 10.6 %collective-permute-start.11 = (bf16[1024,128]{1,0:T(8,128)(2,1)S(1)}, bf16[1024,128]{1,0:T(8,128)(2,1)S(1)}, u32[]{:S(2)}, u32[]{:S(2)}) collective-permute-start(bf16[1024,128]{1,0:T(8,128)(2,1)S(1)} %collective-permute-done.8), channel_id=1, source_target_pairs={{0,2},{1,3},{2,4},{3,5},{4,6},{5,7},{6,8},{7,9},{8,10},{9,11},{10,... | collective-permute-start | bytes 786440 | tf_op jit(solution)/shard_map/ppermute | solution.py:43
  136.3 11.8 %collective-permute-start.12 = (bf16[1024,128]{1,0:T(8,128)(2,1)S(1)}, bf16[1024,128]{1,0:T(8,128)(2,1)S(1)}, u32[]{:S(2)}, u32[]{:S(2)}) collective-permute-start(bf16[1024,128]{1,0:T(8,128)(2,1)S(1)} %collective-permute-done.9), channel_id=1, source_target_pairs={{0,14},{1,15},{2,0},{3,1},{4,2},{5,3},{6,4},{7,5},{8,6},{9,7},{10,... | collective-permute-start | bytes 786440 | tf_op jit(solution)/shard_map/ppermute | solution.py:43
  141.4 27.2 %copy-start.23 = (f32[128]{0:T(128)S(1)}, f32[128]{0:T(128)}, u32[]{:S(2)}) copy-start(f32[128]{0:T(128)} %get-tuple-element.106) | copy-start | bytes 1540
  141.6 27.2 %copy-start.22 = (f32[128]{0:T(128)S(1)}, f32[128]{0:T(128)}, u32[]{:S(2)}) copy-start(f32[128]{0:T(128)} %get-tuple-element.105) | copy-start | bytes 1540
  148.2 20.9 %copy-start.18 = (f32[128]{0:T(128)S(1)}, f32[128]{0:T(128)}, u32[]{:S(2)}) copy-start(f32[128]{0:T(128)} %get-tuple-element.111) | copy-start | bytes 1540
  148.2 20.9 %copy-start.19 = (f32[128]{0:T(128)S(1)}, f32[128]{0:T(128)}, u32[]{:S(2)}) copy-start(f32[128]{0:T(128)} %get-tuple-element.112) | copy-start | bytes 1540
  148.2 26.3 %collective-permute-start.13 = (bf16[1024,256]{1,0:T(8,128)(2,1)S(1)}, bf16[1024,256]{1,0:T(8,128)(2,1)S(1)}, u32[]{:S(2)}, u32[]{:S(2)}) collective-permute-start(bf16[1024,256]{1,0:T(8,128)(2,1)S(1)} %pad_maximum_fusion.5), channel_id=1, source_target_pairs={{0,1},{1,0},{2,3},{3,2},{4,5},{5,4},{6,7},{7,6},{8,9},{9,8},{10,11... | collective-permute-start | bytes 1572872 | tf_op jit(solution)/shard_map/ppermute | solution.py:33
  150.1 10.6 %collective-permute-start.14 = (bf16[1024,128]{1,0:T(8,128)(2,1)S(1)}, bf16[1024,128]{1,0:T(8,128)(2,1)S(1)}, u32[]{:S(2)}, u32[]{:S(2)}) collective-permute-start(bf16[1024,128]{1,0:T(8,128)(2,1)S(1)} %collective-permute-done.11), channel_id=1, source_target_pairs={{0,2},{1,3},{2,4},{3,5},{4,6},{5,7},{6,8},{7,9},{8,10},{9,11},{10,... | collective-permute-start | bytes 786440 | tf_op jit(solution)/shard_map/ppermute | solution.py:43
  152.1 12.1 %collective-permute-start.15 = (bf16[1024,128]{1,0:T(8,128)(2,1)S(1)}, bf16[1024,128]{1,0:T(8,128)(2,1)S(1)}, u32[]{:S(2)}, u32[]{:S(2)}) collective-permute-start(bf16[1024,128]{1,0:T(8,128)(2,1)S(1)} %collective-permute-done.12), channel_id=1, source_target_pairs={{0,14},{1,15},{2,0},{3,1},{4,2},{5,3},{6,4},{7,5},{8,6},{9,7},{10,... | collective-permute-start | bytes 786440 | tf_op jit(solution)/shard_map/ppermute | solution.py:43
  160.8 9.5 %collective-permute-start.17 = (bf16[512,128]{1,0:T(8,128)(2,1)S(1)}, bf16[512,128]{1,0:T(8,128)(2,1)S(1)}, u32[]{:S(2)}, u32[]{:S(2)}) collective-permute-start(bf16[512,128]{1,0:T(8,128)(2,1)S(1)} %slice.184), channel_id=1, source_target_pairs={{0,2},{1,3},{2,4},{3,5},{4,6},{5,7},{6,8},{7,9},{8,10},{9,11},{10,... | collective-permute-start | bytes 393224 | tf_op jit(solution)/shard_map/ppermute | solution.py:43
  164.2 8.1 %collective-permute-start.18 = (bf16[512,128]{1,0:T(8,128)(2,1)S(1)}, bf16[512,128]{1,0:T(8,128)(2,1)S(1)}, u32[]{:S(2)}, u32[]{:S(2)}) collective-permute-start(bf16[512,128]{1,0:T(8,128)(2,1)S(1)} %slice.185), channel_id=1, source_target_pairs={{0,14},{1,15},{2,0},{3,1},{4,2},{5,3},{6,4},{7,5},{8,6},{9,7},{10,... | collective-permute-start | bytes 393224 | tf_op jit(solution)/shard_map/ppermute | solution.py:43
  166.7 9.3 %collective-permute-start.16 = (bf16[1024,256]{1,0:T(8,128)(2,1)S(1)}, bf16[1024,256]{1,0:T(8,128)(2,1)S(1)}, u32[]{:S(2)}, u32[]{:S(2)}) collective-permute-start(bf16[1024,256]{1,0:T(8,128)(2,1)S(1)} %pad_maximum_fusion.6), channel_id=1, source_target_pairs={{0,1},{1,0},{2,3},{3,2},{4,5},{5,4},{6,7},{7,6},{8,9},{9,8},{10,11... | collective-permute-start | bytes 1572872 | tf_op jit(solution)/shard_map/ppermute | solution.py:33
  172.4 3.4 %collective-permute-start.19 = (bf16[1024,128]{1,0:T(8,128)(2,1)S(1)}, bf16[1024,128]{1,0:T(8,128)(2,1)S(1)}, u32[]{:S(2)}, u32[]{:S(2)}) collective-permute-start(bf16[1024,128]{1,0:T(8,128)(2,1)S(1)} %constant_dynamic-update-slice_fusion), channel_id=1, source_target_pairs={{0,1},{1,0},{2,3},{3,2},{4,5},{5,4},{6,7},{7,6},{8,9},{9,8},{10,11... | collective-permute-start | bytes 786440 | tf_op jit(solution)/shard_map/ppermute | solution.py:33
  178.3 3.8 %collective-permute-start.20 = (bf16[1024,256]{0,1:T(8,128)(2,1)S(1)}, bf16[1024,256]{0,1:T(8,128)(2,1)S(1)}, u32[]{:S(2)}, u32[]{:S(2)}) collective-permute-start(bf16[1024,256]{0,1:T(8,128)(2,1)S(1)} %fusion.13), channel_id=1, source_target_pairs={{0,1},{1,0},{2,3},{3,2},{4,5},{5,4},{6,7},{7,6},{8,9},{9,8},{10,11... | collective-permute-start | bytes 1572872 | tf_op jit(solution)/shard_map/ppermute | solution.py:33
  182.7 7.8 %collective-permute-start.21 = (bf16[512,128]{1,0:T(8,128)(2,1)S(1)}, bf16[512,128]{1,0:T(8,128)(2,1)S(1)}, u32[]{:S(2)}, u32[]{:S(2)}) collective-permute-start(bf16[512,128]{1,0:T(8,128)(2,1)S(1)} %get-tuple-element.67), channel_id=1, source_target_pairs={{0,2},{1,3},{2,4},{3,5},{4,6},{5,7},{6,8},{7,9},{8,10},{9,11},{10,... | collective-permute-start | bytes 393224 | tf_op jit(solution)/shard_map/ppermute | solution.py:43
  186.5 8.7 %collective-permute-start.25 = (bf16[512,128]{1,0:T(8,128)(2,1)S(1)}, bf16[512,128]{1,0:T(8,128)(2,1)S(1)}, u32[]{:S(2)}, u32[]{:S(2)}) collective-permute-start(bf16[512,128]{1,0:T(8,128)(2,1)S(1)} %get-tuple-element.68), channel_id=1, source_target_pairs={{0,14},{1,15},{2,0},{3,1},{4,2},{5,3},{6,4},{7,5},{8,6},{9,7},{10,... | collective-permute-start | bytes 393224 | tf_op jit(solution)/shard_map/ppermute | solution.py:43
  190.5 9.6 %collective-permute-start.22 = (bf16[1024,128]{1,0:T(8,128)(2,1)S(1)}, bf16[1024,128]{1,0:T(8,128)(2,1)S(1)}, u32[]{:S(2)}, u32[]{:S(2)}) collective-permute-start(bf16[1024,128]{1,0:T(8,128)(2,1)S(1)} %fusion.78), channel_id=1, source_target_pairs={{0,2},{1,3},{2,4},{3,5},{4,6},{5,7},{6,8},{7,9},{8,10},{9,11},{10,... | collective-permute-start | bytes 786440 | tf_op jit(solution)/shard_map/ppermute | solution.py:43
  195.3 10.3 %collective-permute-start.26 = (bf16[1024,128]{1,0:T(8,128)(2,1)S(1)}, bf16[1024,128]{1,0:T(8,128)(2,1)S(1)}, u32[]{:S(2)}, u32[]{:S(2)}) collective-permute-start(bf16[1024,128]{1,0:T(8,128)(2,1)S(1)} %fusion.75), channel_id=1, source_target_pairs={{0,14},{1,15},{2,0},{3,1},{4,2},{5,3},{6,4},{7,5},{8,6},{9,7},{10,... | collective-permute-start | bytes 786440 | tf_op jit(solution)/shard_map/ppermute | solution.py:43
  200.2 9.0 %collective-permute-start.23 = (bf16[1024,128]{1,0:T(8,128)(2,1)S(1)}, bf16[1024,128]{1,0:T(8,128)(2,1)S(1)}, u32[]{:S(2)}, u32[]{:S(2)}) collective-permute-start(bf16[1024,128]{1,0:T(8,128)(2,1)S(1)} %fusion.77), channel_id=1, source_target_pairs={{0,2},{1,3},{2,4},{3,5},{4,6},{5,7},{6,8},{7,9},{8,10},{9,11},{10,... | collective-permute-start | bytes 786440 | tf_op jit(solution)/shard_map/ppermute | solution.py:43
  205.7 24.4 %copy-start.11 = (f32[256,2]{0,1:T(2,128)S(1)}, f32[256,2]{0,1:T(2,128)}, u32[]{:S(2)}) copy-start(f32[256,2]{0,1:T(2,128)} %param.23) | copy-start | bytes 6148
  205.7 24.5 %copy-start.30 = (f32[256]{0:T(256)S(1)}, f32[256]{0:T(256)}, u32[]{:S(2)}) copy-start(f32[256]{0:T(256)} %param.24) | copy-start | bytes 3076
  205.7 36.0 %copy-start.16 = (s32[256,1]{0,1:T(1,128)S(1)}, s32[256,1]{0,1:T(1,128)}, u32[]{:S(2)}) copy-start(s32[256,1]{0,1:T(1,128)} %copy-done.15) | copy-start | bytes 3076
  205.7 36.3 %copy-start.14 = (s32[256,1]{0,1:T(1,128)S(1)}, s32[256,1]{0,1:T(1,128)}, u32[]{:S(2)}) copy-start(s32[256,1]{0,1:T(1,128)} %copy-done.13) | copy-start | bytes 3076
  205.8 9.5 %collective-permute-start.27 = (bf16[1024,128]{1,0:T(8,128)(2,1)S(1)}, bf16[1024,128]{1,0:T(8,128)(2,1)S(1)}, u32[]{:S(2)}, u32[]{:S(2)}) collective-permute-start(bf16[1024,128]{1,0:T(8,128)(2,1)S(1)} %fusion.74), channel_id=1, source_target_pairs={{0,14},{1,15},{2,0},{3,1},{4,2},{5,3},{6,4},{7,5},{8,6},{9,7},{10,... | collective-permute-start | bytes 786440 | tf_op jit(solution)/shard_map/ppermute | solution.py:43
  209.3 9.5 %collective-permute-start.24 = (bf16[1024,128]{1,0:T(8,128)(2,1)S(1)}, bf16[1024,128]{1,0:T(8,128)(2,1)S(1)}, u32[]{:S(2)}, u32[]{:S(2)}) collective-permute-start(bf16[1024,128]{1,0:T(8,128)(2,1)S(1)} %fusion.76), channel_id=1, source_target_pairs={{0,2},{1,3},{2,4},{3,5},{4,6},{5,7},{6,8},{7,9},{8,10},{9,11},{10,... | collective-permute-start | bytes 786440 | tf_op jit(solution)/shard_map/ppermute | solution.py:43
  215.3 9.5 %collective-permute-start.28 = (bf16[1024,128]{1,0:T(8,128)(2,1)S(1)}, bf16[1024,128]{1,0:T(8,128)(2,1)S(1)}, u32[]{:S(2)}, u32[]{:S(2)}) collective-permute-start(bf16[1024,128]{1,0:T(8,128)(2,1)S(1)} %fusion.73), channel_id=1, source_target_pairs={{0,14},{1,15},{2,0},{3,1},{4,2},{5,3},{6,4},{7,5},{8,6},{9,7},{10,... | collective-permute-start | bytes 786440 | tf_op jit(solution)/shard_map/ppermute | solution.py:43
  225.6 16.1 %all-to-all-start.3 = ((bf16[32,32,128]{2,1,0:T(8,128)(2,1)}), bf16[32,32,128]{2,1,0:T(8,128)(2,1)S(1)}, u32[]{:S(2)}, u32[]{:S(2)}) async-start(bf16[32,32,128]{2,1,0:T(8,128)(2,1)} %bitcast.86), calls=%async_computation.3 | async-start | bytes 524288 | tf_op jit(solution)/shard_map/all_to_all | solution.py:27
  (17 other events, 111.4 us)

commit v3 on v2

--- a/solution.py
+++ b/solution.py
@@ -33,10 +33,8 @@
     return lax.ppermute(value, "tp", [(t, t ^ 1) for t in range(TP)])
 
 
-def x_shift(value, by):
-    return lax.ppermute(
-        value, "sp", [(s, s // X * X + (s + by) % X) for s in range(SP)]
-    )
+def x_swap(value, bit):
+    return lax.ppermute(value, "sp", [(s, s ^ bit) for s in range(SP)])
 
 
 def y_step(value, by):
@@ -104,17 +102,11 @@
     query = jnp.concatenate([queries[:, :NOPE], rotate(queries[:, NOPE:], positions)], axis=1)
     blocks = exchange(jnp.broadcast_to(block, (Z,) + block.shape), "sp", Z_GROUPS)
 
-    query_parts = [query]
-    for by in range(1, X):
-        query_parts.append(x_shift(query, by))
-    query_parts = jnp.stack(query_parts)
+    query_parts = jnp.stack([query, x_swap(query, 1)])
+    query_parts = jnp.concatenate([query_parts, x_swap(query_parts, 2)], axis=0)
     at = lambda a, chip: lax.dynamic_index_in_dim(a, chip, 0, keepdims=False)
-    query_all = jnp.concatenate([at(query_parts, (x - one) % X) for one in range(X)], axis=0)
-
-    gate_up_weight = jnp.concatenate(
-        [gate_weight.reshape(TP, width, ff), up_weight.reshape(TP, width, ff)], axis=2
-    )
-    gains = ffn_gain.astype(f32).reshape(TP, width)
+    query_all = jnp.concatenate([at(query_parts, x ^ one) for one in range(X)], axis=0)
+
     down = down_weight.reshape(Y // 2, 2, 2 * ff, width)
     odd = y % 2
     parity = lambda one: lax.dynamic_index_in_dim(down, one, 1, keepdims=False)
@@ -163,9 +155,7 @@
     factors = jnp.exp(tops - jnp.max(tops, axis=0, keepdims=True))
     merged = jnp.sum(factors[:, None, :] * packed, axis=0)
     attended = (merged[:VDIM] / merged[VDIM + 1 : VDIM + 2]).astype(bf16)
-    attended, gate_up_weight, placed = lax.optimization_barrier(
-        (attended, gate_up_weight, placed)
-    )
+    attended, placed = lax.optimization_barrier((attended, placed))
 
     attended_all = lax.all_gather(attended, "tp", axis=0, tiled=True)
     projected = lax.dot_general(
@@ -174,7 +164,14 @@
     mixed = (residual.astype(f32) + projected).astype(bf16)
 
     sent = lax.dot_general(placed, mixed, (((0,), (0,)), ((), ())), preferred_element_type=f32)
-    arrived = exchange(sent.astype(bf16).reshape(SP, capacity, width), "sp")
+    sent, gate_weight, up_weight, ffn_gain, down = lax.optimization_barrier(
+        (sent.astype(bf16), gate_weight, up_weight, ffn_gain, down)
+    )
+    arrived = exchange(sent.reshape(SP, capacity, width), "sp")
+    gate_up_weight = jnp.concatenate(
+        [gate_weight.reshape(TP, width, ff), up_weight.reshape(TP, width, ff)], axis=2
+    )
+    gains = ffn_gain.astype(f32).reshape(TP, width)
     down = jnp.stack(down).reshape(Y, 2, ff, width)
     down = jnp.where(core == 0, down, down[:, ::-1]).reshape(Y, 2 * ff, width)
 
@@ -186,8 +183,8 @@
         return jnp.concatenate(parts, axis=1)
 
     down_first, down_above, down_below = features([4]), features([3, 2, 1]), features([-3, -2, -1, 0])
-    arrived, down_first, down_above, down_below = lax.optimization_barrier(
-        (arrived.reshape(slots, width), down_first, down_above, down_below)
+    arrived, gate_up_weight, gains, down_first, down_above, down_below = lax.optimization_barrier(
+        (arrived.reshape(slots, width), gate_up_weight, gains, down_first, down_above, down_below)
     )
 
     def products(parts):

time: 245 us -> 242 us (0.988)
  other arithmetic: 26.2 us -> 12.5 us
  blocking collectives: 18.5 us -> 29.1 us
    all_gather x1, blocking collectives: 18.5 us -> 29.1 us  [body(): attended_all = lax.all_gather(attended, 'tp', axis=0, tiled=True)]
    ppermute x19, waiting for transfers between devices: 32.2 us -> 24.5 us  [y_step(): lax.ppermute(value, 'tp', [(t, (t + 2 * by) % TP) for t in range(TP)])]
    ppermute x19, starting transfers between devices: 61.8 us -> 69.5 us  [y_step(): lax.ppermute(value, 'tp', [(t, (t + 2 * by) % TP) for t in range(TP)])]
    all_to_all x4, waiting for transfers between devices: 26.1 us -> 32.2 us  [exchange(): lax.all_to_all(value, axis, split_axis=0, concat_axis=0, tiled=True, axis...]
    ppermute x3 -> x2, starting transfers between devices: 11.5 us -> 8.04 us  [x_swap(): return lax.ppermute(value, 'sp', [(s, s ^ bit) for s in range(SP)])]
    ppermute x3 -> x2, waiting for transfers between devices: 0.01 us -> 3.35 us  [x_swap(): return lax.ppermute(value, 'sp', [(s, s ^ bit) for s in range(SP)])]
    all_to_all x4, starting transfers between devices: 26.5 us -> 23.9 us  [exchange(): lax.all_to_all(value, axis, split_axis=0, concat_axis=0, tiled=True, axis...]
  transfers between devices with their start and end apart: 33 -> 32, of which waited for: 18 -> 17; matrix products, arithmetic and copies ran while one was open for 15% -> 9% of each run, Pallas kernels for 0% -> 0%
where the time goes in v3:
time: 242 us; the launch traced here: 241 us
  starting transfers between devices  117 us (48%)
  waiting for transfers between devices  61.9 us (26%)
  blocking collectives  29.1 us (12%)
  matrix products  13.2 us (5%)
  other arithmetic  12.5 us (5%)
  local copies, waits for them, and re-layouts  5.28 us (2%)
    ppermute x19, starting transfers between devices, y_step(): lax.ppermute(value, 'tp', [(t, (t + 2 * by) % TP) for t in range(TP)])  69.5 us
    all_to_all x4, waiting for transfers between devices, exchange(): lax.all_to_all(value, axis, split_axis=0, concat_axis=0, tiled=True, axis...  32.2 us
    all_gather x1, blocking collectives, body(): attended_all = lax.all_gather(attended, 'tp', axis=0, tiled=True)  29.1 us
    ppermute x19, waiting for transfers between devices, y_step(): lax.ppermute(value, 'tp', [(t, (t + 2 * by) % TP) for t in range(TP)])  24.5 us
    all_to_all x4, starting transfers between devices, exchange(): lax.all_to_all(value, axis, split_axis=0, concat_axis=0, tiled=True, axis...  23.9 us
    ppermute x6, starting transfers between devices, swap(): return lax.ppermute(value, 'tp', [(t, t ^ 1) for t in range(TP)])  12.1 us
    ppermute x2, starting transfers between devices, x_swap(): return lax.ppermute(value, 'sp', [(s, s ^ bit) for s in range(SP)])  8.04 us
  transfers between devices with their start and end apart: 32, of which 17 were waited for; matrix products, arithmetic and copies ran while one was open for 9% of the time, Pallas kernels for 0%

profile of v3, /device:TPU:56, one launch (start us, length us, event | category | flops | bytes accessed | tf_op | source)
XLA Modules:
  0.0 240.6 jit_solution(3328808792170669420)
XLA Ops:
  2.4 3.4 %collective-permute-start = (bf16[256,96]{0,1:T(8,128)(2,1)S(1)}, bf16[256,96]{0,1:T(8,128)(2,1)S(1)}, u32[]{:S(2)}, u32[]{:S(2)}) collective-permute-start(bf16[256,96]{0,1:T(8,128)(2,1)S(1)} %get-tuple-element.114), channel_id=1, source_target_pairs={{0,16},{16,0},{32,48},{48,32},{64,80},{80,64},{96,112},{112,96},{1... | collective-permute-start | bytes 147464 | tf_op jit(solution)/shard_map/ppermute | solution.py:37
  7.0 3.3 %collective-permute-start.2 = (bf16[4,512,128]{2,1,0:T(8,128)(2,1)S(1)}, bf16[4,512,128]{2,1,0:T(8,128)(2,1)S(1)}, u32[]{:S(2)}, u32[]{:S(2)}) collective-permute-start(bf16[4,512,128]{2,1,0:T(8,128)(2,1)S(1)} %dynamic-slice_bitcast_fusion), channel_id=1, source_target_pairs={{0,2},{1,3},{2,0},{3,1},{4,6},{5,7},{6,4},{7,5},{8,10},{9,11},{10,... | collective-permute-start | bytes 1572872 | tf_op jit(solution)/shard_map/ppermute | solution.py:114
  14.0 10.3 %all-to-all-start = ((bf16[8,160,256]{2,1,0:T(8,128)(2,1)}), bf16[8,160,256]{2,1,0:T(8,128)(2,1)S(1)}, u32[]{:S(2)}, u32[]{:S(2)}) async-start(bf16[8,160,256]{2,1,0:T(8,128)(2,1)} %broadcast_in_dim.9), calls=%async_computation | async-start | bytes 1310720 | tf_op jit(solution)/shard_map/all_to_all | solution.py:27
  25.9 4.6 %collective-permute-start.1 = (bf16[2,256,96]{1,2,0:T(8,128)(2,1)S(1)}, bf16[2,256,96]{1,2,0:T(8,128)(2,1)S(1)}, u32[]{:S(2)}, u32[]{:S(2)}) collective-permute-start(bf16[2,256,96]{1,2,0:T(8,128)(2,1)S(1)} %pad_maximum_fusion.13), channel_id=1, source_target_pairs={{0,32},{16,48},{32,0},{48,16},{64,96},{80,112},{96,64},{112,80},{1... | collective-permute-start | bytes 294920 | tf_op jit(solution)/shard_map/ppermute | solution.py:37
  30.6 3.3 %collective-permute-done.1 = bf16[2,256,96]{1,2,0:T(8,128)(2,1)S(1)} collective-permute-done((bf16[2,256,96]{1,2,0:T(8,128)(2,1)S(1)}, bf16[2,256,96]{1,2,0:T(8,128)(2,1)S(1)}, u32[]{:S(2)}, u32[]{:S(2)}) %collective-permute-start.1) | collective-permute-done | bytes 98336 | tf_op jit(solution)/shard_map/ppermute | solution.py:37
  34.0 10.1 %all-to-all-done = bf16[8,160,256]{2,1,0:T(8,128)(2,1)S(1)} async-done(((bf16[8,160,256]{2,1,0:T(8,128)(2,1)}), bf16[8,160,256]{2,1,0:T(8,128)(2,1)S(1)}, u32[]{:S(2)}, u32[]{:S(2)}) %all-to-all-start) | async-done | bytes 655392 | tf_op jit(solution)/shard_map/all_to_all | solution.py:27
  44.1 1.5 fusion.2
  45.6 2.1 fusion
  47.7 2.2 fusion.5
  50.7 4.0 %all-to-all-start.1 = ((f32[4,72,256]{2,1,0:T(8,128)}), f32[4,72,256]{2,1,0:T(8,128)S(1)}, u32[]{:S(2)}, u32[]{:S(2)}) async-start(f32[4,72,256]{2,1,0:T(8,128)} %pad_maximum_fusion.11), calls=%async_computation.1 | async-start | bytes 589824 | tf_op jit(solution)/shard_map/all_to_all | solution.py:27
  54.9 4.0 %collective-permute-start.5 = (bf16[2,512,128]{2,1,0:T(8,128)(2,1)S(1)}, bf16[2,512,128]{2,1,0:T(8,128)(2,1)S(1)}, u32[]{:S(2)}, u32[]{:S(2)}) collective-permute-start(bf16[2,512,128]{2,1,0:T(8,128)(2,1)S(1)} %get-tuple-element.71), channel_id=1, source_target_pairs={{0,12},{1,13},{2,14},{3,15},{4,0},{5,1},{6,2},{7,3},{8,4},{9,5},{1... | collective-permute-start | bytes 786440 | tf_op jit(solution)/shard_map/ppermute | solution.py:41
  59.0 3.9 %collective-permute-start.3 = (bf16[2,512,128]{2,1,0:T(8,128)(2,1)S(1)}, bf16[2,512,128]{2,1,0:T(8,128)(2,1)S(1)}, u32[]{:S(2)}, u32[]{:S(2)}) collective-permute-start(bf16[2,512,128]{2,1,0:T(8,128)(2,1)S(1)} %get-tuple-element.73), channel_id=1, source_target_pairs={{0,4},{1,5},{2,6},{3,7},{4,8},{5,9},{6,10},{7,11},{8,12},{9,13},{1... | collective-permute-start | bytes 786440 | tf_op jit(solution)/shard_map/ppermute | solution.py:41
  62.9 3.8 %collective-permute-start.4 = (bf16[2,512,128]{2,1,0:T(8,128)(2,1)S(1)}, bf16[2,512,128]{2,1,0:T(8,128)(2,1)S(1)}, u32[]{:S(2)}, u32[]{:S(2)}) collective-permute-start(bf16[2,512,128]{2,1,0:T(8,128)(2,1)S(1)} %get-tuple-element.74), channel_id=1, source_target_pairs={{0,8},{1,9},{2,10},{3,11},{4,12},{5,13},{6,14},{7,15},{8,0},{9,1},... | collective-permute-start | bytes 786440 | tf_op jit(solution)/shard_map/ppermute | solution.py:41
  66.8 29.1 %all_gather.3 = bf16[1024,256]{1,0:T(8,128)(2,1)S(1)} all-gather(bf16[64,256]{1,0:T(8,128)(2,1)S(1)} %fusion.145), channel_id=1, replica_groups=mesh['sp'=32,'tp'=16] {'tp'}, dimensions={0}, use_global_device_ids=true | all-gather | bytes 557056 | tf_op jit(solution)/shard_map/all_gather | solution.py:160
  97.4 4.7 %all-to-all-start.2 = ((bf16[32,32,128]{2,1,0:T(8,128)(2,1)}), bf16[32,32,128]{2,1,0:T(8,128)(2,1)S(1)}, u32[]{:S(2)}, u32[]{:S(2)}) async-start(bf16[32,32,128]{2,1,0:T(8,128)(2,1)} %bitcast.33), calls=%async_computation.2 | async-start | bytes 524288 | tf_op jit(solution)/shard_map/all_to_all | solution.py:27
  104.9 10.8 %all-to-all-done.2 = bf16[32,32,128]{2,1,0:T(8,128)(2,1)S(1)} async-done(((bf16[32,32,128]{2,1,0:T(8,128)(2,1)}), bf16[32,32,128]{2,1,0:T(8,128)(2,1)S(1)}, u32[]{:S(2)}, u32[]{:S(2)}) %all-to-all-start.2) | async-done | bytes 262176 | tf_op jit(solution)/shard_map/all_to_all | solution.py:27
  115.7 3.0 %collective-permute-start.8 = (bf16[1024,128]{1,0:T(8,128)(2,1)S(1)}, bf16[1024,128]{1,0:T(8,128)(2,1)S(1)}, u32[]{:S(2)}, u32[]{:S(2)}) collective-permute-start(bf16[1024,128]{1,0:T(8,128)(2,1)S(1)} %bitcast.173), channel_id=1, source_target_pairs={{0,14},{1,15},{2,0},{3,1},{4,2},{5,3},{6,4},{7,5},{8,6},{9,7},{10,... | collective-permute-start | bytes 786440 | tf_op jit(solution)/shard_map/ppermute | solution.py:41
  118.7 4.1 %collective-permute-start.7 = (bf16[1024,128]{1,0:T(8,128)(2,1)S(1)}, bf16[1024,128]{1,0:T(8,128)(2,1)S(1)}, u32[]{:S(2)}, u32[]{:S(2)}) collective-permute-start(bf16[1024,128]{1,0:T(8,128)(2,1)S(1)} %bitcast.174), channel_id=1, source_target_pairs={{0,2},{1,3},{2,4},{3,5},{4,6},{5,7},{6,8},{7,9},{8,10},{9,11},{10,... | collective-permute-start | bytes 786440 | tf_op jit(solution)/shard_map/ppermute | solution.py:41
  122.8 1.9 collective-permute-start.6
  127.0 1.9 collective-permute-start.9
  129.0 3.1 %collective-permute-start.11 = (bf16[1024,128]{1,0:T(8,128)(2,1)S(1)}, bf16[1024,128]{1,0:T(8,128)(2,1)S(1)}, u32[]{:S(2)}, u32[]{:S(2)}) collective-permute-start(bf16[1024,128]{1,0:T(8,128)(2,1)S(1)} %collective-permute-done.8), channel_id=1, source_target_pairs={{0,14},{1,15},{2,0},{3,1},{4,2},{5,3},{6,4},{7,5},{8,6},{9,7},{10,... | collective-permute-start | bytes 786440 | tf_op jit(solution)/shard_map/ppermute | solution.py:41
  132.1 4.1 %collective-permute-start.10 = (bf16[1024,128]{1,0:T(8,128)(2,1)S(1)}, bf16[1024,128]{1,0:T(8,128)(2,1)S(1)}, u32[]{:S(2)}, u32[]{:S(2)}) collective-permute-start(bf16[1024,128]{1,0:T(8,128)(2,1)S(1)} %collective-permute-done.7), channel_id=1, source_target_pairs={{0,2},{1,3},{2,4},{3,5},{4,6},{5,7},{6,8},{7,9},{8,10},{9,11},{10,... | collective-permute-start | bytes 786440 | tf_op jit(solution)/shard_map/ppermute | solution.py:41
  137.4 3.9 %collective-permute-done.11 = bf16[1024,128]{1,0:T(8,128)(2,1)S(1)} collective-permute-done((bf16[1024,128]{1,0:T(8,128)(2,1)S(1)}, bf16[1024,128]{1,0:T(8,128)(2,1)S(1)}, u32[]{:S(2)}, u32[]{:S(2)}) %collective-permute-start.11) | collective-permute-done | bytes 262176 | tf_op jit(solution)/shard_map/ppermute | solution.py:41
  141.3 1.4 collective-permute-done.10
  142.8 1.9 collective-permute-start.12
  144.7 3.6 %collective-permute-start.14 = (bf16[1024,128]{1,0:T(8,128)(2,1)S(1)}, bf16[1024,128]{1,0:T(8,128)(2,1)S(1)}, u32[]{:S(2)}, u32[]{:S(2)}) collective-permute-start(bf16[1024,128]{1,0:T(8,128)(2,1)S(1)} %collective-permute-done.11), channel_id=1, source_target_pairs={{0,14},{1,15},{2,0},{3,1},{4,2},{5,3},{6,4},{7,5},{8,6},{9,7},{10,... | collective-permute-start | bytes 786440 | tf_op jit(solution)/shard_map/ppermute | solution.py:41
  148.3 3.8 %collective-permute-start.13 = (bf16[1024,128]{1,0:T(8,128)(2,1)S(1)}, bf16[1024,128]{1,0:T(8,128)(2,1)S(1)}, u32[]{:S(2)}, u32[]{:S(2)}) collective-permute-start(bf16[1024,128]{1,0:T(8,128)(2,1)S(1)} %collective-permute-done.10), channel_id=1, source_target_pairs={{0,2},{1,3},{2,4},{3,5},{4,6},{5,7},{6,8},{7,9},{8,10},{9,11},{10,... | collective-permute-start | bytes 786440 | tf_op jit(solution)/shard_map/ppermute | solution.py:41
  152.6 4.4 %collective-permute-done.14 = bf16[1024,128]{1,0:T(8,128)(2,1)S(1)} collective-permute-done((bf16[1024,128]{1,0:T(8,128)(2,1)S(1)}, bf16[1024,128]{1,0:T(8,128)(2,1)S(1)}, u32[]{:S(2)}, u32[]{:S(2)}) %collective-permute-start.14) | collective-permute-done | bytes 262176 | tf_op jit(solution)/shard_map/ppermute | solution.py:41
  157.0 1.9 collective-permute-start.17
  159.0 5.1 %collective-permute-start.16 = (bf16[512,128]{1,0:T(8,128)(2,1)S(1)}, bf16[512,128]{1,0:T(8,128)(2,1)S(1)}, u32[]{:S(2)}, u32[]{:S(2)}) collective-permute-start(bf16[512,128]{1,0:T(8,128)(2,1)S(1)} %slice.184), channel_id=1, source_target_pairs={{0,2},{1,3},{2,4},{3,5},{4,6},{5,7},{6,8},{7,9},{8,10},{9,11},{10,... | collective-permute-start | bytes 393224 | tf_op jit(solution)/shard_map/ppermute | solution.py:41
  164.2 1.9 collective-permute-start.15
  167.7 2.4 collective-permute-start.18
  173.9 2.0 collective-permute-start.19
  176.0 1.8 collective-permute-done.19
  178.3 4.2 %collective-permute-start.20 = (bf16[512,128]{1,0:T(8,128)(2,1)S(1)}, bf16[512,128]{1,0:T(8,128)(2,1)S(1)}, u32[]{:S(2)}, u32[]{:S(2)}) collective-permute-start(bf16[512,128]{1,0:T(8,128)(2,1)S(1)} %get-tuple-element.85), channel_id=1, source_target_pairs={{0,2},{1,3},{2,4},{3,5},{4,6},{5,7},{6,8},{7,9},{8,10},{9,11},{10,... | collective-permute-start | bytes 393224 | tf_op jit(solution)/shard_map/ppermute | solution.py:41
  182.5 1.9 collective-permute-start.24
  185.8 5.6 %collective-permute-start.21 = (bf16[1024,128]{1,0:T(8,128)(2,1)S(1)}, bf16[1024,128]{1,0:T(8,128)(2,1)S(1)}, u32[]{:S(2)}, u32[]{:S(2)}) collective-permute-start(bf16[1024,128]{1,0:T(8,128)(2,1)S(1)} %fusion.78), channel_id=1, source_target_pairs={{0,2},{1,3},{2,4},{3,5},{4,6},{5,7},{6,8},{7,9},{8,10},{9,11},{10,... | collective-permute-start | bytes 786440 | tf_op jit(solution)/shard_map/ppermute | solution.py:41
  192.2 1.9 collective-permute-start.25
  194.2 2.4 %collective-permute-done.21 = bf16[1024,128]{1,0:T(8,128)(2,1)S(1)} collective-permute-done((bf16[1024,128]{1,0:T(8,128)(2,1)S(1)}, bf16[1024,128]{1,0:T(8,128)(2,1)S(1)}, u32[]{:S(2)}, u32[]{:S(2)}) %collective-permute-start.21) | collective-permute-done | bytes 262176 | tf_op jit(solution)/shard_map/ppermute | solution.py:41
  196.7 5.6 %collective-permute-start.22 = (bf16[1024,128]{1,0:T(8,128)(2,1)S(1)}, bf16[1024,128]{1,0:T(8,128)(2,1)S(1)}, u32[]{:S(2)}, u32[]{:S(2)}) collective-permute-start(bf16[1024,128]{1,0:T(8,128)(2,1)S(1)} %fusion.77), channel_id=1, source_target_pairs={{0,2},{1,3},{2,4},{3,5},{4,6},{5,7},{6,8},{7,9},{8,10},{9,11},{10,... | collective-permute-start | bytes 786440 | tf_op jit(solution)/shard_map/ppermute | solution.py:41
  202.9 2.1 collective-permute-start.26
  205.0 1.7 collective-permute-done.22
  206.7 5.6 %collective-permute-start.23 = (bf16[1024,128]{1,0:T(8,128)(2,1)S(1)}, bf16[1024,128]{1,0:T(8,128)(2,1)S(1)}, u32[]{:S(2)}, u32[]{:S(2)}) collective-permute-start(bf16[1024,128]{1,0:T(8,128)(2,1)S(1)} %fusion.76), channel_id=1, source_target_pairs={{0,2},{1,3},{2,4},{3,5},{4,6},{5,7},{6,8},{7,9},{8,10},{9,11},{10,... | collective-permute-start | bytes 786440 | tf_op jit(solution)/shard_map/ppermute | solution.py:41
  212.8 1.9 collective-permute-start.27
  214.7 1.5 collective-permute-done.23
  216.2 6.1 %collective-permute-done.27 = bf16[1024,128]{1,0:T(8,128)(2,1)S(1)} collective-permute-done((bf16[1024,128]{1,0:T(8,128)(2,1)S(1)}, bf16[1024,128]{1,0:T(8,128)(2,1)S(1)}, u32[]{:S(2)}, u32[]{:S(2)}) %collective-permute-start.27) | collective-permute-done | bytes 262176 | tf_op jit(solution)/shard_map/ppermute | solution.py:41
  223.1 4.8 %all-to-all-start.3 = ((bf16[32,32,128]{2,1,0:T(8,128)(2,1)}), bf16[32,32,128]{2,1,0:T(8,128)(2,1)S(1)}, u32[]{:S(2)}, u32[]{:S(2)}) async-start(bf16[32,32,128]{2,1,0:T(8,128)(2,1)} %bitcast.84), calls=%async_computation.3 | async-start | bytes 524288 | tf_op jit(solution)/shard_map/all_to_all | solution.py:27
  228.0 11.3 %all-to-all-done.3 = bf16[32,32,128]{2,1,0:T(8,128)(2,1)S(1)} async-done(((bf16[32,32,128]{2,1,0:T(8,128)(2,1)}), bf16[32,32,128]{2,1,0:T(8,128)(2,1)S(1)}, u32[]{:S(2)}, u32[]{:S(2)}) %all-to-all-start.3) | async-done | bytes 262176 | tf_op jit(solution)/shard_map/all_to_all | solution.py:27
  (140 shorter events, 28.4 us)
Async XLA Ops:
  0.0 96.0 %copy-start = (bf16[1024,128]{1,0:T(8,128)(2,1)S(1)}, bf16[1024,128]{1,0:T(8,128)(2,1)}, u32[]{:S(2)}) copy-start(bf16[1024,128]{1,0:T(8,128)(2,1)} %param.19) | copy-start | bytes 786436
  2.3 22.1 %copy-start.9 = (s32[256,2]{0,1:T(2,128)S(1)}, s32[256,2]{0,1:T(2,128)}, u32[]{:S(2)}) copy-start(s32[256,2]{0,1:T(2,128)} %param.22) | copy-start | bytes 6148
  2.4 23.5 %collective-permute-start = (bf16[256,96]{0,1:T(8,128)(2,1)S(1)}, bf16[256,96]{0,1:T(8,128)(2,1)S(1)}, u32[]{:S(2)}, u32[]{:S(2)}) collective-permute-start(bf16[256,96]{0,1:T(8,128)(2,1)S(1)} %get-tuple-element.114), channel_id=1, source_target_pairs={{0,16},{16,0},{32,48},{48,32},{64,80},{80,64},{96,112},{112,96},{1... | collective-permute-start | bytes 147464 | tf_op jit(solution)/shard_map/ppermute | solution.py:37
  7.0 47.7 %collective-permute-start.2 = (bf16[4,512,128]{2,1,0:T(8,128)(2,1)S(1)}, bf16[4,512,128]{2,1,0:T(8,128)(2,1)S(1)}, u32[]{:S(2)}, u32[]{:S(2)}) collective-permute-start(bf16[4,512,128]{2,1,0:T(8,128)(2,1)S(1)} %dynamic-slice_bitcast_fusion), channel_id=1, source_target_pairs={{0,2},{1,3},{2,0},{3,1},{4,6},{5,7},{6,4},{7,5},{8,10},{9,11},{10,... | collective-permute-start | bytes 1572872 | tf_op jit(solution)/shard_map/ppermute | solution.py:114
  14.0 30.1 %all-to-all-start = ((bf16[8,160,256]{2,1,0:T(8,128)(2,1)}), bf16[8,160,256]{2,1,0:T(8,128)(2,1)S(1)}, u32[]{:S(2)}, u32[]{:S(2)}) async-start(bf16[8,160,256]{2,1,0:T(8,128)(2,1)} %broadcast_in_dim.9), calls=%async_computation | async-start | bytes 1310720 | tf_op jit(solution)/shard_map/all_to_all | solution.py:27
  25.9 8.0 %collective-permute-start.1 = (bf16[2,256,96]{1,2,0:T(8,128)(2,1)S(1)}, bf16[2,256,96]{1,2,0:T(8,128)(2,1)S(1)}, u32[]{:S(2)}, u32[]{:S(2)}) collective-permute-start(bf16[2,256,96]{1,2,0:T(8,128)(2,1)S(1)} %pad_maximum_fusion.13), channel_id=1, source_target_pairs={{0,32},{16,48},{32,0},{48,16},{64,96},{80,112},{96,64},{112,80},{1... | collective-permute-start | bytes 294920 | tf_op jit(solution)/shard_map/ppermute | solution.py:37
  49.8 4.9 %copy-start.1 = (bf16[1,4096,128]{2,1,0:T(8,128)(2,1)S(1)}, bf16[1,4096,128]{2,1,0:T(8,128)(2,1)}, u32[]{:S(2)}) copy-start(bf16[1,4096,128]{2,1,0:T(8,128)(2,1)} %param.27) | copy-start | bytes 3145732
  50.7 16.0 %all-to-all-start.1 = ((f32[4,72,256]{2,1,0:T(8,128)}), f32[4,72,256]{2,1,0:T(8,128)S(1)}, u32[]{:S(2)}, u32[]{:S(2)}) async-start(f32[4,72,256]{2,1,0:T(8,128)} %pad_maximum_fusion.11), calls=%async_computation.1 | async-start | bytes 589824 | tf_op jit(solution)/shard_map/all_to_all | solution.py:27
  54.8 41.2 %copy-start.7 = (bf16[256,128]{1,0:T(8,128)(2,1)S(1)}, bf16[256,128]{1,0:T(8,128)(2,1)}, u32[]{:S(2)}) copy-start(bf16[256,128]{1,0:T(8,128)(2,1)} %param.20) | copy-start | bytes 196612
  54.9 42.5 %collective-permute-start.5 = (bf16[2,512,128]{2,1,0:T(8,128)(2,1)S(1)}, bf16[2,512,128]{2,1,0:T(8,128)(2,1)S(1)}, u32[]{:S(2)}, u32[]{:S(2)}) collective-permute-start(bf16[2,512,128]{2,1,0:T(8,128)(2,1)S(1)} %get-tuple-element.71), channel_id=1, source_target_pairs={{0,12},{1,13},{2,14},{3,15},{4,0},{5,1},{6,2},{7,3},{8,4},{9,5},{1... | collective-permute-start | bytes 786440 | tf_op jit(solution)/shard_map/ppermute | solution.py:41
  59.0 38.4 %collective-permute-start.3 = (bf16[2,512,128]{2,1,0:T(8,128)(2,1)S(1)}, bf16[2,512,128]{2,1,0:T(8,128)(2,1)S(1)}, u32[]{:S(2)}, u32[]{:S(2)}) collective-permute-start(bf16[2,512,128]{2,1,0:T(8,128)(2,1)S(1)} %get-tuple-element.73), channel_id=1, source_target_pairs={{0,4},{1,5},{2,6},{3,7},{4,8},{5,9},{6,10},{7,11},{8,12},{9,13},{1... | collective-permute-start | bytes 786440 | tf_op jit(solution)/shard_map/ppermute | solution.py:41
  62.9 34.5 %collective-permute-start.4 = (bf16[2,512,128]{2,1,0:T(8,128)(2,1)S(1)}, bf16[2,512,128]{2,1,0:T(8,128)(2,1)S(1)}, u32[]{:S(2)}, u32[]{:S(2)}) collective-permute-start(bf16[2,512,128]{2,1,0:T(8,128)(2,1)S(1)} %get-tuple-element.74), channel_id=1, source_target_pairs={{0,8},{1,9},{2,10},{3,11},{4,12},{5,13},{6,14},{7,15},{8,0},{9,1},... | collective-permute-start | bytes 786440 | tf_op jit(solution)/shard_map/ppermute | solution.py:41
  96.3 6.2 %copy-start.4 = (bf16[256,128]{1,0:T(8,128)(2,1)}, bf16[256,128]{1,0:T(8,128)(2,1)S(1)}, u32[]{:S(2)}) copy-start(bf16[256,128]{1,0:T(8,128)(2,1)S(1)} %fusion.10) | copy-start | bytes 196612
  97.4 18.3 %all-to-all-start.2 = ((bf16[32,32,128]{2,1,0:T(8,128)(2,1)}), bf16[32,32,128]{2,1,0:T(8,128)(2,1)S(1)}, u32[]{:S(2)}, u32[]{:S(2)}) async-start(bf16[32,32,128]{2,1,0:T(8,128)(2,1)} %bitcast.33), calls=%async_computation.2 | async-start | bytes 524288 | tf_op jit(solution)/shard_map/all_to_all | solution.py:27
  102.6 1.3 copy-start.2
  102.6 1.6 copy-start.3
  104.2 0.7 copy-start.10
  115.7 9.8 %collective-permute-start.8 = (bf16[1024,128]{1,0:T(8,128)(2,1)S(1)}, bf16[1024,128]{1,0:T(8,128)(2,1)S(1)}, u32[]{:S(2)}, u32[]{:S(2)}) collective-permute-start(bf16[1024,128]{1,0:T(8,128)(2,1)S(1)} %bitcast.173), channel_id=1, source_target_pairs={{0,14},{1,15},{2,0},{3,1},{4,2},{5,3},{6,4},{7,5},{8,6},{9,7},{10,... | collective-permute-start | bytes 786440 | tf_op jit(solution)/shard_map/ppermute | solution.py:41
  118.7 8.3 %collective-permute-start.7 = (bf16[1024,128]{1,0:T(8,128)(2,1)S(1)}, bf16[1024,128]{1,0:T(8,128)(2,1)S(1)}, u32[]{:S(2)}, u32[]{:S(2)}) collective-permute-start(bf16[1024,128]{1,0:T(8,128)(2,1)S(1)} %bitcast.174), channel_id=1, source_target_pairs={{0,2},{1,3},{2,4},{3,5},{4,6},{5,7},{6,8},{7,9},{8,10},{9,11},{10,... | collective-permute-start | bytes 786440 | tf_op jit(solution)/shard_map/ppermute | solution.py:41
  122.8 13.6 %collective-permute-start.6 = (bf16[1024,128]{1,0:T(8,128)(2,1)S(1)}, bf16[1024,128]{1,0:T(8,128)(2,1)S(1)}, u32[]{:S(2)}, u32[]{:S(2)}) collective-permute-start(bf16[1024,128]{1,0:T(8,128)(2,1)S(1)} %bitcast.175), channel_id=1, source_target_pairs={{0,1},{1,0},{2,3},{3,2},{4,5},{5,4},{6,7},{7,6},{8,9},{9,8},{10,11... | collective-permute-start | bytes 786440 | tf_op jit(solution)/shard_map/ppermute | solution.py:33
  127.0 39.5 %collective-permute-start.9 = (bf16[1024,256]{1,0:T(8,128)(2,1)S(1)}, bf16[1024,256]{1,0:T(8,128)(2,1)S(1)}, u32[]{:S(2)}, u32[]{:S(2)}) collective-permute-start(bf16[1024,256]{1,0:T(8,128)(2,1)S(1)} %pad_maximum_fusion.4), channel_id=1, source_target_pairs={{0,1},{1,0},{2,3},{3,2},{4,5},{5,4},{6,7},{7,6},{8,9},{9,8},{10,11... | collective-permute-start | bytes 1572872 | tf_op jit(solution)/shard_map/ppermute | solution.py:33
  129.0 12.3 %collective-permute-start.11 = (bf16[1024,128]{1,0:T(8,128)(2,1)S(1)}, bf16[1024,128]{1,0:T(8,128)(2,1)S(1)}, u32[]{:S(2)}, u32[]{:S(2)}) collective-permute-start(bf16[1024,128]{1,0:T(8,128)(2,1)S(1)} %collective-permute-done.8), channel_id=1, source_target_pairs={{0,14},{1,15},{2,0},{3,1},{4,2},{5,3},{6,4},{7,5},{8,6},{9,7},{10,... | collective-permute-start | bytes 786440 | tf_op jit(solution)/shard_map/ppermute | solution.py:41
  132.1 10.6 %collective-permute-start.10 = (bf16[1024,128]{1,0:T(8,128)(2,1)S(1)}, bf16[1024,128]{1,0:T(8,128)(2,1)S(1)}, u32[]{:S(2)}, u32[]{:S(2)}) collective-permute-start(bf16[1024,128]{1,0:T(8,128)(2,1)S(1)} %collective-permute-done.7), channel_id=1, source_target_pairs={{0,2},{1,3},{2,4},{3,5},{4,6},{5,7},{6,8},{7,9},{8,10},{9,11},{10,... | collective-permute-start | bytes 786440 | tf_op jit(solution)/shard_map/ppermute | solution.py:41
  142.8 27.6 %collective-permute-start.12 = (bf16[1024,256]{1,0:T(8,128)(2,1)S(1)}, bf16[1024,256]{1,0:T(8,128)(2,1)S(1)}, u32[]{:S(2)}, u32[]{:S(2)}) collective-permute-start(bf16[1024,256]{1,0:T(8,128)(2,1)S(1)} %pad_maximum_fusion.5), channel_id=1, source_target_pairs={{0,1},{1,0},{2,3},{3,2},{4,5},{5,4},{6,7},{7,6},{8,9},{9,8},{10,11... | collective-permute-start | bytes 1572872 | tf_op jit(solution)/shard_map/ppermute | solution.py:33
  144.7 12.3 %collective-permute-start.14 = (bf16[1024,128]{1,0:T(8,128)(2,1)S(1)}, bf16[1024,128]{1,0:T(8,128)(2,1)S(1)}, u32[]{:S(2)}, u32[]{:S(2)}) collective-permute-start(bf16[1024,128]{1,0:T(8,128)(2,1)S(1)} %collective-permute-done.11), channel_id=1, source_target_pairs={{0,14},{1,15},{2,0},{3,1},{4,2},{5,3},{6,4},{7,5},{8,6},{9,7},{10,... | collective-permute-start | bytes 786440 | tf_op jit(solution)/shard_map/ppermute | solution.py:41
  148.3 10.6 %collective-permute-start.13 = (bf16[1024,128]{1,0:T(8,128)(2,1)S(1)}, bf16[1024,128]{1,0:T(8,128)(2,1)S(1)}, u32[]{:S(2)}, u32[]{:S(2)}) collective-permute-start(bf16[1024,128]{1,0:T(8,128)(2,1)S(1)} %collective-permute-done.10), channel_id=1, source_target_pairs={{0,2},{1,3},{2,4},{3,5},{4,6},{5,7},{6,8},{7,9},{8,10},{9,11},{10,... | collective-permute-start | bytes 786440 | tf_op jit(solution)/shard_map/ppermute | solution.py:41
  157.0 10.7 %collective-permute-start.17 = (bf16[512,128]{1,0:T(8,128)(2,1)S(1)}, bf16[512,128]{1,0:T(8,128)(2,1)S(1)}, u32[]{:S(2)}, u32[]{:S(2)}) collective-permute-start(bf16[512,128]{1,0:T(8,128)(2,1)S(1)} %slice.185), channel_id=1, source_target_pairs={{0,14},{1,15},{2,0},{3,1},{4,2},{5,3},{6,4},{7,5},{8,6},{9,7},{10,... | collective-permute-start | bytes 393224 | tf_op jit(solution)/shard_map/ppermute | solution.py:41
  159.0 8.7 %collective-permute-start.16 = (bf16[512,128]{1,0:T(8,128)(2,1)S(1)}, bf16[512,128]{1,0:T(8,128)(2,1)S(1)}, u32[]{:S(2)}, u32[]{:S(2)}) collective-permute-start(bf16[512,128]{1,0:T(8,128)(2,1)S(1)} %slice.184), channel_id=1, source_target_pairs={{0,2},{1,3},{2,4},{3,5},{4,6},{5,7},{6,8},{7,9},{8,10},{9,11},{10,... | collective-permute-start | bytes 393224 | tf_op jit(solution)/shard_map/ppermute | solution.py:41
  164.2 7.6 %collective-permute-start.15 = (bf16[1024,256]{1,0:T(8,128)(2,1)S(1)}, bf16[1024,256]{1,0:T(8,128)(2,1)S(1)}, u32[]{:S(2)}, u32[]{:S(2)}) collective-permute-start(bf16[1024,256]{1,0:T(8,128)(2,1)S(1)} %pad_maximum_fusion.6), channel_id=1, source_target_pairs={{0,1},{1,0},{2,3},{3,2},{4,5},{5,4},{6,7},{7,6},{8,9},{9,8},{10,11... | collective-permute-start | bytes 1572872 | tf_op jit(solution)/shard_map/ppermute | solution.py:33
  167.7 3.8 %collective-permute-start.18 = (bf16[1024,128]{1,0:T(8,128)(2,1)S(1)}, bf16[1024,128]{1,0:T(8,128)(2,1)S(1)}, u32[]{:S(2)}, u32[]{:S(2)}) collective-permute-start(bf16[1024,128]{1,0:T(8,128)(2,1)S(1)} %constant_dynamic-update-slice_fusion), channel_id=1, source_target_pairs={{0,1},{1,0},{2,3},{3,2},{4,5},{5,4},{6,7},{7,6},{8,9},{9,8},{10,11... | collective-permute-start | bytes 786440 | tf_op jit(solution)/shard_map/ppermute | solution.py:33
  173.6 4.1 %copy-start.6 = (bf16[512,128]{1,0:T(8,128)(2,1)S(1)}, bf16[512,128]{1,0:T(8,128)(2,1)}, u32[]{:S(2)}) copy-start(bf16[512,128]{1,0:T(8,128)(2,1)} %get-tuple-element.35) | copy-start | bytes 393220
  173.9 3.8 %collective-permute-start.19 = (bf16[1024,256]{0,1:T(8,128)(2,1)S(1)}, bf16[1024,256]{0,1:T(8,128)(2,1)S(1)}, u32[]{:S(2)}, u32[]{:S(2)}) collective-permute-start(bf16[1024,256]{0,1:T(8,128)(2,1)S(1)} %fusion.13), channel_id=1, source_target_pairs={{0,1},{1,0},{2,3},{3,2},{4,5},{5,4},{6,7},{7,6},{8,9},{9,8},{10,11... | collective-permute-start | bytes 1572872 | tf_op jit(solution)/shard_map/ppermute | solution.py:33
  178.3 7.5 %collective-permute-start.20 = (bf16[512,128]{1,0:T(8,128)(2,1)S(1)}, bf16[512,128]{1,0:T(8,128)(2,1)S(1)}, u32[]{:S(2)}, u32[]{:S(2)}) collective-permute-start(bf16[512,128]{1,0:T(8,128)(2,1)S(1)} %get-tuple-element.85), channel_id=1, source_target_pairs={{0,2},{1,3},{2,4},{3,5},{4,6},{5,7},{6,8},{7,9},{8,10},{9,11},{10,... | collective-permute-start | bytes 393224 | tf_op jit(solution)/shard_map/ppermute | solution.py:41
  182.5 9.7 %collective-permute-start.24 = (bf16[512,128]{1,0:T(8,128)(2,1)S(1)}, bf16[512,128]{1,0:T(8,128)(2,1)S(1)}, u32[]{:S(2)}, u32[]{:S(2)}) collective-permute-start(bf16[512,128]{1,0:T(8,128)(2,1)S(1)} %get-tuple-element.86), channel_id=1, source_target_pairs={{0,14},{1,15},{2,0},{3,1},{4,2},{5,3},{6,4},{7,5},{8,6},{9,7},{10,... | collective-permute-start | bytes 393224 | tf_op jit(solution)/shard_map/ppermute | solution.py:41
  185.8 10.8 %collective-permute-start.21 = (bf16[1024,128]{1,0:T(8,128)(2,1)S(1)}, bf16[1024,128]{1,0:T(8,128)(2,1)S(1)}, u32[]{:S(2)}, u32[]{:S(2)}) collective-permute-start(bf16[1024,128]{1,0:T(8,128)(2,1)S(1)} %fusion.78), channel_id=1, source_target_pairs={{0,2},{1,3},{2,4},{3,5},{4,6},{5,7},{6,8},{7,9},{8,10},{9,11},{10,... | collective-permute-start | bytes 786440 | tf_op jit(solution)/shard_map/ppermute | solution.py:41
  192.2 10.5 %collective-permute-start.25 = (bf16[1024,128]{1,0:T(8,128)(2,1)S(1)}, bf16[1024,128]{1,0:T(8,128)(2,1)S(1)}, u32[]{:S(2)}, u32[]{:S(2)}) collective-permute-start(bf16[1024,128]{1,0:T(8,128)(2,1)S(1)} %fusion.75), channel_id=1, source_target_pairs={{0,14},{1,15},{2,0},{3,1},{4,2},{5,3},{6,4},{7,5},{8,6},{9,7},{10,... | collective-permute-start | bytes 786440 | tf_op jit(solution)/shard_map/ppermute | solution.py:41
  196.7 10.0 %collective-permute-start.22 = (bf16[1024,128]{1,0:T(8,128)(2,1)S(1)}, bf16[1024,128]{1,0:T(8,128)(2,1)S(1)}, u32[]{:S(2)}, u32[]{:S(2)}) collective-permute-start(bf16[1024,128]{1,0:T(8,128)(2,1)S(1)} %fusion.77), channel_id=1, source_target_pairs={{0,2},{1,3},{2,4},{3,5},{4,6},{5,7},{6,8},{7,9},{8,10},{9,11},{10,... | collective-permute-start | bytes 786440 | tf_op jit(solution)/shard_map/ppermute | solution.py:41
  202.9 25.1 %copy-start.8 = (f32[256,2]{0,1:T(2,128)S(1)}, f32[256,2]{0,1:T(2,128)}, u32[]{:S(2)}) copy-start(f32[256,2]{0,1:T(2,128)} %param.23) | copy-start | bytes 6148
  202.9 25.1 %copy-start.11 = (f32[256]{0:T(256)S(1)}, f32[256]{0:T(256)}, u32[]{:S(2)}) copy-start(f32[256]{0:T(256)} %param.24) | copy-start | bytes 3076
  202.9 36.4 %copy-start.5 = (bf16[256,128]{1,0:T(8,128)(2,1)S(1)}, bf16[256,128]{1,0:T(8,128)(2,1)}, u32[]{:S(2)}) copy-start(bf16[256,128]{1,0:T(8,128)(2,1)} %copy-done.4) | copy-start | bytes 196612
  202.9 9.8 %collective-permute-start.26 = (bf16[1024,128]{1,0:T(8,128)(2,1)S(1)}, bf16[1024,128]{1,0:T(8,128)(2,1)S(1)}, u32[]{:S(2)}, u32[]{:S(2)}) collective-permute-start(bf16[1024,128]{1,0:T(8,128)(2,1)S(1)} %fusion.74), channel_id=1, source_target_pairs={{0,14},{1,15},{2,0},{3,1},{4,2},{5,3},{6,4},{7,5},{8,6},{9,7},{10,... | collective-permute-start | bytes 786440 | tf_op jit(solution)/shard_map/ppermute | solution.py:41
  206.7 9.5 %collective-permute-start.23 = (bf16[1024,128]{1,0:T(8,128)(2,1)S(1)}, bf16[1024,128]{1,0:T(8,128)(2,1)S(1)}, u32[]{:S(2)}, u32[]{:S(2)}) collective-permute-start(bf16[1024,128]{1,0:T(8,128)(2,1)S(1)} %fusion.76), channel_id=1, source_target_pairs={{0,2},{1,3},{2,4},{3,5},{4,6},{5,7},{6,8},{7,9},{8,10},{9,11},{10,... | collective-permute-start | bytes 786440 | tf_op jit(solution)/shard_map/ppermute | solution.py:41
  212.8 9.5 %collective-permute-start.27 = (bf16[1024,128]{1,0:T(8,128)(2,1)S(1)}, bf16[1024,128]{1,0:T(8,128)(2,1)S(1)}, u32[]{:S(2)}, u32[]{:S(2)}) collective-permute-start(bf16[1024,128]{1,0:T(8,128)(2,1)S(1)} %fusion.73), channel_id=1, source_target_pairs={{0,14},{1,15},{2,0},{3,1},{4,2},{5,3},{6,4},{7,5},{8,6},{9,7},{10,... | collective-permute-start | bytes 786440 | tf_op jit(solution)/shard_map/ppermute | solution.py:41
  223.1 16.2 %all-to-all-start.3 = ((bf16[32,32,128]{2,1,0:T(8,128)(2,1)}), bf16[32,32,128]{2,1,0:T(8,128)(2,1)S(1)}, u32[]{:S(2)}, u32[]{:S(2)}) async-start(bf16[32,32,128]{2,1,0:T(8,128)(2,1)} %bitcast.84), calls=%async_computation.3 | async-start | bytes 524288 | tf_op jit(solution)/shard_map/all_to_all | solution.py:27

commit v4 on v3

--- a/solution.py
+++ b/solution.py
@@ -112,7 +112,8 @@
     parity = lambda one: lax.dynamic_index_in_dim(down, one, 1, keepdims=False)
     kept = parity(odd)
     got = lax.ppermute(parity(1 - odd), "tp", [(t, t ^ 2) for t in range(TP)])
-    both = jnp.stack([jnp.where(odd == 0, kept, got), jnp.where(odd == 0, got, kept)], axis=1)
+    both = [jnp.where(odd == 0, kept, got), jnp.where(odd == 0, got, kept)]
+    both = jnp.concatenate(both, axis=2)
     down = [at(both, y // 2)]
     for by in (1, 2, 3):
         down.append(y_step(at(both, (y // 2 + by) % (Y // 2)), 2 * by))
@@ -164,27 +165,16 @@
     mixed = (residual.astype(f32) + projected).astype(bf16)
 
     sent = lax.dot_general(placed, mixed, (((0,), (0,)), ((), ())), preferred_element_type=f32)
-    sent, gate_weight, up_weight, ffn_gain, down = lax.optimization_barrier(
-        (sent.astype(bf16), gate_weight, up_weight, ffn_gain, down)
+    sent, gate_weight, up_weight, ffn_gain = lax.optimization_barrier(
+        (sent.astype(bf16), gate_weight, up_weight, ffn_gain)
     )
     arrived = exchange(sent.reshape(SP, capacity, width), "sp")
     gate_up_weight = jnp.concatenate(
         [gate_weight.reshape(TP, width, ff), up_weight.reshape(TP, width, ff)], axis=2
     )
     gains = ffn_gain.astype(f32).reshape(TP, width)
-    down = jnp.stack(down).reshape(Y, 2, ff, width)
-    down = jnp.where(core == 0, down, down[:, ::-1]).reshape(Y, 2 * ff, width)
-
-    def features(steps):
-        parts = []
-        for k in steps:
-            chip = (y + k) % Y
-            parts.append(at(down, (y // 2 - chip // 2) % (Y // 2) * 2 + chip % 2))
-        return jnp.concatenate(parts, axis=1)
-
-    down_first, down_above, down_below = features([4]), features([3, 2, 1]), features([-3, -2, -1, 0])
-    arrived, gate_up_weight, gains, down_first, down_above, down_below = lax.optimization_barrier(
-        (arrived.reshape(slots, width), gate_up_weight, gains, down_first, down_above, down_below)
+    arrived, gate_up_weight, gains = lax.optimization_barrier(
+        (arrived.reshape(slots, width), gate_up_weight, gains)
     )
 
     def products(parts):
@@ -202,45 +192,61 @@
         )
         return product, squares
 
-    half = slots // 2
-
     def ring(above, below):
         above = y_step(above, 1)
         below = y_step(below, -1)
         return above, below
 
     above = below = arrived
+    opposite = y_step(arrived, 4)
     gate_up, squares = products([(arrived, y, core), (swap(arrived), y, 1 - core)])
     for k in range(1, 4):
         above, below = ring(above, below)
-        crossed = swap(jnp.concatenate([above, below], axis=1))
-        more, more_squares = products(
-            [
-                (above, y - k, core),
-                (below, y + k, core),
-                (crossed[:, :width], y - k, 1 - core),
-                (crossed[:, width:], y + k, 1 - core),
-            ]
-        )
-        gate_up, squares = gate_up + more, squares + more_squares
-    last = jnp.concatenate(ring(above[:half], below[half:]), axis=0)
-    more, more_squares = products([(last, y + 4, core), (swap(last), y + 4, 1 - core)])
-    gate_up, squares = gate_up + more, squares + more_squares
+        blocks = [(above, y - k), (below, y + k)]
+        if k == 3:
+            above, below, opposite = lax.optimization_barrier((above, below, opposite))
+            blocks = [(above, y - k), (below, y + k), (opposite, y + 4)]
+        crossed = swap(jnp.concatenate([rows for rows, _ in blocks], axis=1))
+        parts = [(rows, chip, core) for rows, chip in blocks]
+        for i, (_, chip) in enumerate(blocks):
+            parts.append((crossed[:, i * width : (i + 1) * width], chip, 1 - core))
+        count = len(blocks)
+        for group in ((0, 1, count, count + 1), (2, 5))[: count - 1]:
+            more, more_squares = products([parts[i] for i in group])
+            gate_up, squares = gate_up + more, squares + more_squares
     gate_up = gate_up * lax.rsqrt(squares / D + EPSILON)
     hidden = (jax.nn.silu(gate_up[:, :ff]) * gate_up[:, ff:]).astype(bf16)
 
-    hidden = jnp.concatenate([hidden, swap(hidden)], axis=1)
-    first = jnp.dot(hidden, down_first, preferred_element_type=f32).astype(bf16)
-    part_above = lax.optimization_barrier(jnp.dot(hidden, down_above, preferred_element_type=f32))
-    part_below = lax.optimization_barrier(jnp.dot(hidden, down_below, preferred_element_type=f32))
-    column = lambda a, i: a[:, i * width : (i + 1) * width]
-    nothing = jnp.zeros((half, width), bf16)
-    above = jnp.concatenate([y_step(first[:half], 1), nothing], axis=0)
-    below = jnp.concatenate([nothing, y_step(first[half:], -1)], axis=0)
-    for i in range(3):
-        above = y_step((above.astype(f32) + column(part_above, i)).astype(bf16), 1)
-        below = y_step((below.astype(f32) + column(part_below, i)).astype(bf16), -1)
-    expert_out = column(part_below, 3) + above.astype(f32) + below.astype(f32)
+    other = swap(hidden)
+    hidden = jnp.where(
+        core == 0,
+        jnp.concatenate([hidden, other], axis=1),
+        jnp.concatenate([other, hidden], axis=1),
+    )
+    pairs = [
+        lax.optimization_barrier(jnp.dot(hidden, one, preferred_element_type=f32)) for one in down
+    ]
+
+    def term(by):
+        for r in range(Y // 2):
+            for h in range(2):
+                columns = pairs[r][:, h * width : (h + 1) * width]
+                if (h - 2 * r - by) % Y == 0:
+                    even_part = columns
+                if (h - 2 * r - 1 - by) % Y == 0:
+                    odd_part = columns
+        return jnp.where(odd == 0, even_part, odd_part)
+
+    above, below = term(3).astype(bf16), term(-3).astype(bf16)
+    for k in (2, 1, 0):
+        above = y_step(above, 1)
+        below = y_step(below, -1)
+        if k == 2:
+            opposite = y_step(term(4).astype(bf16), 4)
+        if k > 0:
+            above = (above.astype(f32) + term(k)).astype(bf16)
+            below = (below.astype(f32) + term(-k)).astype(bf16)
+    expert_out = term(0) + above.astype(f32) + below.astype(f32) + opposite.astype(f32)
     expert_out = expert_out.astype(bf16).reshape(SP, capacity, width)
 
     returned = exchange(expert_out, "sp").reshape(slots, width)

time: 242 us -> 253 us (1.045)
  the two profiles are of different devices: /device:TPU:56 before, /device:TPU:1 now
where the time goes in v4:
time: 253 us; the launch traced here: 251 us
  starting transfers between devices  115 us (45%)
  waiting for transfers between devices  74 us (29%)
  blocking collectives  20.8 us (8%)
  matrix products  19.3 us (8%)
  other arithmetic  18.5 us (7%)
    ppermute x17, starting transfers between devices, y_step(): lax.ppermute(value, 'tp', [(t, (t + 2 * by) % TP) for t in range(TP)])  58.7 us
    all_to_all x4, waiting for transfers between devices, exchange(): lax.all_to_all(value, axis, split_axis=0, concat_axis=0, tiled=True, axis...  38 us
    ppermute x17, waiting for transfers between devices, y_step(): lax.ppermute(value, 'tp', [(t, (t + 2 * by) % TP) for t in range(TP)])  33.2 us
    ppermute x5, starting transfers between devices, swap(): return lax.ppermute(value, 'tp', [(t, t ^ 1) for t in range(TP)])  23.1 us
    all_to_all x4, starting transfers between devices, exchange(): lax.all_to_all(value, axis, split_axis=0, concat_axis=0, tiled=True, axis...  22.8 us
    all_gather x1, blocking collectives, body(): attended_all = lax.all_gather(attended, 'tp', axis=0, tiled=True)  20.8 us
    ppermute x2, starting transfers between devices, x_swap(): return lax.ppermute(value, 'sp', [(s, s ^ bit) for s in range(SP)])  8.3 us
    dot_general x4, matrix products, body(): jnp.dot(hidden, one, preferred_element_type=f32)  8.11 us
  transfers between devices with their start and end apart: 29, of which 12 were waited for; matrix products, arithmetic and copies ran while one was open for 10% of the time, Pallas kernels for 0%

profile of v4, /device:TPU:1, one launch (start us, length us, event | category | flops | bytes accessed | tf_op | source)
XLA Modules:
  0.0 251.0 jit_solution(2834353098663075287)
XLA Ops:
  2.4 3.9 %collective-permute-start = (bf16[256,96]{0,1:T(8,128)(2,1)S(1)}, bf16[256,96]{0,1:T(8,128)(2,1)S(1)}, u32[]{:S(2)}, u32[]{:S(2)}) collective-permute-start(bf16[256,96]{0,1:T(8,128)(2,1)S(1)} %get-tuple-element.100), channel_id=1, source_target_pairs={{0,16},{16,0},{32,48},{48,32},{64,80},{80,64},{96,112},{112,96},{1... | collective-permute-start | bytes 147464 | tf_op jit(solution)/shard_map/ppermute | solution.py:37
  10.2 10.0 %all-to-all-start = ((bf16[8,160,256]{2,1,0:T(8,128)(2,1)}), bf16[8,160,256]{2,1,0:T(8,128)(2,1)S(1)}, u32[]{:S(2)}, u32[]{:S(2)}) async-start(bf16[8,160,256]{2,1,0:T(8,128)(2,1)} %broadcast_in_dim.9), calls=%async_computation | async-start | bytes 1310720 | tf_op jit(solution)/shard_map/all_to_all | solution.py:27
  20.8 4.4 %collective-permute-start.1 = (bf16[2,256,96]{1,2,0:T(8,128)(2,1)S(1)}, bf16[2,256,96]{1,2,0:T(8,128)(2,1)S(1)}, u32[]{:S(2)}, u32[]{:S(2)}) collective-permute-start(bf16[2,256,96]{1,2,0:T(8,128)(2,1)S(1)} %pad_maximum_fusion.6), channel_id=1, source_target_pairs={{0,32},{16,48},{32,0},{48,16},{64,96},{80,112},{96,64},{112,80},{1... | collective-permute-start | bytes 294920 | tf_op jit(solution)/shard_map/ppermute | solution.py:37
  25.1 2.8 %collective-permute-done.1 = bf16[2,256,96]{1,2,0:T(8,128)(2,1)S(1)} collective-permute-done((bf16[2,256,96]{1,2,0:T(8,128)(2,1)S(1)}, bf16[2,256,96]{1,2,0:T(8,128)(2,1)S(1)}, u32[]{:S(2)}, u32[]{:S(2)}) %collective-permute-start.1) | collective-permute-done | bytes 98336 | tf_op jit(solution)/shard_map/ppermute | solution.py:37
  28.0 13.0 %all-to-all-done = bf16[8,160,256]{2,1,0:T(8,128)(2,1)S(1)} async-done(((bf16[8,160,256]{2,1,0:T(8,128)(2,1)}), bf16[8,160,256]{2,1,0:T(8,128)(2,1)S(1)}, u32[]{:S(2)}, u32[]{:S(2)}) %all-to-all-start) | async-done | bytes 655392 | tf_op jit(solution)/shard_map/all_to_all | solution.py:27
  42.5 2.1 fusion
  44.6 2.2 fusion.5
  47.6 3.8 %all-to-all-start.1 = ((f32[4,72,256]{2,1,0:T(8,128)}), f32[4,72,256]{2,1,0:T(8,128)S(1)}, u32[]{:S(2)}, u32[]{:S(2)}) async-start(f32[4,72,256]{2,1,0:T(8,128)} %pad_maximum_fusion.4), calls=%async_computation.1 | async-start | bytes 589824 | tf_op jit(solution)/shard_map/all_to_all | solution.py:27
  51.7 5.8 %all-to-all-done.1 = f32[4,72,256]{2,1,0:T(8,128)S(1)} async-done(((f32[4,72,256]{2,1,0:T(8,128)}), f32[4,72,256]{2,1,0:T(8,128)S(1)}, u32[]{:S(2)}, u32[]{:S(2)}) %all-to-all-start.1) | async-done | bytes 294944 | tf_op jit(solution)/shard_map/all_to_all | solution.py:27
  57.6 20.8 %all_gather.3 = bf16[1024,256]{1,0:T(8,128)(2,1)S(1)} all-gather(bf16[64,256]{1,0:T(8,128)(2,1)S(1)} %fusion.135), channel_id=1, replica_groups=mesh['sp'=32,'tp'=16] {'tp'}, dimensions={0}, use_global_device_ids=true | all-gather | bytes 557056 | tf_op jit(solution)/shard_map/all_gather | solution.py:161
  79.8 3.9 %all-to-all-start.2 = ((bf16[32,32,128]{2,1,0:T(8,128)(2,1)}), bf16[32,32,128]{2,1,0:T(8,128)(2,1)S(1)}, u32[]{:S(2)}, u32[]{:S(2)}) async-start(bf16[32,32,128]{2,1,0:T(8,128)(2,1)} %bitcast.24), calls=%async_computation.2 | async-start | bytes 524288 | tf_op jit(solution)/shard_map/all_to_all | solution.py:27
  83.8 1.9 collective-permute-start.14
  87.8 8.0 %all-to-all-done.2 = bf16[32,32,128]{2,1,0:T(8,128)(2,1)S(1)} async-done(((bf16[32,32,128]{2,1,0:T(8,128)(2,1)}), bf16[32,32,128]{2,1,0:T(8,128)(2,1)S(1)}, u32[]{:S(2)}, u32[]{:S(2)}) %all-to-all-start.2) | async-done | bytes 262176 | tf_op jit(solution)/shard_map/all_to_all | solution.py:27
  95.8 2.4 collective-permute-start.4
  98.2 2.8 %collective-permute-start.3 = (bf16[1024,128]{1,0:T(8,128)(2,1)S(1)}, bf16[1024,128]{1,0:T(8,128)(2,1)S(1)}, u32[]{:S(2)}, u32[]{:S(2)}) collective-permute-start(bf16[1024,128]{1,0:T(8,128)(2,1)S(1)} %bitcast.143), channel_id=1, source_target_pairs={{0,2},{1,3},{2,4},{3,5},{4,6},{5,7},{6,8},{7,9},{8,10},{9,11},{10,... | collective-permute-start | bytes 786440 | tf_op jit(solution)/shard_map/ppermute | solution.py:41
  101.1 4.7 %collective-permute-start.11 = (bf16[1024,128]{1,0:T(8,128)(2,1)S(1)}, bf16[1024,128]{1,0:T(8,128)(2,1)S(1)}, u32[]{:S(2)}, u32[]{:S(2)}) collective-permute-start(bf16[1024,128]{1,0:T(8,128)(2,1)S(1)} %bitcast.144), channel_id=1, source_target_pairs={{0,8},{1,9},{2,10},{3,11},{4,12},{5,13},{6,14},{7,15},{8,0},{9,1},... | collective-permute-start | bytes 786440 | tf_op jit(solution)/shard_map/ppermute | solution.py:41
  105.8 4.6 %collective-permute-start.2 = (bf16[1024,128]{1,0:T(8,128)(2,1)S(1)}, bf16[1024,128]{1,0:T(8,128)(2,1)S(1)}, u32[]{:S(2)}, u32[]{:S(2)}) collective-permute-start(bf16[1024,128]{1,0:T(8,128)(2,1)S(1)} %bitcast.145), channel_id=1, source_target_pairs={{0,1},{1,0},{2,3},{3,2},{4,5},{5,4},{6,7},{7,6},{8,9},{9,8},{10,11... | collective-permute-start | bytes 786440 | tf_op jit(solution)/shard_map/ppermute | solution.py:33
  111.0 9.5 %collective-permute-start.5 = (bf16[1024,256]{1,0:T(8,128)(2,1)S(1)}, bf16[1024,256]{1,0:T(8,128)(2,1)S(1)}, u32[]{:S(2)}, u32[]{:S(2)}) collective-permute-start(bf16[1024,256]{1,0:T(8,128)(2,1)S(1)} %pad_maximum_fusion.2), channel_id=1, source_target_pairs={{0,1},{1,0},{2,3},{3,2},{4,5},{5,4},{6,7},{7,6},{8,9},{9,8},{10,11... | collective-permute-start | bytes 1572872 | tf_op jit(solution)/shard_map/ppermute | solution.py:33
  120.5 1.9 collective-permute-start.7
  122.7 3.4 %collective-permute-start.6 = (bf16[1024,128]{1,0:T(8,128)(2,1)S(1)}, bf16[1024,128]{1,0:T(8,128)(2,1)S(1)}, u32[]{:S(2)}, u32[]{:S(2)}) collective-permute-start(bf16[1024,128]{1,0:T(8,128)(2,1)S(1)} %collective-permute-done.3), channel_id=1, source_target_pairs={{0,2},{1,3},{2,4},{3,5},{4,6},{5,7},{6,8},{7,9},{8,10},{9,11},{10,... | collective-permute-start | bytes 786440 | tf_op jit(solution)/shard_map/ppermute | solution.py:41
  126.9 3.3 %collective-permute-done.7 = bf16[1024,128]{1,0:T(8,128)(2,1)S(1)} collective-permute-done((bf16[1024,128]{1,0:T(8,128)(2,1)S(1)}, bf16[1024,128]{1,0:T(8,128)(2,1)S(1)}, u32[]{:S(2)}, u32[]{:S(2)}) %collective-permute-start.7) | collective-permute-done | bytes 262176 | tf_op jit(solution)/shard_map/ppermute | solution.py:41
  130.2 3.4 %collective-permute-start.10 = (bf16[1024,128]{1,0:T(8,128)(2,1)S(1)}, bf16[1024,128]{1,0:T(8,128)(2,1)S(1)}, u32[]{:S(2)}, u32[]{:S(2)}) collective-permute-start(bf16[1024,128]{1,0:T(8,128)(2,1)S(1)} %collective-permute-done.7), channel_id=1, source_target_pairs={{0,14},{1,15},{2,0},{3,1},{4,2},{5,3},{6,4},{7,5},{8,6},{9,7},{10,... | collective-permute-start | bytes 786440 | tf_op jit(solution)/shard_map/ppermute | solution.py:41
  133.7 1.9 collective-permute-start.9
  136.1 3.3 %collective-permute-start.8 = (bf16[1024,256]{1,0:T(8,128)(2,1)S(1)}, bf16[1024,256]{1,0:T(8,128)(2,1)S(1)}, u32[]{:S(2)}, u32[]{:S(2)}) collective-permute-start(bf16[1024,256]{1,0:T(8,128)(2,1)S(1)} %pad_maximum_fusion.3), channel_id=1, source_target_pairs={{0,1},{1,0},{2,3},{3,2},{4,5},{5,4},{6,7},{7,6},{8,9},{9,8},{10,11... | collective-permute-start | bytes 1572872 | tf_op jit(solution)/shard_map/ppermute | solution.py:33
  139.4 4.3 %collective-permute-done.9 = bf16[1024,128]{1,0:T(8,128)(2,1)S(1)} collective-permute-done((bf16[1024,128]{1,0:T(8,128)(2,1)S(1)}, bf16[1024,128]{1,0:T(8,128)(2,1)S(1)}, u32[]{:S(2)}, u32[]{:S(2)}) %collective-permute-start.9) | collective-permute-done | bytes 262176 | tf_op jit(solution)/shard_map/ppermute | solution.py:41
  143.9 3.8 %collective-permute-start.12 = (bf16[1024,384]{1,0:T(8,128)(2,1)S(1)}, bf16[1024,384]{1,0:T(8,128)(2,1)S(1)}, u32[]{:S(2)}, u32[]{:S(2)}) collective-permute-start(bf16[1024,384]{1,0:T(8,128)(2,1)S(1)} %pad_maximum_fusion.1), channel_id=1, source_target_pairs={{0,1},{1,0},{2,3},{3,2},{4,5},{5,4},{6,7},{7,6},{8,9},{9,8},{10,11... | collective-permute-start | bytes 2359304 | tf_op jit(solution)/shard_map/ppermute | solution.py:33
  152.8 1.9 collective-permute-start.13
  156.8 1.9 collective-permute-start.20
  158.7 5.5 %collective-permute-start.15 = (bf16[512,256]{1,0:T(8,128)(2,1)S(1)}, bf16[512,256]{1,0:T(8,128)(2,1)}, u32[]{:S(2)}, u32[]{:S(2)}) collective-permute-start(bf16[512,256]{1,0:T(8,128)(2,1)S(1)} %get-tuple-element.58), channel_id=1, source_target_pairs={{0,12},{1,13},{2,14},{3,15},{4,0},{5,1},{6,2},{7,3},{8,4},{9,5},{1... | collective-permute-start | bytes 786440 | tf_op jit(solution)/shard_map/ppermute | solution.py:41
  164.2 6.3 %collective-permute-start.16 = (bf16[512,256]{1,0:T(8,128)(2,1)}, bf16[512,256]{1,0:T(8,128)(2,1)S(1)}, u32[]{:S(2)}, u32[]{:S(2)}) collective-permute-start(bf16[512,256]{1,0:T(8,128)(2,1)} %get-tuple-element.59), channel_id=1, source_target_pairs={{0,8},{1,9},{2,10},{3,11},{4,12},{5,13},{6,14},{7,15},{8,0},{9,1},... | collective-permute-start | bytes 786440 | tf_op jit(solution)/shard_map/ppermute | solution.py:41
  170.5 2.6 %collective-permute-done.20 = bf16[512,256]{1,0:T(8,128)(2,1)S(1)} collective-permute-done((bf16[512,256]{1,0:T(8,128)(2,1)S(1)}, bf16[512,256]{1,0:T(8,128)(2,1)S(1)}, u32[]{:S(2)}, u32[]{:S(2)}) %collective-permute-start.20) | collective-permute-done | bytes 262176 | tf_op jit(solution)/shard_map/ppermute | solution.py:41
  173.1 1.8 fusion.187
  174.9 7.9 %collective-permute-done.15 = bf16[512,256]{1,0:T(8,128)(2,1)} collective-permute-done((bf16[512,256]{1,0:T(8,128)(2,1)S(1)}, bf16[512,256]{1,0:T(8,128)(2,1)}, u32[]{:S(2)}, u32[]{:S(2)}) %collective-permute-start.15) | collective-permute-done | bytes 262176 | tf_op jit(solution)/shard_map/ppermute | solution.py:41
  182.7 2.3 fusion.189
  185.1 1.8 fusion.188
  187.7 1.9 collective-permute-start.21
  189.6 6.8 %collective-permute-start.17 = (bf16[1024,128]{1,0:T(8,128)(2,1)S(1)}, bf16[1024,128]{1,0:T(8,128)(2,1)S(1)}, u32[]{:S(2)}, u32[]{:S(2)}) collective-permute-start(bf16[1024,128]{1,0:T(8,128)(2,1)S(1)} %get-tuple-element.64), channel_id=1, source_target_pairs={{0,2},{1,3},{2,4},{3,5},{4,6},{5,7},{6,8},{7,9},{8,10},{9,11},{10,... | collective-permute-start | bytes 786440 | tf_op jit(solution)/shard_map/ppermute | solution.py:41
  196.4 3.1 %collective-permute-done.21 = bf16[1024,128]{1,0:T(8,128)(2,1)S(1)} collective-permute-done((bf16[1024,128]{1,0:T(8,128)(2,1)S(1)}, bf16[1024,128]{1,0:T(8,128)(2,1)S(1)}, u32[]{:S(2)}, u32[]{:S(2)}) %collective-permute-start.21) | collective-permute-done | bytes 262176 | tf_op jit(solution)/shard_map/ppermute | solution.py:41
  200.3 1.9 collective-permute-start.22
  203.0 3.4 %collective-permute-start.18 = (bf16[1024,128]{1,0:T(8,128)(2,1)}, bf16[1024,128]{1,0:T(8,128)(2,1)}, u32[]{:S(2)}, u32[]{:S(2)}) collective-permute-start(bf16[1024,128]{1,0:T(8,128)(2,1)} %add_convert_fusion.4), channel_id=1, source_target_pairs={{0,2},{1,3},{2,4},{3,5},{4,6},{5,7},{6,8},{7,9},{8,10},{9,11},{10,... | collective-permute-start | bytes 786440 | tf_op jit(solution)/shard_map/ppermute | solution.py:41
  206.4 2.2 fusion.112
  208.7 4.1 %collective-permute-start.24 = (bf16[1024,128]{1,0:T(8,128)(2,1)S(1)}, bf16[1024,128]{1,0:T(8,128)(2,1)S(1)}, u32[]{:S(2)}, u32[]{:S(2)}) collective-permute-start(bf16[1024,128]{1,0:T(8,128)(2,1)S(1)} %copy-done.5), channel_id=1, source_target_pairs={{0,8},{1,9},{2,10},{3,11},{4,12},{5,13},{6,14},{7,15},{8,0},{9,1},... | collective-permute-start | bytes 786440 | tf_op jit(solution)/shard_map/ppermute | solution.py:41
  214.0 3.1 %collective-permute-start.19 = (bf16[1024,128]{1,0:T(8,128)(2,1)S(1)}, bf16[1024,128]{1,0:T(8,128)(2,1)S(1)}, u32[]{:S(2)}, u32[]{:S(2)}) collective-permute-start(bf16[1024,128]{1,0:T(8,128)(2,1)S(1)} %get-tuple-element.56), channel_id=1, source_target_pairs={{0,2},{1,3},{2,4},{3,5},{4,6},{5,7},{6,8},{7,9},{8,10},{9,11},{10,... | collective-permute-start | bytes 786440 | tf_op jit(solution)/shard_map/ppermute | solution.py:41
  217.1 3.4 %collective-permute-start.23 = (bf16[1024,128]{1,0:T(8,128)(2,1)S(1)}, bf16[1024,128]{1,0:T(8,128)(2,1)S(1)}, u32[]{:S(2)}, u32[]{:S(2)}) collective-permute-start(bf16[1024,128]{1,0:T(8,128)(2,1)S(1)} %get-tuple-element.57), channel_id=1, source_target_pairs={{0,14},{1,15},{2,0},{3,1},{4,2},{5,3},{6,4},{7,5},{8,6},{9,7},{10,... | collective-permute-start | bytes 786440 | tf_op jit(solution)/shard_map/ppermute | solution.py:41
  220.5 3.9 %collective-permute-done.24 = bf16[1024,128]{1,0:T(8,128)(2,1)S(1)} collective-permute-done((bf16[1024,128]{1,0:T(8,128)(2,1)S(1)}, bf16[1024,128]{1,0:T(8,128)(2,1)S(1)}, u32[]{:S(2)}, u32[]{:S(2)}) %collective-permute-start.24) | collective-permute-done | bytes 262176 | tf_op jit(solution)/shard_map/ppermute | solution.py:41
  224.4 8.1 %collective-permute-done.19 = bf16[1024,128]{1,0:T(8,128)(2,1)S(1)} collective-permute-done((bf16[1024,128]{1,0:T(8,128)(2,1)S(1)}, bf16[1024,128]{1,0:T(8,128)(2,1)S(1)}, u32[]{:S(2)}, u32[]{:S(2)}) %collective-permute-start.19) | collective-permute-done | bytes 262176 | tf_op jit(solution)/shard_map/ppermute | solution.py:41
  233.4 5.0 %all-to-all-start.3 = ((bf16[32,32,128]{2,1,0:T(8,128)(2,1)}), bf16[32,32,128]{2,1,0:T(8,128)(2,1)S(1)}, u32[]{:S(2)}, u32[]{:S(2)}) async-start(bf16[32,32,128]{2,1,0:T(8,128)(2,1)} %bitcast.68), calls=%async_computation.3 | async-start | bytes 524288 | tf_op jit(solution)/shard_map/all_to_all | solution.py:27
  238.4 11.2 %all-to-all-done.3 = bf16[32,32,128]{2,1,0:T(8,128)(2,1)S(1)} async-done(((bf16[32,32,128]{2,1,0:T(8,128)(2,1)}), bf16[32,32,128]{2,1,0:T(8,128)(2,1)S(1)}, u32[]{:S(2)}, u32[]{:S(2)}) %all-to-all-start.3) | async-done | bytes 262176 | tf_op jit(solution)/shard_map/all_to_all | solution.py:27
  (119 shorter events, 27.8 us)
Async XLA Ops:
  0.0 78.4 %copy-start = (bf16[1024,128]{1,0:T(8,128)(2,1)S(1)}, bf16[1024,128]{1,0:T(8,128)(2,1)}, u32[]{:S(2)}) copy-start(bf16[1024,128]{1,0:T(8,128)(2,1)} %param.19) | copy-start | bytes 786436
  0.0 20.2 %copy-start.8 = (s32[256,2]{0,1:T(2,128)S(1)}, s32[256,2]{0,1:T(2,128)}, u32[]{:S(2)}) copy-start(s32[256,2]{0,1:T(2,128)} %param.22) | copy-start | bytes 6148
  2.4 18.3 %collective-permute-start = (bf16[256,96]{0,1:T(8,128)(2,1)S(1)}, bf16[256,96]{0,1:T(8,128)(2,1)S(1)}, u32[]{:S(2)}, u32[]{:S(2)}) collective-permute-start(bf16[256,96]{0,1:T(8,128)(2,1)S(1)} %get-tuple-element.100), channel_id=1, source_target_pairs={{0,16},{16,0},{32,48},{48,32},{64,80},{80,64},{96,112},{112,96},{1... | collective-permute-start | bytes 147464 | tf_op jit(solution)/shard_map/ppermute | solution.py:37
  10.2 30.8 %all-to-all-start = ((bf16[8,160,256]{2,1,0:T(8,128)(2,1)}), bf16[8,160,256]{2,1,0:T(8,128)(2,1)S(1)}, u32[]{:S(2)}, u32[]{:S(2)}) async-start(bf16[8,160,256]{2,1,0:T(8,128)(2,1)} %broadcast_in_dim.9), calls=%async_computation | async-start | bytes 1310720 | tf_op jit(solution)/shard_map/all_to_all | solution.py:27
  20.8 7.2 %collective-permute-start.1 = (bf16[2,256,96]{1,2,0:T(8,128)(2,1)S(1)}, bf16[2,256,96]{1,2,0:T(8,128)(2,1)S(1)}, u32[]{:S(2)}, u32[]{:S(2)}) collective-permute-start(bf16[2,256,96]{1,2,0:T(8,128)(2,1)S(1)} %pad_maximum_fusion.6), channel_id=1, source_target_pairs={{0,32},{16,48},{32,0},{48,16},{64,96},{80,112},{96,64},{112,80},{1... | collective-permute-start | bytes 294920 | tf_op jit(solution)/shard_map/ppermute | solution.py:37
  46.8 31.7 %copy-start.6 = (bf16[256,128]{1,0:T(8,128)(2,1)S(1)}, bf16[256,128]{1,0:T(8,128)(2,1)}, u32[]{:S(2)}) copy-start(bf16[256,128]{1,0:T(8,128)(2,1)} %param.20) | copy-start | bytes 196612
  47.6 36.1 %copy-start.1 = (bf16[1,4096,128]{2,1,0:T(8,128)(2,1)S(1)}, bf16[1,4096,128]{2,1,0:T(8,128)(2,1)}, u32[]{:S(2)}) copy-start(bf16[1,4096,128]{2,1,0:T(8,128)(2,1)} %param.27) | copy-start | bytes 3145732
  47.6 9.9 %all-to-all-start.1 = ((f32[4,72,256]{2,1,0:T(8,128)}), f32[4,72,256]{2,1,0:T(8,128)S(1)}, u32[]{:S(2)}, u32[]{:S(2)}) async-start(f32[4,72,256]{2,1,0:T(8,128)} %pad_maximum_fusion.4), calls=%async_computation.1 | async-start | bytes 589824 | tf_op jit(solution)/shard_map/all_to_all | solution.py:27
  79.8 15.9 %all-to-all-start.2 = ((bf16[32,32,128]{2,1,0:T(8,128)(2,1)}), bf16[32,32,128]{2,1,0:T(8,128)(2,1)S(1)}, u32[]{:S(2)}, u32[]{:S(2)}) async-start(bf16[32,32,128]{2,1,0:T(8,128)(2,1)} %bitcast.24), calls=%async_computation.2 | async-start | bytes 524288 | tf_op jit(solution)/shard_map/all_to_all | solution.py:27
  83.8 71.0 %collective-permute-start.14 = (bf16[4,512,128]{2,1,0:T(8,128)(2,1)S(1)}, bf16[4,512,128]{2,1,0:T(8,128)(2,1)}, u32[]{:S(2)}, u32[]{:S(2)}) collective-permute-start(bf16[4,512,128]{2,1,0:T(8,128)(2,1)S(1)} %dynamic-slice_bitcast_fusion), channel_id=1, source_target_pairs={{0,2},{1,3},{2,0},{3,1},{4,6},{5,7},{6,4},{7,5},{8,10},{9,11},{10,... | collective-permute-start | bytes 1572872 | tf_op jit(solution)/shard_map/ppermute | solution.py:114
  86.1 1.8 copy-start.9
  95.8 15.1 %collective-permute-start.4 = (bf16[1024,128]{1,0:T(8,128)(2,1)S(1)}, bf16[1024,128]{1,0:T(8,128)(2,1)S(1)}, u32[]{:S(2)}, u32[]{:S(2)}) collective-permute-start(bf16[1024,128]{1,0:T(8,128)(2,1)S(1)} %bitcast.142), channel_id=1, source_target_pairs={{0,14},{1,15},{2,0},{3,1},{4,2},{5,3},{6,4},{7,5},{8,6},{9,7},{10,... | collective-permute-start | bytes 786440 | tf_op jit(solution)/shard_map/ppermute | solution.py:41
  98.2 12.7 %collective-permute-start.3 = (bf16[1024,128]{1,0:T(8,128)(2,1)S(1)}, bf16[1024,128]{1,0:T(8,128)(2,1)S(1)}, u32[]{:S(2)}, u32[]{:S(2)}) collective-permute-start(bf16[1024,128]{1,0:T(8,128)(2,1)S(1)} %bitcast.143), channel_id=1, source_target_pairs={{0,2},{1,3},{2,4},{3,5},{4,6},{5,7},{6,8},{7,9},{8,10},{9,11},{10,... | collective-permute-start | bytes 786440 | tf_op jit(solution)/shard_map/ppermute | solution.py:41
  101.1 35.0 %collective-permute-start.11 = (bf16[1024,128]{1,0:T(8,128)(2,1)S(1)}, bf16[1024,128]{1,0:T(8,128)(2,1)S(1)}, u32[]{:S(2)}, u32[]{:S(2)}) collective-permute-start(bf16[1024,128]{1,0:T(8,128)(2,1)S(1)} %bitcast.144), channel_id=1, source_target_pairs={{0,8},{1,9},{2,10},{3,11},{4,12},{5,13},{6,14},{7,15},{8,0},{9,1},... | collective-permute-start | bytes 786440 | tf_op jit(solution)/shard_map/ppermute | solution.py:41
  105.8 16.9 %collective-permute-start.2 = (bf16[1024,128]{1,0:T(8,128)(2,1)S(1)}, bf16[1024,128]{1,0:T(8,128)(2,1)S(1)}, u32[]{:S(2)}, u32[]{:S(2)}) collective-permute-start(bf16[1024,128]{1,0:T(8,128)(2,1)S(1)} %bitcast.145), channel_id=1, source_target_pairs={{0,1},{1,0},{2,3},{3,2},{4,5},{5,4},{6,7},{7,6},{8,9},{9,8},{10,11... | collective-permute-start | bytes 786440 | tf_op jit(solution)/shard_map/ppermute | solution.py:33
  111.0 37.2 %collective-permute-start.5 = (bf16[1024,256]{1,0:T(8,128)(2,1)S(1)}, bf16[1024,256]{1,0:T(8,128)(2,1)S(1)}, u32[]{:S(2)}, u32[]{:S(2)}) collective-permute-start(bf16[1024,256]{1,0:T(8,128)(2,1)S(1)} %pad_maximum_fusion.2), channel_id=1, source_target_pairs={{0,1},{1,0},{2,3},{3,2},{4,5},{5,4},{6,7},{7,6},{8,9},{9,8},{10,11... | collective-permute-start | bytes 1572872 | tf_op jit(solution)/shard_map/ppermute | solution.py:33
  120.5 9.7 %collective-permute-start.7 = (bf16[1024,128]{1,0:T(8,128)(2,1)S(1)}, bf16[1024,128]{1,0:T(8,128)(2,1)S(1)}, u32[]{:S(2)}, u32[]{:S(2)}) collective-permute-start(bf16[1024,128]{1,0:T(8,128)(2,1)S(1)} %collective-permute-done.4), channel_id=1, source_target_pairs={{0,14},{1,15},{2,0},{3,1},{4,2},{5,3},{6,4},{7,5},{8,6},{9,7},{10,... | collective-permute-start | bytes 786440 | tf_op jit(solution)/shard_map/ppermute | solution.py:41
  122.7 11.0 %collective-permute-start.6 = (bf16[1024,128]{1,0:T(8,128)(2,1)S(1)}, bf16[1024,128]{1,0:T(8,128)(2,1)S(1)}, u32[]{:S(2)}, u32[]{:S(2)}) collective-permute-start(bf16[1024,128]{1,0:T(8,128)(2,1)S(1)} %collective-permute-done.3), channel_id=1, source_target_pairs={{0,2},{1,3},{2,4},{3,5},{4,6},{5,7},{6,8},{7,9},{8,10},{9,11},{10,... | collective-permute-start | bytes 786440 | tf_op jit(solution)/shard_map/ppermute | solution.py:41
  130.2 9.2 %collective-permute-start.10 = (bf16[1024,128]{1,0:T(8,128)(2,1)S(1)}, bf16[1024,128]{1,0:T(8,128)(2,1)S(1)}, u32[]{:S(2)}, u32[]{:S(2)}) collective-permute-start(bf16[1024,128]{1,0:T(8,128)(2,1)S(1)} %collective-permute-done.7), channel_id=1, source_target_pairs={{0,14},{1,15},{2,0},{3,1},{4,2},{5,3},{6,4},{7,5},{8,6},{9,7},{10,... | collective-permute-start | bytes 786440 | tf_op jit(solution)/shard_map/ppermute | solution.py:41
  133.7 10.1 %collective-permute-start.9 = (bf16[1024,128]{1,0:T(8,128)(2,1)S(1)}, bf16[1024,128]{1,0:T(8,128)(2,1)S(1)}, u32[]{:S(2)}, u32[]{:S(2)}) collective-permute-start(bf16[1024,128]{1,0:T(8,128)(2,1)S(1)} %collective-permute-done.6), channel_id=1, source_target_pairs={{0,2},{1,3},{2,4},{3,5},{4,6},{5,7},{6,8},{7,9},{8,10},{9,11},{10,... | collective-permute-start | bytes 786440 | tf_op jit(solution)/shard_map/ppermute | solution.py:41
  136.1 13.3 %collective-permute-start.8 = (bf16[1024,256]{1,0:T(8,128)(2,1)S(1)}, bf16[1024,256]{1,0:T(8,128)(2,1)S(1)}, u32[]{:S(2)}, u32[]{:S(2)}) collective-permute-start(bf16[1024,256]{1,0:T(8,128)(2,1)S(1)} %pad_maximum_fusion.3), channel_id=1, source_target_pairs={{0,1},{1,0},{2,3},{3,2},{4,5},{5,4},{6,7},{7,6},{8,9},{9,8},{10,11... | collective-permute-start | bytes 1572872 | tf_op jit(solution)/shard_map/ppermute | solution.py:33
  143.9 6.7 %collective-permute-start.12 = (bf16[1024,384]{1,0:T(8,128)(2,1)S(1)}, bf16[1024,384]{1,0:T(8,128)(2,1)S(1)}, u32[]{:S(2)}, u32[]{:S(2)}) collective-permute-start(bf16[1024,384]{1,0:T(8,128)(2,1)S(1)} %pad_maximum_fusion.1), channel_id=1, source_target_pairs={{0,1},{1,0},{2,3},{3,2},{4,5},{5,4},{6,7},{7,6},{8,9},{9,8},{10,11... | collective-permute-start | bytes 2359304 | tf_op jit(solution)/shard_map/ppermute | solution.py:33
  152.5 2.3 copy-start.2
  152.8 22.0 %copy-start.3 = (bf16[1024,256]{0,1:T(8,128)(2,1)}, bf16[1024,256]{0,1:T(8,128)(2,1)S(1)}, u32[]{:S(2)}) copy-start(bf16[1024,256]{0,1:T(8,128)(2,1)S(1)} %fusion.13) | copy-start | bytes 1572868
  152.8 20.2 %collective-permute-start.13 = (bf16[1024,256]{0,1:T(8,128)(2,1)S(1)}, bf16[1024,256]{0,1:T(8,128)(2,1)}, u32[]{:S(2)}, u32[]{:S(2)}) collective-permute-start(bf16[1024,256]{0,1:T(8,128)(2,1)S(1)} %fusion.13), channel_id=1, source_target_pairs={{0,1},{1,0},{2,3},{3,2},{4,5},{5,4},{6,7},{7,6},{8,9},{9,8},{10,11... | collective-permute-start | bytes 1572872 | tf_op jit(solution)/shard_map/ppermute | solution.py:33
  156.8 16.3 %collective-permute-start.20 = (bf16[512,256]{1,0:T(8,128)(2,1)S(1)}, bf16[512,256]{1,0:T(8,128)(2,1)S(1)}, u32[]{:S(2)}, u32[]{:S(2)}) collective-permute-start(bf16[512,256]{1,0:T(8,128)(2,1)S(1)} %get-tuple-element.60), channel_id=1, source_target_pairs={{0,4},{1,5},{2,6},{3,7},{4,8},{5,9},{6,10},{7,11},{8,12},{9,13},{1... | collective-permute-start | bytes 786440 | tf_op jit(solution)/shard_map/ppermute | solution.py:41
  158.7 24.0 %collective-permute-start.15 = (bf16[512,256]{1,0:T(8,128)(2,1)S(1)}, bf16[512,256]{1,0:T(8,128)(2,1)}, u32[]{:S(2)}, u32[]{:S(2)}) collective-permute-start(bf16[512,256]{1,0:T(8,128)(2,1)S(1)} %get-tuple-element.58), channel_id=1, source_target_pairs={{0,12},{1,13},{2,14},{3,15},{4,0},{5,1},{6,2},{7,3},{8,4},{9,5},{1... | collective-permute-start | bytes 786440 | tf_op jit(solution)/shard_map/ppermute | solution.py:41
  164.2 20.9 %collective-permute-start.16 = (bf16[512,256]{1,0:T(8,128)(2,1)}, bf16[512,256]{1,0:T(8,128)(2,1)S(1)}, u32[]{:S(2)}, u32[]{:S(2)}) collective-permute-start(bf16[512,256]{1,0:T(8,128)(2,1)} %get-tuple-element.59), channel_id=1, source_target_pairs={{0,8},{1,9},{2,10},{3,11},{4,12},{5,13},{6,14},{7,15},{8,0},{9,1},... | collective-permute-start | bytes 786440 | tf_op jit(solution)/shard_map/ppermute | solution.py:41
  182.7 2.4 copy-start.4
  187.7 11.8 %collective-permute-start.21 = (bf16[1024,128]{1,0:T(8,128)(2,1)S(1)}, bf16[1024,128]{1,0:T(8,128)(2,1)S(1)}, u32[]{:S(2)}, u32[]{:S(2)}) collective-permute-start(bf16[1024,128]{1,0:T(8,128)(2,1)S(1)} %get-tuple-element.66), channel_id=1, source_target_pairs={{0,14},{1,15},{2,0},{3,1},{4,2},{5,3},{6,4},{7,5},{8,6},{9,7},{10,... | collective-permute-start | bytes 786440 | tf_op jit(solution)/shard_map/ppermute | solution.py:41
  189.6 12.6 %collective-permute-start.17 = (bf16[1024,128]{1,0:T(8,128)(2,1)S(1)}, bf16[1024,128]{1,0:T(8,128)(2,1)S(1)}, u32[]{:S(2)}, u32[]{:S(2)}) collective-permute-start(bf16[1024,128]{1,0:T(8,128)(2,1)S(1)} %get-tuple-element.64), channel_id=1, source_target_pairs={{0,2},{1,3},{2,4},{3,5},{4,6},{5,7},{6,8},{7,9},{8,10},{9,11},{10,... | collective-permute-start | bytes 786440 | tf_op jit(solution)/shard_map/ppermute | solution.py:41
  200.3 12.4 %collective-permute-start.22 = (bf16[1024,128]{1,0:T(8,128)(2,1)}, bf16[1024,128]{1,0:T(8,128)(2,1)}, u32[]{:S(2)}, u32[]{:S(2)}) collective-permute-start(bf16[1024,128]{1,0:T(8,128)(2,1)} %add_convert_fusion.2), channel_id=1, source_target_pairs={{0,14},{1,15},{2,0},{3,1},{4,2},{5,3},{6,4},{7,5},{8,6},{9,7},{10,... | collective-permute-start | bytes 786440 | tf_op jit(solution)/shard_map/ppermute | solution.py:41
  203.0 9.7 %collective-permute-start.18 = (bf16[1024,128]{1,0:T(8,128)(2,1)}, bf16[1024,128]{1,0:T(8,128)(2,1)}, u32[]{:S(2)}, u32[]{:S(2)}) collective-permute-start(bf16[1024,128]{1,0:T(8,128)(2,1)} %add_convert_fusion.4), channel_id=1, source_target_pairs={{0,2},{1,3},{2,4},{3,5},{4,6},{5,7},{6,8},{7,9},{8,10},{9,11},{10,... | collective-permute-start | bytes 786440 | tf_op jit(solution)/shard_map/ppermute | solution.py:41
  206.4 2.2 copy-start.5
  208.7 15.8 %collective-permute-start.24 = (bf16[1024,128]{1,0:T(8,128)(2,1)S(1)}, bf16[1024,128]{1,0:T(8,128)(2,1)S(1)}, u32[]{:S(2)}, u32[]{:S(2)}) collective-permute-start(bf16[1024,128]{1,0:T(8,128)(2,1)S(1)} %copy-done.5), channel_id=1, source_target_pairs={{0,8},{1,9},{2,10},{3,11},{4,12},{5,13},{6,14},{7,15},{8,0},{9,1},... | collective-permute-start | bytes 786440 | tf_op jit(solution)/shard_map/ppermute | solution.py:41
  214.0 24.4 %copy-start.7 = (f32[256,2]{0,1:T(2,128)S(1)}, f32[256,2]{0,1:T(2,128)}, u32[]{:S(2)}) copy-start(f32[256,2]{0,1:T(2,128)} %param.23) | copy-start | bytes 6148
  214.0 24.4 %copy-start.10 = (f32[256]{0:T(256)S(1)}, f32[256]{0:T(256)}, u32[]{:S(2)}) copy-start(f32[256]{0:T(256)} %param.24) | copy-start | bytes 3076
  214.0 18.5 %collective-permute-start.19 = (bf16[1024,128]{1,0:T(8,128)(2,1)S(1)}, bf16[1024,128]{1,0:T(8,128)(2,1)S(1)}, u32[]{:S(2)}, u32[]{:S(2)}) collective-permute-start(bf16[1024,128]{1,0:T(8,128)(2,1)S(1)} %get-tuple-element.56), channel_id=1, source_target_pairs={{0,2},{1,3},{2,4},{3,5},{4,6},{5,7},{6,8},{7,9},{8,10},{9,11},{10,... | collective-permute-start | bytes 786440 | tf_op jit(solution)/shard_map/ppermute | solution.py:41
  217.1 15.4 %collective-permute-start.23 = (bf16[1024,128]{1,0:T(8,128)(2,1)S(1)}, bf16[1024,128]{1,0:T(8,128)(2,1)S(1)}, u32[]{:S(2)}, u32[]{:S(2)}) collective-permute-start(bf16[1024,128]{1,0:T(8,128)(2,1)S(1)} %get-tuple-element.57), channel_id=1, source_target_pairs={{0,14},{1,15},{2,0},{3,1},{4,2},{5,3},{6,4},{7,5},{8,6},{9,7},{10,... | collective-permute-start | bytes 786440 | tf_op jit(solution)/shard_map/ppermute | solution.py:41
  233.4 16.3 %all-to-all-start.3 = ((bf16[32,32,128]{2,1,0:T(8,128)(2,1)}), bf16[32,32,128]{2,1,0:T(8,128)(2,1)S(1)}, u32[]{:S(2)}, u32[]{:S(2)}) async-start(bf16[32,32,128]{2,1,0:T(8,128)(2,1)} %bitcast.68), calls=%async_computation.3 | async-start | bytes 524288 | tf_op jit(solution)/shard_map/all_to_all | solution.py:27

commit v5 on v3

--- a/solution.py
+++ b/solution.py
@@ -99,6 +99,7 @@
     positions = sp * tokens + local
     rotated = rotate(rope_key, positions).T
     block = jnp.concatenate([key_value[:NOPE], rotated, key_value[NOPE:]], axis=0)
+    block, queries = lax.optimization_barrier((block, queries))
     query = jnp.concatenate([queries[:, :NOPE], rotate(queries[:, NOPE:], positions)], axis=1)
     blocks = exchange(jnp.broadcast_to(block, (Z,) + block.shape), "sp", Z_GROUPS)
 
@@ -112,7 +113,8 @@
     parity = lambda one: lax.dynamic_index_in_dim(down, one, 1, keepdims=False)
     kept = parity(odd)
     got = lax.ppermute(parity(1 - odd), "tp", [(t, t ^ 2) for t in range(TP)])
-    both = jnp.stack([jnp.where(odd == 0, kept, got), jnp.where(odd == 0, got, kept)], axis=1)
+    both = [jnp.where(odd == 0, kept, got), jnp.where(odd == 0, got, kept)]
+    both = jnp.concatenate(both, axis=2)
     down = [at(both, y // 2)]
     for by in (1, 2, 3):
         down.append(y_step(at(both, (y // 2 + by) % (Y // 2)), 2 * by))
@@ -164,27 +166,16 @@
     mixed = (residual.astype(f32) + projected).astype(bf16)
 
     sent = lax.dot_general(placed, mixed, (((0,), (0,)), ((), ())), preferred_element_type=f32)
-    sent, gate_weight, up_weight, ffn_gain, down = lax.optimization_barrier(
-        (sent.astype(bf16), gate_weight, up_weight, ffn_gain, down)
+    sent, gate_weight, up_weight, ffn_gain = lax.optimization_barrier(
+        (sent.astype(bf16), gate_weight, up_weight, ffn_gain)
     )
     arrived = exchange(sent.reshape(SP, capacity, width), "sp")
     gate_up_weight = jnp.concatenate(
         [gate_weight.reshape(TP, width, ff), up_weight.reshape(TP, width, ff)], axis=2
     )
     gains = ffn_gain.astype(f32).reshape(TP, width)
-    down = jnp.stack(down).reshape(Y, 2, ff, width)
-    down = jnp.where(core == 0, down, down[:, ::-1]).reshape(Y, 2 * ff, width)
-
-    def features(steps):
-        parts = []
-        for k in steps:
-            chip = (y + k) % Y
-            parts.append(at(down, (y // 2 - chip // 2) % (Y // 2) * 2 + chip % 2))
-        return jnp.concatenate(parts, axis=1)
-
-    down_first, down_above, down_below = features([4]), features([3, 2, 1]), features([-3, -2, -1, 0])
-    arrived, gate_up_weight, gains, down_first, down_above, down_below = lax.optimization_barrier(
-        (arrived.reshape(slots, width), gate_up_weight, gains, down_first, down_above, down_below)
+    arrived, gate_up_weight, gains = lax.optimization_barrier(
+        (arrived.reshape(slots, width), gate_up_weight, gains)
     )
 
     def products(parts):
@@ -202,13 +193,12 @@
         )
         return product, squares
 
-    half = slots // 2
-
     def ring(above, below):
         above = y_step(above, 1)
         below = y_step(below, -1)
         return above, below
 
+    half = slots // 2
     above = below = arrived
     gate_up, squares = products([(arrived, y, core), (swap(arrived), y, 1 - core)])
     for k in range(1, 4):
@@ -224,12 +214,34 @@
         )
         gate_up, squares = gate_up + more, squares + more_squares
     last = jnp.concatenate(ring(above[:half], below[half:]), axis=0)
+    last, down = lax.optimization_barrier((last, down))
+
+    def features(steps):
+        parts = []
+        for by in steps:
+            for r in range(Y // 2):
+                for h in range(2):
+                    columns = down[r][:, h * width : (h + 1) * width]
+                    if (h - 2 * r - by) % Y == 0:
+                        even_part = columns
+                    if (h - 2 * r - 1 - by) % Y == 0:
+                        odd_part = columns
+            parts.append(jnp.where(odd == 0, even_part, odd_part))
+        return jnp.concatenate(parts, axis=1)
+
+    down_first, down_above, down_below = features([4]), features([3, 2, 1]), features([-3, -2, -1, 0])
     more, more_squares = products([(last, y + 4, core), (swap(last), y + 4, 1 - core)])
     gate_up, squares = gate_up + more, squares + more_squares
     gate_up = gate_up * lax.rsqrt(squares / D + EPSILON)
     hidden = (jax.nn.silu(gate_up[:, :ff]) * gate_up[:, ff:]).astype(bf16)
 
-    hidden = jnp.concatenate([hidden, swap(hidden)], axis=1)
+    other = swap(hidden)
+    hidden = jnp.where(
+        core == 0,
+        jnp.concatenate([hidden, other], axis=1),
+        jnp.concatenate([other, hidden], axis=1),
+    )
+    hidden = lax.optimization_barrier(hidden)
     first = jnp.dot(hidden, down_first, preferred_element_type=f32).astype(bf16)
     part_above = lax.optimization_barrier(jnp.dot(hidden, down_above, preferred_element_type=f32))
     part_below = lax.optimization_barrier(jnp.dot(hidden, down_below, preferred_element_type=f32))

time: 242 us -> 249 us (1.029)
  the two profiles are of different devices: /device:TPU:56 before, /device:TPU:64 now
where the time goes in v5:
time: 249 us; the launch traced here: 247 us
  starting transfers between devices  114 us (46%)
  waiting for transfers between devices  78.8 us (32%)
  blocking collectives  19 us (8%)
  other arithmetic  17.4 us (7%)
  matrix products  14.1 us (6%)
  local copies, waits for them, and re-layouts  3.04 us (1%)
    ppermute x19, starting transfers between devices, y_step(): lax.ppermute(value, 'tp', [(t, (t + 2 * by) % TP) for t in range(TP)])  60.8 us
    ppermute x19, waiting for transfers between devices, y_step(): lax.ppermute(value, 'tp', [(t, (t + 2 * by) % TP) for t in range(TP)])  53.4 us
    all_to_all x4, starting transfers between devices, exchange(): lax.all_to_all(value, axis, split_axis=0, concat_axis=0, tiled=True, axis...  29.2 us
    all_to_all x4, waiting for transfers between devices, exchange(): lax.all_to_all(value, axis, split_axis=0, concat_axis=0, tiled=True, axis...  21.6 us
    all_gather x1, blocking collectives, body(): attended_all = lax.all_gather(attended, 'tp', axis=0, tiled=True)  19 us
    ppermute x6, starting transfers between devices, swap(): return lax.ppermute(value, 'tp', [(t, t ^ 1) for t in range(TP)])  12.3 us
    ppermute x2, starting transfers between devices, x_swap(): return lax.ppermute(value, 'sp', [(s, s ^ bit) for s in range(SP)])  8.04 us
  transfers between devices with their start and end apart: 32, of which 18 were waited for; matrix products, arithmetic and copies ran while one was open for 9% of the time, Pallas kernels for 0%

profile of v5, /device:TPU:64, one launch (start us, length us, event | category | flops | bytes accessed | tf_op | source)
XLA Modules:
  0.0 247.4 jit_solution(11408466234166444004)
XLA Ops:
  5.6 3.4 %collective-permute-start = (bf16[256,96]{0,1:T(8,128)(2,1)S(1)}, bf16[256,96]{0,1:T(8,128)(2,1)S(1)}, u32[]{:S(2)}, u32[]{:S(2)}) collective-permute-start(bf16[256,96]{0,1:T(8,128)(2,1)S(1)} %get-tuple-element.113), channel_id=1, source_target_pairs={{0,16},{16,0},{32,48},{48,32},{64,80},{80,64},{96,112},{112,96},{1... | collective-permute-start | bytes 147464 | tf_op jit(solution)/shard_map/ppermute | solution.py:37
  9.9 10.0 %all-to-all-start = ((bf16[8,160,256]{2,1,0:T(8,128)(2,1)}), bf16[8,160,256]{2,1,0:T(8,128)(2,1)S(1)}, u32[]{:S(2)}, u32[]{:S(2)}) async-start(bf16[8,160,256]{2,1,0:T(8,128)(2,1)} %broadcast_in_dim.9), calls=%async_computation | async-start | bytes 1310720 | tf_op jit(solution)/shard_map/all_to_all | solution.py:27
  20.6 3.5 %collective-permute-start.14 = (bf16[4,512,128]{2,1,0:T(8,128)(2,1)}, bf16[4,512,128]{2,1,0:T(8,128)(2,1)}, u32[]{:S(2)}, u32[]{:S(2)}) collective-permute-start(bf16[4,512,128]{2,1,0:T(8,128)(2,1)} %dynamic-slice_bitcast_fusion), channel_id=1, source_target_pairs={{0,2},{1,3},{2,0},{3,1},{4,6},{5,7},{6,4},{7,5},{8,10},{9,11},{10,... | collective-permute-start | bytes 1572872 | tf_op jit(solution)/shard_map/ppermute | solution.py:115
  25.2 4.6 %collective-permute-start.1 = (bf16[2,256,96]{1,2,0:T(8,128)(2,1)S(1)}, bf16[2,256,96]{1,2,0:T(8,128)(2,1)S(1)}, u32[]{:S(2)}, u32[]{:S(2)}) collective-permute-start(bf16[2,256,96]{1,2,0:T(8,128)(2,1)S(1)} %pad_maximum_fusion.7), channel_id=1, source_target_pairs={{0,32},{16,48},{32,0},{48,16},{64,96},{80,112},{96,64},{112,80},{1... | collective-permute-start | bytes 294920 | tf_op jit(solution)/shard_map/ppermute | solution.py:37
  29.9 3.3 %collective-permute-done.1 = bf16[2,256,96]{1,2,0:T(8,128)(2,1)S(1)} collective-permute-done((bf16[2,256,96]{1,2,0:T(8,128)(2,1)S(1)}, bf16[2,256,96]{1,2,0:T(8,128)(2,1)S(1)}, u32[]{:S(2)}, u32[]{:S(2)}) %collective-permute-start.1) | collective-permute-done | bytes 98336 | tf_op jit(solution)/shard_map/ppermute | solution.py:37
  33.3 5.1 %all-to-all-done = bf16[8,160,256]{2,1,0:T(8,128)(2,1)S(1)} async-done(((bf16[8,160,256]{2,1,0:T(8,128)(2,1)}), bf16[8,160,256]{2,1,0:T(8,128)(2,1)S(1)}, u32[]{:S(2)}, u32[]{:S(2)}) %all-to-all-start) | async-done | bytes 655392 | tf_op jit(solution)/shard_map/all_to_all | solution.py:27
  39.9 2.1 fusion
  42.0 2.2 fusion.5
  45.0 4.0 %all-to-all-start.1 = ((f32[4,72,256]{2,1,0:T(8,128)}), f32[4,72,256]{2,1,0:T(8,128)S(1)}, u32[]{:S(2)}, u32[]{:S(2)}) async-start(f32[4,72,256]{2,1,0:T(8,128)} %pad_maximum_fusion.4), calls=%async_computation.1 | async-start | bytes 589824 | tf_op jit(solution)/shard_map/all_to_all | solution.py:27
  50.1 5.7 %all-to-all-done.1 = f32[4,72,256]{2,1,0:T(8,128)S(1)} async-done(((f32[4,72,256]{2,1,0:T(8,128)}), f32[4,72,256]{2,1,0:T(8,128)S(1)}, u32[]{:S(2)}, u32[]{:S(2)}) %all-to-all-start.1) | async-done | bytes 294944 | tf_op jit(solution)/shard_map/all_to_all | solution.py:27
  56.0 19.0 %all_gather.3 = bf16[1024,256]{1,0:T(8,128)(2,1)S(1)} all-gather(bf16[64,256]{1,0:T(8,128)(2,1)S(1)} %fusion.159), channel_id=1, replica_groups=mesh['sp'=32,'tp'=16] {'tp'}, dimensions={0}, use_global_device_ids=true | all-gather | bytes 557056 | tf_op jit(solution)/shard_map/all_gather | solution.py:162
  76.4 5.4 %all-to-all-start.2 = ((bf16[32,32,128]{2,1,0:T(8,128)(2,1)}), bf16[32,32,128]{2,1,0:T(8,128)(2,1)S(1)}, u32[]{:S(2)}, u32[]{:S(2)}) async-start(bf16[32,32,128]{2,1,0:T(8,128)(2,1)} %bitcast.24), calls=%async_computation.2 | async-start | bytes 524288 | tf_op jit(solution)/shard_map/all_to_all | solution.py:27
  82.7 2.1 collective-permute-start.15
  84.9 4.9 %collective-permute-start.16 = (bf16[512,256]{1,0:T(8,128)(2,1)}, bf16[512,256]{1,0:T(8,128)(2,1)}, u32[]{:S(2)}, u32[]{:S(2)}) collective-permute-start(bf16[512,256]{1,0:T(8,128)(2,1)} %get-tuple-element.66), channel_id=1, source_target_pairs={{0,8},{1,9},{2,10},{3,11},{4,12},{5,13},{6,14},{7,15},{8,0},{9,1},... | collective-permute-start | bytes 786440 | tf_op jit(solution)/shard_map/ppermute | solution.py:41
  89.8 5.8 %collective-permute-start.17 = (bf16[512,256]{1,0:T(8,128)(2,1)}, bf16[512,256]{1,0:T(8,128)(2,1)}, u32[]{:S(2)}, u32[]{:S(2)}) collective-permute-start(bf16[512,256]{1,0:T(8,128)(2,1)} %get-tuple-element.63), channel_id=1, source_target_pairs={{0,12},{1,13},{2,14},{3,15},{4,0},{5,1},{6,2},{7,3},{8,4},{9,5},{1... | collective-permute-start | bytes 786440 | tf_op jit(solution)/shard_map/ppermute | solution.py:41
  95.6 1.7 pad_maximum_fusion
  97.4 2.0 collective-permute-start.4
  99.5 1.9 collective-permute-start.2
  102.0 17.9 %collective-permute-done.4 = bf16[1024,128]{1,0:T(8,128)(2,1)S(1)} collective-permute-done((bf16[1024,128]{1,0:T(8,128)(2,1)S(1)}, bf16[1024,128]{1,0:T(8,128)(2,1)S(1)}, u32[]{:S(2)}, u32[]{:S(2)}) %collective-permute-start.4) | collective-permute-done | bytes 262176 | tf_op jit(solution)/shard_map/ppermute | solution.py:41
  119.9 3.9 %collective-permute-start.3 = (bf16[1024,128]{1,0:T(8,128)(2,1)S(1)}, bf16[1024,128]{1,0:T(8,128)(2,1)S(1)}, u32[]{:S(2)}, u32[]{:S(2)}) collective-permute-start(bf16[1024,128]{1,0:T(8,128)(2,1)S(1)} %bitcast.144), channel_id=1, source_target_pairs={{0,2},{1,3},{2,4},{3,5},{4,6},{5,7},{6,8},{7,9},{8,10},{9,11},{10,... | collective-permute-start | bytes 786440 | tf_op jit(solution)/shard_map/ppermute | solution.py:41
  123.8 3.2 %collective-permute-start.7 = (bf16[1024,128]{1,0:T(8,128)(2,1)S(1)}, bf16[1024,128]{1,0:T(8,128)(2,1)S(1)}, u32[]{:S(2)}, u32[]{:S(2)}) collective-permute-start(bf16[1024,128]{1,0:T(8,128)(2,1)S(1)} %collective-permute-done.4), channel_id=1, source_target_pairs={{0,14},{1,15},{2,0},{3,1},{4,2},{5,3},{6,4},{7,5},{8,6},{9,7},{10,... | collective-permute-start | bytes 786440 | tf_op jit(solution)/shard_map/ppermute | solution.py:41
  127.6 3.3 %collective-permute-done.3 = bf16[1024,128]{1,0:T(8,128)(2,1)S(1)} collective-permute-done((bf16[1024,128]{1,0:T(8,128)(2,1)S(1)}, bf16[1024,128]{1,0:T(8,128)(2,1)S(1)}, u32[]{:S(2)}, u32[]{:S(2)}) %collective-permute-start.3) | collective-permute-done | bytes 262176 | tf_op jit(solution)/shard_map/ppermute | solution.py:41
  131.0 2.9 %collective-permute-start.6 = (bf16[1024,128]{1,0:T(8,128)(2,1)S(1)}, bf16[1024,128]{1,0:T(8,128)(2,1)S(1)}, u32[]{:S(2)}, u32[]{:S(2)}) collective-permute-start(bf16[1024,128]{1,0:T(8,128)(2,1)S(1)} %collective-permute-done.3), channel_id=1, source_target_pairs={{0,2},{1,3},{2,4},{3,5},{4,6},{5,7},{6,8},{7,9},{8,10},{9,11},{10,... | collective-permute-start | bytes 786440 | tf_op jit(solution)/shard_map/ppermute | solution.py:41
  134.4 4.2 %collective-permute-start.10 = (bf16[1024,128]{1,0:T(8,128)(2,1)S(1)}, bf16[1024,128]{1,0:T(8,128)(2,1)S(1)}, u32[]{:S(2)}, u32[]{:S(2)}) collective-permute-start(bf16[1024,128]{1,0:T(8,128)(2,1)S(1)} %collective-permute-done.7), channel_id=1, source_target_pairs={{0,14},{1,15},{2,0},{3,1},{4,2},{5,3},{6,4},{7,5},{8,6},{9,7},{10,... | collective-permute-start | bytes 786440 | tf_op jit(solution)/shard_map/ppermute | solution.py:41
  138.5 2.7 %collective-permute-done.6 = bf16[1024,128]{1,0:T(8,128)(2,1)S(1)} collective-permute-done((bf16[1024,128]{1,0:T(8,128)(2,1)S(1)}, bf16[1024,128]{1,0:T(8,128)(2,1)S(1)}, u32[]{:S(2)}, u32[]{:S(2)}) %collective-permute-start.6) | collective-permute-done | bytes 262176 | tf_op jit(solution)/shard_map/ppermute | solution.py:41
  141.2 1.9 collective-permute-start.9
  143.7 1.9 collective-permute-start.5
  145.6 5.1 %collective-permute-done.9 = bf16[1024,128]{1,0:T(8,128)(2,1)S(1)} collective-permute-done((bf16[1024,128]{1,0:T(8,128)(2,1)S(1)}, bf16[1024,128]{1,0:T(8,128)(2,1)S(1)}, u32[]{:S(2)}, u32[]{:S(2)}) %collective-permute-start.9) | collective-permute-done | bytes 262176 | tf_op jit(solution)/shard_map/ppermute | solution.py:41
  150.7 2.1 collective-permute-start.8
  153.3 1.9 collective-permute-start.13
  155.6 5.5 %collective-permute-done.13 = bf16[512,128]{1,0:T(8,128)(2,1)S(1)} collective-permute-done((bf16[512,128]{1,0:T(8,128)(2,1)S(1)}, bf16[512,128]{1,0:T(8,128)(2,1)S(1)}, u32[]{:S(2)}, u32[]{:S(2)}) %collective-permute-start.13) | collective-permute-done | bytes 131104 | tf_op jit(solution)/shard_map/ppermute | solution.py:41
  161.1 1.9 collective-permute-start.12
  163.8 5.5 %collective-permute-done.12 = bf16[512,128]{1,0:T(8,128)(2,1)S(1)} collective-permute-done((bf16[512,128]{1,0:T(8,128)(2,1)S(1)}, bf16[512,128]{1,0:T(8,128)(2,1)S(1)}, u32[]{:S(2)}, u32[]{:S(2)}) %collective-permute-start.12) | collective-permute-done | bytes 131104 | tf_op jit(solution)/shard_map/ppermute | solution.py:41
  169.3 1.9 collective-permute-start.11
  171.2 2.4 collective-permute-start.18
  177.4 2.1 collective-permute-start.19
  183.2 2.5 %collective-permute-start.24 = (bf16[512,128]{1,0:T(8,128)(2,1)S(1)}, bf16[512,128]{1,0:T(8,128)(2,1)S(1)}, u32[]{:S(2)}, u32[]{:S(2)}) collective-permute-start(bf16[512,128]{1,0:T(8,128)(2,1)S(1)} %get-tuple-element.78), channel_id=1, source_target_pairs={{0,14},{1,15},{2,0},{3,1},{4,2},{5,3},{6,4},{7,5},{8,6},{9,7},{10,... | collective-permute-start | bytes 393224 | tf_op jit(solution)/shard_map/ppermute | solution.py:41
  186.4 3.4 %collective-permute-start.20 = (bf16[512,128]{1,0:T(8,128)(2,1)S(1)}, bf16[512,128]{1,0:T(8,128)(2,1)S(1)}, u32[]{:S(2)}, u32[]{:S(2)}) collective-permute-start(bf16[512,128]{1,0:T(8,128)(2,1)S(1)} %get-tuple-element.77), channel_id=1, source_target_pairs={{0,2},{1,3},{2,4},{3,5},{4,6},{5,7},{6,8},{7,9},{8,10},{9,11},{10,... | collective-permute-start | bytes 393224 | tf_op jit(solution)/shard_map/ppermute | solution.py:41
  190.7 3.7 %collective-permute-start.25 = (bf16[1024,128]{1,0:T(8,128)(2,1)S(1)}, bf16[1024,128]{1,0:T(8,128)(2,1)S(1)}, u32[]{:S(2)}, u32[]{:S(2)}) collective-permute-start(bf16[1024,128]{1,0:T(8,128)(2,1)S(1)} %fusion.75), channel_id=1, source_target_pairs={{0,14},{1,15},{2,0},{3,1},{4,2},{5,3},{6,4},{7,5},{8,6},{9,7},{10,... | collective-permute-start | bytes 786440 | tf_op jit(solution)/shard_map/ppermute | solution.py:41
  195.2 2.1 collective-permute-start.21
  197.4 2.7 %collective-permute-done.25 = bf16[1024,128]{1,0:T(8,128)(2,1)S(1)} collective-permute-done((bf16[1024,128]{1,0:T(8,128)(2,1)S(1)}, bf16[1024,128]{1,0:T(8,128)(2,1)S(1)}, u32[]{:S(2)}, u32[]{:S(2)}) %collective-permute-start.25) | collective-permute-done | bytes 262176 | tf_op jit(solution)/shard_map/ppermute | solution.py:41
  200.2 4.9 %collective-permute-start.26 = (bf16[1024,128]{1,0:T(8,128)(2,1)S(1)}, bf16[1024,128]{1,0:T(8,128)(2,1)S(1)}, u32[]{:S(2)}, u32[]{:S(2)}) collective-permute-start(bf16[1024,128]{1,0:T(8,128)(2,1)S(1)} %fusion.74), channel_id=1, source_target_pairs={{0,14},{1,15},{2,0},{3,1},{4,2},{5,3},{6,4},{7,5},{8,6},{9,7},{10,... | collective-permute-start | bytes 786440 | tf_op jit(solution)/shard_map/ppermute | solution.py:41
  205.6 1.9 collective-permute-start.22
  209.3 5.6 %collective-permute-start.27 = (bf16[1024,128]{1,0:T(8,128)(2,1)S(1)}, bf16[1024,128]{1,0:T(8,128)(2,1)S(1)}, u32[]{:S(2)}, u32[]{:S(2)}) collective-permute-start(bf16[1024,128]{1,0:T(8,128)(2,1)S(1)} %fusion.73), channel_id=1, source_target_pairs={{0,14},{1,15},{2,0},{3,1},{4,2},{5,3},{6,4},{7,5},{8,6},{9,7},{10,... | collective-permute-start | bytes 786440 | tf_op jit(solution)/shard_map/ppermute | solution.py:41
  215.2 1.9 collective-permute-start.23
  218.8 5.8 %collective-permute-done.23 = bf16[1024,128]{1,0:T(8,128)(2,1)S(1)} collective-permute-done((bf16[1024,128]{1,0:T(8,128)(2,1)S(1)}, bf16[1024,128]{1,0:T(8,128)(2,1)S(1)}, u32[]{:S(2)}, u32[]{:S(2)}) %collective-permute-start.23) | collective-permute-done | bytes 262176 | tf_op jit(solution)/shard_map/ppermute | solution.py:41
  225.4 9.9 %all-to-all-start.3 = ((bf16[32,32,128]{2,1,0:T(8,128)(2,1)}), bf16[32,32,128]{2,1,0:T(8,128)(2,1)S(1)}, u32[]{:S(2)}, u32[]{:S(2)}) async-start(bf16[32,32,128]{2,1,0:T(8,128)(2,1)} %bitcast.68), calls=%async_computation.3 | async-start | bytes 524288 | tf_op jit(solution)/shard_map/all_to_all | solution.py:27
  235.4 10.7 %all-to-all-done.3 = bf16[32,32,128]{2,1,0:T(8,128)(2,1)S(1)} async-done(((bf16[32,32,128]{2,1,0:T(8,128)(2,1)}), bf16[32,32,128]{2,1,0:T(8,128)(2,1)S(1)}, u32[]{:S(2)}, u32[]{:S(2)}) %all-to-all-start.3) | async-done | bytes 262176 | tf_op jit(solution)/shard_map/all_to_all | solution.py:27
  (127 shorter events, 33.9 us)
Async XLA Ops:
  0.0 75.0 %copy-start = (bf16[1024,128]{1,0:T(8,128)(2,1)S(1)}, bf16[1024,128]{1,0:T(8,128)(2,1)}, u32[]{:S(2)}) copy-start(bf16[1024,128]{1,0:T(8,128)(2,1)} %param.19) | copy-start | bytes 786436
  0.0 19.8 %copy-start.1 = (bf16[1,4096,128]{2,1,0:T(8,128)(2,1)S(1)}, bf16[1,4096,128]{2,1,0:T(8,128)(2,1)}, u32[]{:S(2)}) copy-start(bf16[1,4096,128]{2,1,0:T(8,128)(2,1)} %param.27) | copy-start | bytes 3145732
  1.8 22.3 %copy-start.4 = (s32[256,2]{0,1:T(2,128)S(1)}, s32[256,2]{0,1:T(2,128)}, u32[]{:S(2)}) copy-start(s32[256,2]{0,1:T(2,128)} %param.22) | copy-start | bytes 6148
  5.6 19.6 %collective-permute-start = (bf16[256,96]{0,1:T(8,128)(2,1)S(1)}, bf16[256,96]{0,1:T(8,128)(2,1)S(1)}, u32[]{:S(2)}, u32[]{:S(2)}) collective-permute-start(bf16[256,96]{0,1:T(8,128)(2,1)S(1)} %get-tuple-element.113), channel_id=1, source_target_pairs={{0,16},{16,0},{32,48},{48,32},{64,80},{80,64},{96,112},{112,96},{1... | collective-permute-start | bytes 147464 | tf_op jit(solution)/shard_map/ppermute | solution.py:37
  9.9 28.5 %all-to-all-start = ((bf16[8,160,256]{2,1,0:T(8,128)(2,1)}), bf16[8,160,256]{2,1,0:T(8,128)(2,1)S(1)}, u32[]{:S(2)}, u32[]{:S(2)}) async-start(bf16[8,160,256]{2,1,0:T(8,128)(2,1)} %broadcast_in_dim.9), calls=%async_computation | async-start | bytes 1310720 | tf_op jit(solution)/shard_map/all_to_all | solution.py:27
  20.6 28.4 %collective-permute-start.14 = (bf16[4,512,128]{2,1,0:T(8,128)(2,1)}, bf16[4,512,128]{2,1,0:T(8,128)(2,1)}, u32[]{:S(2)}, u32[]{:S(2)}) collective-permute-start(bf16[4,512,128]{2,1,0:T(8,128)(2,1)} %dynamic-slice_bitcast_fusion), channel_id=1, source_target_pairs={{0,2},{1,3},{2,0},{3,1},{4,6},{5,7},{6,4},{7,5},{8,10},{9,11},{10,... | collective-permute-start | bytes 1572872 | tf_op jit(solution)/shard_map/ppermute | solution.py:115
  25.2 8.0 %collective-permute-start.1 = (bf16[2,256,96]{1,2,0:T(8,128)(2,1)S(1)}, bf16[2,256,96]{1,2,0:T(8,128)(2,1)S(1)}, u32[]{:S(2)}, u32[]{:S(2)}) collective-permute-start(bf16[2,256,96]{1,2,0:T(8,128)(2,1)S(1)} %pad_maximum_fusion.7), channel_id=1, source_target_pairs={{0,32},{16,48},{32,0},{48,16},{64,96},{80,112},{96,64},{112,80},{1... | collective-permute-start | bytes 294920 | tf_op jit(solution)/shard_map/ppermute | solution.py:37
  44.3 30.7 %copy-start.2 = (bf16[256,128]{1,0:T(8,128)(2,1)S(1)}, bf16[256,128]{1,0:T(8,128)(2,1)}, u32[]{:S(2)}) copy-start(bf16[256,128]{1,0:T(8,128)(2,1)} %param.20) | copy-start | bytes 196612
  45.0 10.8 %all-to-all-start.1 = ((f32[4,72,256]{2,1,0:T(8,128)}), f32[4,72,256]{2,1,0:T(8,128)S(1)}, u32[]{:S(2)}, u32[]{:S(2)}) async-start(f32[4,72,256]{2,1,0:T(8,128)} %pad_maximum_fusion.4), calls=%async_computation.1 | async-start | bytes 589824 | tf_op jit(solution)/shard_map/all_to_all | solution.py:27
  76.4 21.0 %all-to-all-start.2 = ((bf16[32,32,128]{2,1,0:T(8,128)(2,1)}), bf16[32,32,128]{2,1,0:T(8,128)(2,1)S(1)}, u32[]{:S(2)}, u32[]{:S(2)}) async-start(bf16[32,32,128]{2,1,0:T(8,128)(2,1)} %bitcast.24), calls=%async_computation.2 | async-start | bytes 524288 | tf_op jit(solution)/shard_map/all_to_all | solution.py:27
  82.7 88.5 %collective-permute-start.15 = (bf16[512,256]{1,0:T(8,128)(2,1)}, bf16[512,256]{1,0:T(8,128)(2,1)}, u32[]{:S(2)}, u32[]{:S(2)}) collective-permute-start(bf16[512,256]{1,0:T(8,128)(2,1)} %get-tuple-element.65), channel_id=1, source_target_pairs={{0,4},{1,5},{2,6},{3,7},{4,8},{5,9},{6,10},{7,11},{8,12},{9,13},{1... | collective-permute-start | bytes 786440 | tf_op jit(solution)/shard_map/ppermute | solution.py:41
  84.9 86.4 %collective-permute-start.16 = (bf16[512,256]{1,0:T(8,128)(2,1)}, bf16[512,256]{1,0:T(8,128)(2,1)}, u32[]{:S(2)}, u32[]{:S(2)}) collective-permute-start(bf16[512,256]{1,0:T(8,128)(2,1)} %get-tuple-element.66), channel_id=1, source_target_pairs={{0,8},{1,9},{2,10},{3,11},{4,12},{5,13},{6,14},{7,15},{8,0},{9,1},... | collective-permute-start | bytes 786440 | tf_op jit(solution)/shard_map/ppermute | solution.py:41
  89.8 81.4 %collective-permute-start.17 = (bf16[512,256]{1,0:T(8,128)(2,1)}, bf16[512,256]{1,0:T(8,128)(2,1)}, u32[]{:S(2)}, u32[]{:S(2)}) collective-permute-start(bf16[512,256]{1,0:T(8,128)(2,1)} %get-tuple-element.63), channel_id=1, source_target_pairs={{0,12},{1,13},{2,14},{3,15},{4,0},{5,1},{6,2},{7,3},{8,4},{9,5},{1... | collective-permute-start | bytes 786440 | tf_op jit(solution)/shard_map/ppermute | solution.py:41
  95.6 1.8 copy-start.5
  97.4 22.5 %collective-permute-start.4 = (bf16[1024,128]{1,0:T(8,128)(2,1)S(1)}, bf16[1024,128]{1,0:T(8,128)(2,1)S(1)}, u32[]{:S(2)}, u32[]{:S(2)}) collective-permute-start(bf16[1024,128]{1,0:T(8,128)(2,1)S(1)} %bitcast.141), channel_id=1, source_target_pairs={{0,14},{1,15},{2,0},{3,1},{4,2},{5,3},{6,4},{7,5},{8,6},{9,7},{10,... | collective-permute-start | bytes 786440 | tf_op jit(solution)/shard_map/ppermute | solution.py:41
  99.5 24.3 %collective-permute-start.2 = (bf16[1024,128]{1,0:T(8,128)(2,1)S(1)}, bf16[1024,128]{1,0:T(8,128)(2,1)S(1)}, u32[]{:S(2)}, u32[]{:S(2)}) collective-permute-start(bf16[1024,128]{1,0:T(8,128)(2,1)S(1)} %bitcast.142), channel_id=1, source_target_pairs={{0,1},{1,0},{2,3},{3,2},{4,5},{5,4},{6,7},{7,6},{8,9},{9,8},{10,11... | collective-permute-start | bytes 786440 | tf_op jit(solution)/shard_map/ppermute | solution.py:33
  119.9 11.1 %collective-permute-start.3 = (bf16[1024,128]{1,0:T(8,128)(2,1)S(1)}, bf16[1024,128]{1,0:T(8,128)(2,1)S(1)}, u32[]{:S(2)}, u32[]{:S(2)}) collective-permute-start(bf16[1024,128]{1,0:T(8,128)(2,1)S(1)} %bitcast.144), channel_id=1, source_target_pairs={{0,2},{1,3},{2,4},{3,5},{4,6},{5,7},{6,8},{7,9},{8,10},{9,11},{10,... | collective-permute-start | bytes 786440 | tf_op jit(solution)/shard_map/ppermute | solution.py:41
  123.8 10.6 %collective-permute-start.7 = (bf16[1024,128]{1,0:T(8,128)(2,1)S(1)}, bf16[1024,128]{1,0:T(8,128)(2,1)S(1)}, u32[]{:S(2)}, u32[]{:S(2)}) collective-permute-start(bf16[1024,128]{1,0:T(8,128)(2,1)S(1)} %collective-permute-done.4), channel_id=1, source_target_pairs={{0,14},{1,15},{2,0},{3,1},{4,2},{5,3},{6,4},{7,5},{8,6},{9,7},{10,... | collective-permute-start | bytes 786440 | tf_op jit(solution)/shard_map/ppermute | solution.py:41
  131.0 10.2 %collective-permute-start.6 = (bf16[1024,128]{1,0:T(8,128)(2,1)S(1)}, bf16[1024,128]{1,0:T(8,128)(2,1)S(1)}, u32[]{:S(2)}, u32[]{:S(2)}) collective-permute-start(bf16[1024,128]{1,0:T(8,128)(2,1)S(1)} %collective-permute-done.3), channel_id=1, source_target_pairs={{0,2},{1,3},{2,4},{3,5},{4,6},{5,7},{6,8},{7,9},{8,10},{9,11},{10,... | collective-permute-start | bytes 786440 | tf_op jit(solution)/shard_map/ppermute | solution.py:41
  134.4 9.3 %collective-permute-start.10 = (bf16[1024,128]{1,0:T(8,128)(2,1)S(1)}, bf16[1024,128]{1,0:T(8,128)(2,1)S(1)}, u32[]{:S(2)}, u32[]{:S(2)}) collective-permute-start(bf16[1024,128]{1,0:T(8,128)(2,1)S(1)} %collective-permute-done.7), channel_id=1, source_target_pairs={{0,14},{1,15},{2,0},{3,1},{4,2},{5,3},{6,4},{7,5},{8,6},{9,7},{10,... | collective-permute-start | bytes 786440 | tf_op jit(solution)/shard_map/ppermute | solution.py:41
  141.2 9.5 %collective-permute-start.9 = (bf16[1024,128]{1,0:T(8,128)(2,1)S(1)}, bf16[1024,128]{1,0:T(8,128)(2,1)S(1)}, u32[]{:S(2)}, u32[]{:S(2)}) collective-permute-start(bf16[1024,128]{1,0:T(8,128)(2,1)S(1)} %collective-permute-done.6), channel_id=1, source_target_pairs={{0,2},{1,3},{2,4},{3,5},{4,6},{5,7},{6,8},{7,9},{8,10},{9,11},{10,... | collective-permute-start | bytes 786440 | tf_op jit(solution)/shard_map/ppermute | solution.py:41
  143.7 9.7 %collective-permute-start.5 = (bf16[1024,256]{1,0:T(8,128)(2,1)S(1)}, bf16[1024,256]{1,0:T(8,128)(2,1)S(1)}, u32[]{:S(2)}, u32[]{:S(2)}) collective-permute-start(bf16[1024,256]{1,0:T(8,128)(2,1)S(1)} %pad_maximum_fusion.1), channel_id=1, source_target_pairs={{0,1},{1,0},{2,3},{3,2},{4,5},{5,4},{6,7},{7,6},{8,9},{9,8},{10,11... | collective-permute-start | bytes 1572872 | tf_op jit(solution)/shard_map/ppermute | solution.py:33
  150.7 23.2 %collective-permute-start.8 = (bf16[1024,256]{1,0:T(8,128)(2,1)S(1)}, bf16[1024,256]{1,0:T(8,128)(2,1)S(1)}, u32[]{:S(2)}, u32[]{:S(2)}) collective-permute-start(bf16[1024,256]{1,0:T(8,128)(2,1)S(1)} %pad_maximum_fusion.2), channel_id=1, source_target_pairs={{0,1},{1,0},{2,3},{3,2},{4,5},{5,4},{6,7},{7,6},{8,9},{9,8},{10,11... | collective-permute-start | bytes 1572872 | tf_op jit(solution)/shard_map/ppermute | solution.py:33
  153.3 7.8 %collective-permute-start.13 = (bf16[512,128]{1,0:T(8,128)(2,1)S(1)}, bf16[512,128]{1,0:T(8,128)(2,1)S(1)}, u32[]{:S(2)}, u32[]{:S(2)}) collective-permute-start(bf16[512,128]{1,0:T(8,128)(2,1)S(1)} %slice.225), channel_id=1, source_target_pairs={{0,14},{1,15},{2,0},{3,1},{4,2},{5,3},{6,4},{7,5},{8,6},{9,7},{10,... | collective-permute-start | bytes 393224 | tf_op jit(solution)/shard_map/ppermute | solution.py:41
  161.1 8.1 %collective-permute-start.12 = (bf16[512,128]{1,0:T(8,128)(2,1)S(1)}, bf16[512,128]{1,0:T(8,128)(2,1)S(1)}, u32[]{:S(2)}, u32[]{:S(2)}) collective-permute-start(bf16[512,128]{1,0:T(8,128)(2,1)S(1)} %slice.224), channel_id=1, source_target_pairs={{0,2},{1,3},{2,4},{3,5},{4,6},{5,7},{6,8},{7,9},{8,10},{9,11},{10,... | collective-permute-start | bytes 393224 | tf_op jit(solution)/shard_map/ppermute | solution.py:41
  169.3 6.0 %collective-permute-start.11 = (bf16[1024,256]{1,0:T(8,128)(2,1)S(1)}, bf16[1024,256]{1,0:T(8,128)(2,1)S(1)}, u32[]{:S(2)}, u32[]{:S(2)}) collective-permute-start(bf16[1024,256]{1,0:T(8,128)(2,1)S(1)} %pad_maximum_fusion.3), channel_id=1, source_target_pairs={{0,1},{1,0},{2,3},{3,2},{4,5},{5,4},{6,7},{7,6},{8,9},{9,8},{10,11... | collective-permute-start | bytes 1572872 | tf_op jit(solution)/shard_map/ppermute | solution.py:33
  171.2 3.8 %collective-permute-start.18 = (bf16[1024,128]{1,0:T(8,128)(2,1)S(1)}, bf16[1024,128]{1,0:T(8,128)(2,1)S(1)}, u32[]{:S(2)}, u32[]{:S(2)}) collective-permute-start(bf16[1024,128]{1,0:T(8,128)(2,1)S(1)} %pad_maximum_fusion.5), channel_id=1, source_target_pairs={{0,1},{1,0},{2,3},{3,2},{4,5},{5,4},{6,7},{7,6},{8,9},{9,8},{10,11... | collective-permute-start | bytes 786440 | tf_op jit(solution)/shard_map/ppermute | solution.py:33
  177.4 3.8 %collective-permute-start.19 = (bf16[1024,256]{0,1:T(8,128)(2,1)S(1)}, bf16[1024,256]{0,1:T(8,128)(2,1)S(1)}, u32[]{:S(2)}, u32[]{:S(2)}) collective-permute-start(bf16[1024,256]{0,1:T(8,128)(2,1)S(1)} %fusion.13), channel_id=1, source_target_pairs={{0,1},{1,0},{2,3},{3,2},{4,5},{5,4},{6,7},{7,6},{8,9},{9,8},{10,11... | collective-permute-start | bytes 1572872 | tf_op jit(solution)/shard_map/ppermute | solution.py:33
  183.2 7.4 %collective-permute-start.24 = (bf16[512,128]{1,0:T(8,128)(2,1)S(1)}, bf16[512,128]{1,0:T(8,128)(2,1)S(1)}, u32[]{:S(2)}, u32[]{:S(2)}) collective-permute-start(bf16[512,128]{1,0:T(8,128)(2,1)S(1)} %get-tuple-element.78), channel_id=1, source_target_pairs={{0,14},{1,15},{2,0},{3,1},{4,2},{5,3},{6,4},{7,5},{8,6},{9,7},{10,... | collective-permute-start | bytes 393224 | tf_op jit(solution)/shard_map/ppermute | solution.py:41
  186.4 8.7 %collective-permute-start.20 = (bf16[512,128]{1,0:T(8,128)(2,1)S(1)}, bf16[512,128]{1,0:T(8,128)(2,1)S(1)}, u32[]{:S(2)}, u32[]{:S(2)}) collective-permute-start(bf16[512,128]{1,0:T(8,128)(2,1)S(1)} %get-tuple-element.77), channel_id=1, source_target_pairs={{0,2},{1,3},{2,4},{3,5},{4,6},{5,7},{6,8},{7,9},{8,10},{9,11},{10,... | collective-permute-start | bytes 393224 | tf_op jit(solution)/shard_map/ppermute | solution.py:41
  190.7 9.4 %collective-permute-start.25 = (bf16[1024,128]{1,0:T(8,128)(2,1)S(1)}, bf16[1024,128]{1,0:T(8,128)(2,1)S(1)}, u32[]{:S(2)}, u32[]{:S(2)}) collective-permute-start(bf16[1024,128]{1,0:T(8,128)(2,1)S(1)} %fusion.75), channel_id=1, source_target_pairs={{0,14},{1,15},{2,0},{3,1},{4,2},{5,3},{6,4},{7,5},{8,6},{9,7},{10,... | collective-permute-start | bytes 786440 | tf_op jit(solution)/shard_map/ppermute | solution.py:41
  195.2 10.3 %collective-permute-start.21 = (bf16[1024,128]{1,0:T(8,128)(2,1)S(1)}, bf16[1024,128]{1,0:T(8,128)(2,1)S(1)}, u32[]{:S(2)}, u32[]{:S(2)}) collective-permute-start(bf16[1024,128]{1,0:T(8,128)(2,1)S(1)} %fusion.78), channel_id=1, source_target_pairs={{0,2},{1,3},{2,4},{3,5},{4,6},{5,7},{6,8},{7,9},{8,10},{9,11},{10,... | collective-permute-start | bytes 786440 | tf_op jit(solution)/shard_map/ppermute | solution.py:41
  200.2 9.0 %collective-permute-start.26 = (bf16[1024,128]{1,0:T(8,128)(2,1)S(1)}, bf16[1024,128]{1,0:T(8,128)(2,1)S(1)}, u32[]{:S(2)}, u32[]{:S(2)}) collective-permute-start(bf16[1024,128]{1,0:T(8,128)(2,1)S(1)} %fusion.74), channel_id=1, source_target_pairs={{0,14},{1,15},{2,0},{3,1},{4,2},{5,3},{6,4},{7,5},{8,6},{9,7},{10,... | collective-permute-start | bytes 786440 | tf_op jit(solution)/shard_map/ppermute | solution.py:41
  205.6 29.7 %copy-start.3 = (f32[256,2]{0,1:T(2,128)S(1)}, f32[256,2]{0,1:T(2,128)}, u32[]{:S(2)}) copy-start(f32[256,2]{0,1:T(2,128)} %param.23) | copy-start | bytes 6148
  205.6 29.7 %copy-start.6 = (f32[256]{0:T(256)S(1)}, f32[256]{0:T(256)}, u32[]{:S(2)}) copy-start(f32[256]{0:T(256)} %param.24) | copy-start | bytes 3076
  205.6 9.5 %collective-permute-start.22 = (bf16[1024,128]{1,0:T(8,128)(2,1)S(1)}, bf16[1024,128]{1,0:T(8,128)(2,1)S(1)}, u32[]{:S(2)}, u32[]{:S(2)}) collective-permute-start(bf16[1024,128]{1,0:T(8,128)(2,1)S(1)} %fusion.77), channel_id=1, source_target_pairs={{0,2},{1,3},{2,4},{3,5},{4,6},{5,7},{6,8},{7,9},{8,10},{9,11},{10,... | collective-permute-start | bytes 786440 | tf_op jit(solution)/shard_map/ppermute | solution.py:41
  209.3 9.5 %collective-permute-start.27 = (bf16[1024,128]{1,0:T(8,128)(2,1)S(1)}, bf16[1024,128]{1,0:T(8,128)(2,1)S(1)}, u32[]{:S(2)}, u32[]{:S(2)}) collective-permute-start(bf16[1024,128]{1,0:T(8,128)(2,1)S(1)} %fusion.73), channel_id=1, source_target_pairs={{0,14},{1,15},{2,0},{3,1},{4,2},{5,3},{6,4},{7,5},{8,6},{9,7},{10,... | collective-permute-start | bytes 786440 | tf_op jit(solution)/shard_map/ppermute | solution.py:41
  215.2 9.5 %collective-permute-start.23 = (bf16[1024,128]{1,0:T(8,128)(2,1)S(1)}, bf16[1024,128]{1,0:T(8,128)(2,1)S(1)}, u32[]{:S(2)}, u32[]{:S(2)}) collective-permute-start(bf16[1024,128]{1,0:T(8,128)(2,1)S(1)} %fusion.76), channel_id=1, source_target_pairs={{0,2},{1,3},{2,4},{3,5},{4,6},{5,7},{6,8},{7,9},{8,10},{9,11},{10,... | collective-permute-start | bytes 786440 | tf_op jit(solution)/shard_map/ppermute | solution.py:41
  225.4 20.7 %all-to-all-start.3 = ((bf16[32,32,128]{2,1,0:T(8,128)(2,1)}), bf16[32,32,128]{2,1,0:T(8,128)(2,1)S(1)}, u32[]{:S(2)}, u32[]{:S(2)}) async-start(bf16[32,32,128]{2,1,0:T(8,128)(2,1)} %bitcast.68), calls=%async_computation.3 | async-start | bytes 524288 | tf_op jit(solution)/shard_map/all_to_all | solution.py:27

commit v6 on v3

--- a/solution.py
+++ b/solution.py
@@ -99,6 +99,7 @@
     positions = sp * tokens + local
     rotated = rotate(rope_key, positions).T
     block = jnp.concatenate([key_value[:NOPE], rotated, key_value[NOPE:]], axis=0)
+    block, queries = lax.optimization_barrier((block, queries))
     query = jnp.concatenate([queries[:, :NOPE], rotate(queries[:, NOPE:], positions)], axis=1)
     blocks = exchange(jnp.broadcast_to(block, (Z,) + block.shape), "sp", Z_GROUPS)
 
@@ -112,7 +113,8 @@
     parity = lambda one: lax.dynamic_index_in_dim(down, one, 1, keepdims=False)
     kept = parity(odd)
     got = lax.ppermute(parity(1 - odd), "tp", [(t, t ^ 2) for t in range(TP)])
-    both = jnp.stack([jnp.where(odd == 0, kept, got), jnp.where(odd == 0, got, kept)], axis=1)
+    both = [jnp.where(odd == 0, kept, got), jnp.where(odd == 0, got, kept)]
+    both = jnp.concatenate(both, axis=2)
     down = [at(both, y // 2)]
     for by in (1, 2, 3):
         down.append(y_step(at(both, (y // 2 + by) % (Y // 2)), 2 * by))
@@ -172,14 +174,18 @@
         [gate_weight.reshape(TP, width, ff), up_weight.reshape(TP, width, ff)], axis=2
     )
     gains = ffn_gain.astype(f32).reshape(TP, width)
-    down = jnp.stack(down).reshape(Y, 2, ff, width)
-    down = jnp.where(core == 0, down, down[:, ::-1]).reshape(Y, 2 * ff, width)
 
     def features(steps):
         parts = []
-        for k in steps:
-            chip = (y + k) % Y
-            parts.append(at(down, (y // 2 - chip // 2) % (Y // 2) * 2 + chip % 2))
+        for by in steps:
+            for r in range(Y // 2):
+                for h in range(2):
+                    columns = down[r][:, h * width : (h + 1) * width]
+                    if (h - 2 * r - by) % Y == 0:
+                        even_part = columns
+                    if (h - 2 * r - 1 - by) % Y == 0:
+                        odd_part = columns
+            parts.append(jnp.where(odd == 0, even_part, odd_part))
         return jnp.concatenate(parts, axis=1)
 
     down_first, down_above, down_below = features([4]), features([3, 2, 1]), features([-3, -2, -1, 0])
@@ -202,13 +208,12 @@
         )
         return product, squares
 
-    half = slots // 2
-
     def ring(above, below):
         above = y_step(above, 1)
         below = y_step(below, -1)
         return above, below
 
+    half = slots // 2
     above = below = arrived
     gate_up, squares = products([(arrived, y, core), (swap(arrived), y, 1 - core)])
     for k in range(1, 4):
@@ -229,7 +234,13 @@
     gate_up = gate_up * lax.rsqrt(squares / D + EPSILON)
     hidden = (jax.nn.silu(gate_up[:, :ff]) * gate_up[:, ff:]).astype(bf16)
 
-    hidden = jnp.concatenate([hidden, swap(hidden)], axis=1)
+    other = swap(hidden)
+    hidden = jnp.where(
+        core == 0,
+        jnp.concatenate([hidden, other], axis=1),
+        jnp.concatenate([other, hidden], axis=1),
+    )
+    hidden = lax.optimization_barrier(hidden)
     first = jnp.dot(hidden, down_first, preferred_element_type=f32).astype(bf16)
     part_above = lax.optimization_barrier(jnp.dot(hidden, down_above, preferred_element_type=f32))
     part_below = lax.optimization_barrier(jnp.dot(hidden, down_below, preferred_element_type=f32))

time: 242 us -> 244 us (level)
  the two profiles are of different devices: /device:TPU:56 before, /device:TPU:24 now
where the time goes in v6:
time: 244 us; the launch traced here: 242 us
  starting transfers between devices  117 us (48%)
  waiting for transfers between devices  63.4 us (26%)
  blocking collectives  29.1 us (12%)
  other arithmetic  13.5 us (6%)
  matrix products  13.2 us (5%)
  local copies, waits for them, and re-layouts  4.54 us (2%)
    ppermute x19, starting transfers between devices, y_step(): lax.ppermute(value, 'tp', [(t, (t + 2 * by) % TP) for t in range(TP)])  70.9 us
    all_to_all x4, waiting for transfers between devices, exchange(): lax.all_to_all(value, axis, split_axis=0, concat_axis=0, tiled=True, axis...  33.2 us
    all_gather x1, blocking collectives, body(): attended_all = lax.all_gather(attended, 'tp', axis=0, tiled=True)  29.1 us
    ppermute x19, waiting for transfers between devices, y_step(): lax.ppermute(value, 'tp', [(t, (t + 2 * by) % TP) for t in range(TP)])  25.1 us
    all_to_all x4, starting transfers between devices, exchange(): lax.all_to_all(value, axis, split_axis=0, concat_axis=0, tiled=True, axis...  23.8 us
    ppermute x6, starting transfers between devices, swap(): return lax.ppermute(value, 'tp', [(t, t ^ 1) for t in range(TP)])  12.1 us
    ppermute x2, starting transfers between devices, x_swap(): return lax.ppermute(value, 'sp', [(s, s ^ bit) for s in range(SP)])  8.04 us
  transfers between devices with their start and end apart: 32, of which 16 were waited for; matrix products, arithmetic and copies ran while one was open for 8% of the time, Pallas kernels for 0%

profile of v6, /device:TPU:24, one launch (start us, length us, event | category | flops | bytes accessed | tf_op | source)
XLA Modules:
  0.0 242.3 jit_solution(4749168288332533219)
XLA Ops:
  5.5 3.4 %collective-permute-start = (bf16[256,96]{0,1:T(8,128)(2,1)S(1)}, bf16[256,96]{0,1:T(8,128)(2,1)S(1)}, u32[]{:S(2)}, u32[]{:S(2)}) collective-permute-start(bf16[256,96]{0,1:T(8,128)(2,1)S(1)} %get-tuple-element.118), channel_id=1, source_target_pairs={{0,16},{16,0},{32,48},{48,32},{64,80},{80,64},{96,112},{112,96},{1... | collective-permute-start | bytes 147464 | tf_op jit(solution)/shard_map/ppermute | solution.py:37
  10.0 2.4 collective-permute-start.2
  13.3 10.3 %all-to-all-start = ((bf16[8,160,256]{2,1,0:T(8,128)(2,1)}), bf16[8,160,256]{2,1,0:T(8,128)(2,1)S(1)}, u32[]{:S(2)}, u32[]{:S(2)}) async-start(bf16[8,160,256]{2,1,0:T(8,128)(2,1)} %broadcast_in_dim.9), calls=%async_computation | async-start | bytes 1310720 | tf_op jit(solution)/shard_map/all_to_all | solution.py:27
  24.7 4.6 %collective-permute-start.1 = (bf16[2,256,96]{1,2,0:T(8,128)(2,1)S(1)}, bf16[2,256,96]{1,2,0:T(8,128)(2,1)S(1)}, u32[]{:S(2)}, u32[]{:S(2)}) collective-permute-start(bf16[2,256,96]{1,2,0:T(8,128)(2,1)S(1)} %pad_maximum_fusion.8), channel_id=1, source_target_pairs={{0,32},{16,48},{32,0},{48,16},{64,96},{80,112},{96,64},{112,80},{1... | collective-permute-start | bytes 294920 | tf_op jit(solution)/shard_map/ppermute | solution.py:37
  29.4 3.3 %collective-permute-done.1 = bf16[2,256,96]{1,2,0:T(8,128)(2,1)S(1)} collective-permute-done((bf16[2,256,96]{1,2,0:T(8,128)(2,1)S(1)}, bf16[2,256,96]{1,2,0:T(8,128)(2,1)S(1)}, u32[]{:S(2)}, u32[]{:S(2)}) %collective-permute-start.1) | collective-permute-done | bytes 98336 | tf_op jit(solution)/shard_map/ppermute | solution.py:37
  32.8 10.6 %all-to-all-done = bf16[8,160,256]{2,1,0:T(8,128)(2,1)S(1)} async-done(((bf16[8,160,256]{2,1,0:T(8,128)(2,1)}), bf16[8,160,256]{2,1,0:T(8,128)(2,1)S(1)}, u32[]{:S(2)}, u32[]{:S(2)}) %all-to-all-start) | async-done | bytes 655392 | tf_op jit(solution)/shard_map/all_to_all | solution.py:27
  43.4 1.5 fusion.2
  44.8 2.1 fusion
  46.9 2.2 fusion.5
  50.0 4.0 %all-to-all-start.1 = ((f32[4,72,256]{2,1,0:T(8,128)}), f32[4,72,256]{2,1,0:T(8,128)S(1)}, u32[]{:S(2)}, u32[]{:S(2)}) async-start(f32[4,72,256]{2,1,0:T(8,128)} %pad_maximum_fusion.6), calls=%async_computation.1 | async-start | bytes 589824 | tf_op jit(solution)/shard_map/all_to_all | solution.py:27
  54.2 2.2 collective-permute-start.5
  56.5 5.7 %collective-permute-start.3 = (bf16[512,256]{1,0:T(8,128)(2,1)S(1)}, bf16[512,256]{1,0:T(8,128)(2,1)S(1)}, u32[]{:S(2)}, u32[]{:S(2)}) collective-permute-start(bf16[512,256]{1,0:T(8,128)(2,1)S(1)} %get-tuple-element.69), channel_id=1, source_target_pairs={{0,4},{1,5},{2,6},{3,7},{4,8},{5,9},{6,10},{7,11},{8,12},{9,13},{1... | collective-permute-start | bytes 786440 | tf_op jit(solution)/shard_map/ppermute | solution.py:41
  62.2 5.9 %collective-permute-start.4 = (bf16[512,256]{1,0:T(8,128)(2,1)S(1)}, bf16[512,256]{1,0:T(8,128)(2,1)S(1)}, u32[]{:S(2)}, u32[]{:S(2)}) collective-permute-start(bf16[512,256]{1,0:T(8,128)(2,1)S(1)} %get-tuple-element.70), channel_id=1, source_target_pairs={{0,8},{1,9},{2,10},{3,11},{4,12},{5,13},{6,14},{7,15},{8,0},{9,1},... | collective-permute-start | bytes 786440 | tf_op jit(solution)/shard_map/ppermute | solution.py:41
  68.2 29.1 %all_gather.3 = bf16[1024,256]{1,0:T(8,128)(2,1)S(1)} all-gather(bf16[64,256]{1,0:T(8,128)(2,1)S(1)} %fusion.141), channel_id=1, replica_groups=mesh['sp'=32,'tp'=16] {'tp'}, dimensions={0}, use_global_device_ids=true | all-gather | bytes 557056 | tf_op jit(solution)/shard_map/all_gather | solution.py:162
  98.8 4.9 %all-to-all-start.2 = ((bf16[32,32,128]{2,1,0:T(8,128)(2,1)}), bf16[32,32,128]{2,1,0:T(8,128)(2,1)S(1)}, u32[]{:S(2)}, u32[]{:S(2)}) async-start(bf16[32,32,128]{2,1,0:T(8,128)(2,1)} %bitcast.31), calls=%async_computation.2 | async-start | bytes 524288 | tf_op jit(solution)/shard_map/all_to_all | solution.py:27
  106.0 11.3 %all-to-all-done.2 = bf16[32,32,128]{2,1,0:T(8,128)(2,1)S(1)} async-done(((bf16[32,32,128]{2,1,0:T(8,128)(2,1)}), bf16[32,32,128]{2,1,0:T(8,128)(2,1)S(1)}, u32[]{:S(2)}, u32[]{:S(2)}) %all-to-all-start.2) | async-done | bytes 262176 | tf_op jit(solution)/shard_map/all_to_all | solution.py:27
  117.2 3.1 %collective-permute-start.8 = (bf16[1024,128]{1,0:T(8,128)(2,1)S(1)}, bf16[1024,128]{1,0:T(8,128)(2,1)S(1)}, u32[]{:S(2)}, u32[]{:S(2)}) collective-permute-start(bf16[1024,128]{1,0:T(8,128)(2,1)S(1)} %bitcast.144), channel_id=1, source_target_pairs={{0,14},{1,15},{2,0},{3,1},{4,2},{5,3},{6,4},{7,5},{8,6},{9,7},{10,... | collective-permute-start | bytes 786440 | tf_op jit(solution)/shard_map/ppermute | solution.py:41
  120.3 4.0 %collective-permute-start.7 = (bf16[1024,128]{1,0:T(8,128)(2,1)S(1)}, bf16[1024,128]{1,0:T(8,128)(2,1)S(1)}, u32[]{:S(2)}, u32[]{:S(2)}) collective-permute-start(bf16[1024,128]{1,0:T(8,128)(2,1)S(1)} %bitcast.145), channel_id=1, source_target_pairs={{0,2},{1,3},{2,4},{3,5},{4,6},{5,7},{6,8},{7,9},{8,10},{9,11},{10,... | collective-permute-start | bytes 786440 | tf_op jit(solution)/shard_map/ppermute | solution.py:41
  124.3 1.9 collective-permute-start.6
  126.8 1.8 collective-permute-done.7
  128.6 1.9 collective-permute-start.9
  130.6 3.1 %collective-permute-start.11 = (bf16[1024,128]{1,0:T(8,128)(2,1)S(1)}, bf16[1024,128]{1,0:T(8,128)(2,1)S(1)}, u32[]{:S(2)}, u32[]{:S(2)}) collective-permute-start(bf16[1024,128]{1,0:T(8,128)(2,1)S(1)} %collective-permute-done.8), channel_id=1, source_target_pairs={{0,14},{1,15},{2,0},{3,1},{4,2},{5,3},{6,4},{7,5},{8,6},{9,7},{10,... | collective-permute-start | bytes 786440 | tf_op jit(solution)/shard_map/ppermute | solution.py:41
  133.7 4.0 %collective-permute-start.10 = (bf16[1024,128]{1,0:T(8,128)(2,1)S(1)}, bf16[1024,128]{1,0:T(8,128)(2,1)S(1)}, u32[]{:S(2)}, u32[]{:S(2)}) collective-permute-start(bf16[1024,128]{1,0:T(8,128)(2,1)S(1)} %collective-permute-done.7), channel_id=1, source_target_pairs={{0,2},{1,3},{2,4},{3,5},{4,6},{5,7},{6,8},{7,9},{8,10},{9,11},{10,... | collective-permute-start | bytes 786440 | tf_op jit(solution)/shard_map/ppermute | solution.py:41
  138.8 3.9 %collective-permute-done.11 = bf16[1024,128]{1,0:T(8,128)(2,1)S(1)} collective-permute-done((bf16[1024,128]{1,0:T(8,128)(2,1)S(1)}, bf16[1024,128]{1,0:T(8,128)(2,1)S(1)}, u32[]{:S(2)}, u32[]{:S(2)}) %collective-permute-start.11) | collective-permute-done | bytes 262176 | tf_op jit(solution)/shard_map/ppermute | solution.py:41
  142.7 1.6 collective-permute-done.10
  144.4 1.9 collective-permute-start.12
  146.3 3.6 %collective-permute-start.14 = (bf16[1024,128]{1,0:T(8,128)(2,1)S(1)}, bf16[1024,128]{1,0:T(8,128)(2,1)S(1)}, u32[]{:S(2)}, u32[]{:S(2)}) collective-permute-start(bf16[1024,128]{1,0:T(8,128)(2,1)S(1)} %collective-permute-done.11), channel_id=1, source_target_pairs={{0,14},{1,15},{2,0},{3,1},{4,2},{5,3},{6,4},{7,5},{8,6},{9,7},{10,... | collective-permute-start | bytes 786440 | tf_op jit(solution)/shard_map/ppermute | solution.py:41
  149.9 3.5 %collective-permute-start.13 = (bf16[1024,128]{1,0:T(8,128)(2,1)S(1)}, bf16[1024,128]{1,0:T(8,128)(2,1)S(1)}, u32[]{:S(2)}, u32[]{:S(2)}) collective-permute-start(bf16[1024,128]{1,0:T(8,128)(2,1)S(1)} %collective-permute-done.10), channel_id=1, source_target_pairs={{0,2},{1,3},{2,4},{3,5},{4,6},{5,7},{6,8},{7,9},{8,10},{9,11},{10,... | collective-permute-start | bytes 786440 | tf_op jit(solution)/shard_map/ppermute | solution.py:41
  153.8 4.6 %collective-permute-done.14 = bf16[1024,128]{1,0:T(8,128)(2,1)S(1)} collective-permute-done((bf16[1024,128]{1,0:T(8,128)(2,1)S(1)}, bf16[1024,128]{1,0:T(8,128)(2,1)S(1)}, u32[]{:S(2)}, u32[]{:S(2)}) %collective-permute-start.14) | collective-permute-done | bytes 262176 | tf_op jit(solution)/shard_map/ppermute | solution.py:41
  158.5 2.1 collective-permute-start.17
  160.6 5.1 %collective-permute-start.16 = (bf16[512,128]{1,0:T(8,128)(2,1)S(1)}, bf16[512,128]{1,0:T(8,128)(2,1)S(1)}, u32[]{:S(2)}, u32[]{:S(2)}) collective-permute-start(bf16[512,128]{1,0:T(8,128)(2,1)S(1)} %slice.224), channel_id=1, source_target_pairs={{0,2},{1,3},{2,4},{3,5},{4,6},{5,7},{6,8},{7,9},{8,10},{9,11},{10,... | collective-permute-start | bytes 393224 | tf_op jit(solution)/shard_map/ppermute | solution.py:41
  165.8 1.9 collective-permute-start.15
  169.4 2.4 collective-permute-start.18
  175.6 2.0 collective-permute-start.19
  177.6 1.7 collective-permute-done.19
  180.4 4.0 %collective-permute-start.20 = (bf16[512,128]{1,0:T(8,128)(2,1)S(1)}, bf16[512,128]{1,0:T(8,128)(2,1)S(1)}, u32[]{:S(2)}, u32[]{:S(2)}) collective-permute-start(bf16[512,128]{1,0:T(8,128)(2,1)S(1)} %get-tuple-element.81), channel_id=1, source_target_pairs={{0,2},{1,3},{2,4},{3,5},{4,6},{5,7},{6,8},{7,9},{8,10},{9,11},{10,... | collective-permute-start | bytes 393224 | tf_op jit(solution)/shard_map/ppermute | solution.py:41
  184.4 1.9 collective-permute-start.24
  187.9 5.5 %collective-permute-start.21 = (bf16[1024,128]{1,0:T(8,128)(2,1)S(1)}, bf16[1024,128]{1,0:T(8,128)(2,1)S(1)}, u32[]{:S(2)}, u32[]{:S(2)}) collective-permute-start(bf16[1024,128]{1,0:T(8,128)(2,1)S(1)} %fusion.78), channel_id=1, source_target_pairs={{0,2},{1,3},{2,4},{3,5},{4,6},{5,7},{6,8},{7,9},{8,10},{9,11},{10,... | collective-permute-start | bytes 786440 | tf_op jit(solution)/shard_map/ppermute | solution.py:41
  194.2 1.9 collective-permute-start.25
  196.1 2.4 %collective-permute-done.21 = bf16[1024,128]{1,0:T(8,128)(2,1)S(1)} collective-permute-done((bf16[1024,128]{1,0:T(8,128)(2,1)S(1)}, bf16[1024,128]{1,0:T(8,128)(2,1)S(1)}, u32[]{:S(2)}, u32[]{:S(2)}) %collective-permute-start.21) | collective-permute-done | bytes 262176 | tf_op jit(solution)/shard_map/ppermute | solution.py:41
  198.6 5.6 %collective-permute-start.22 = (bf16[1024,128]{1,0:T(8,128)(2,1)S(1)}, bf16[1024,128]{1,0:T(8,128)(2,1)S(1)}, u32[]{:S(2)}, u32[]{:S(2)}) collective-permute-start(bf16[1024,128]{1,0:T(8,128)(2,1)S(1)} %fusion.77), channel_id=1, source_target_pairs={{0,2},{1,3},{2,4},{3,5},{4,6},{5,7},{6,8},{7,9},{8,10},{9,11},{10,... | collective-permute-start | bytes 786440 | tf_op jit(solution)/shard_map/ppermute | solution.py:41
  204.8 2.1 collective-permute-start.26
  206.9 1.7 collective-permute-done.22
  208.6 5.6 %collective-permute-start.23 = (bf16[1024,128]{1,0:T(8,128)(2,1)S(1)}, bf16[1024,128]{1,0:T(8,128)(2,1)S(1)}, u32[]{:S(2)}, u32[]{:S(2)}) collective-permute-start(bf16[1024,128]{1,0:T(8,128)(2,1)S(1)} %fusion.76), channel_id=1, source_target_pairs={{0,2},{1,3},{2,4},{3,5},{4,6},{5,7},{6,8},{7,9},{8,10},{9,11},{10,... | collective-permute-start | bytes 786440 | tf_op jit(solution)/shard_map/ppermute | solution.py:41
  214.7 1.9 collective-permute-start.27
  218.1 6.1 %collective-permute-done.27 = bf16[1024,128]{1,0:T(8,128)(2,1)S(1)} collective-permute-done((bf16[1024,128]{1,0:T(8,128)(2,1)S(1)}, bf16[1024,128]{1,0:T(8,128)(2,1)S(1)}, u32[]{:S(2)}, u32[]{:S(2)}) %collective-permute-start.27) | collective-permute-done | bytes 262176 | tf_op jit(solution)/shard_map/ppermute | solution.py:41
  225.0 4.6 %all-to-all-start.3 = ((bf16[32,32,128]{2,1,0:T(8,128)(2,1)}), bf16[32,32,128]{2,1,0:T(8,128)(2,1)S(1)}, u32[]{:S(2)}, u32[]{:S(2)}) async-start(bf16[32,32,128]{2,1,0:T(8,128)(2,1)} %bitcast.68), calls=%async_computation.3 | async-start | bytes 524288 | tf_op jit(solution)/shard_map/all_to_all | solution.py:27
  229.7 11.3 %all-to-all-done.3 = bf16[32,32,128]{2,1,0:T(8,128)(2,1)S(1)} async-done(((bf16[32,32,128]{2,1,0:T(8,128)(2,1)}), bf16[32,32,128]{2,1,0:T(8,128)(2,1)S(1)}, u32[]{:S(2)}, u32[]{:S(2)}) %all-to-all-start.3) | async-done | bytes 262176 | tf_op jit(solution)/shard_map/all_to_all | solution.py:27
  (140 shorter events, 28.6 us)
Async XLA Ops:
  0.0 97.3 %copy-start = (bf16[1024,128]{1,0:T(8,128)(2,1)S(1)}, bf16[1024,128]{1,0:T(8,128)(2,1)}, u32[]{:S(2)}) copy-start(bf16[1024,128]{1,0:T(8,128)(2,1)} %param.19) | copy-start | bytes 786436
  1.8 21.9 %copy-start.9 = (s32[256,2]{0,1:T(2,128)S(1)}, s32[256,2]{0,1:T(2,128)}, u32[]{:S(2)}) copy-start(s32[256,2]{0,1:T(2,128)} %param.22) | copy-start | bytes 6148
  5.5 19.2 %collective-permute-start = (bf16[256,96]{0,1:T(8,128)(2,1)S(1)}, bf16[256,96]{0,1:T(8,128)(2,1)S(1)}, u32[]{:S(2)}, u32[]{:S(2)}) collective-permute-start(bf16[256,96]{0,1:T(8,128)(2,1)S(1)} %get-tuple-element.118), channel_id=1, source_target_pairs={{0,16},{16,0},{32,48},{48,32},{64,80},{80,64},{96,112},{112,96},{1... | collective-permute-start | bytes 147464 | tf_op jit(solution)/shard_map/ppermute | solution.py:37
  10.0 43.9 %collective-permute-start.2 = (bf16[4,512,128]{2,1,0:T(8,128)(2,1)S(1)}, bf16[4,512,128]{2,1,0:T(8,128)(2,1)S(1)}, u32[]{:S(2)}, u32[]{:S(2)}) collective-permute-start(bf16[4,512,128]{2,1,0:T(8,128)(2,1)S(1)} %dynamic-slice_bitcast_fusion), channel_id=1, source_target_pairs={{0,2},{1,3},{2,0},{3,1},{4,6},{5,7},{6,4},{7,5},{8,10},{9,11},{10,... | collective-permute-start | bytes 1572872 | tf_op jit(solution)/shard_map/ppermute | solution.py:115
  13.3 30.1 %all-to-all-start = ((bf16[8,160,256]{2,1,0:T(8,128)(2,1)}), bf16[8,160,256]{2,1,0:T(8,128)(2,1)S(1)}, u32[]{:S(2)}, u32[]{:S(2)}) async-start(bf16[8,160,256]{2,1,0:T(8,128)(2,1)} %broadcast_in_dim.9), calls=%async_computation | async-start | bytes 1310720 | tf_op jit(solution)/shard_map/all_to_all | solution.py:27
  24.7 8.0 %collective-permute-start.1 = (bf16[2,256,96]{1,2,0:T(8,128)(2,1)S(1)}, bf16[2,256,96]{1,2,0:T(8,128)(2,1)S(1)}, u32[]{:S(2)}, u32[]{:S(2)}) collective-permute-start(bf16[2,256,96]{1,2,0:T(8,128)(2,1)S(1)} %pad_maximum_fusion.8), channel_id=1, source_target_pairs={{0,32},{16,48},{32,0},{48,16},{64,96},{80,112},{96,64},{112,80},{1... | collective-permute-start | bytes 294920 | tf_op jit(solution)/shard_map/ppermute | solution.py:37
  49.1 4.9 %copy-start.1 = (bf16[1,4096,128]{2,1,0:T(8,128)(2,1)S(1)}, bf16[1,4096,128]{2,1,0:T(8,128)(2,1)}, u32[]{:S(2)}) copy-start(bf16[1,4096,128]{2,1,0:T(8,128)(2,1)} %param.27) | copy-start | bytes 3145732
  50.0 18.2 %all-to-all-start.1 = ((f32[4,72,256]{2,1,0:T(8,128)}), f32[4,72,256]{2,1,0:T(8,128)S(1)}, u32[]{:S(2)}, u32[]{:S(2)}) async-start(f32[4,72,256]{2,1,0:T(8,128)} %pad_maximum_fusion.6), calls=%async_computation.1 | async-start | bytes 589824 | tf_op jit(solution)/shard_map/all_to_all | solution.py:27
  54.1 43.3 %copy-start.7 = (bf16[256,128]{1,0:T(8,128)(2,1)S(1)}, bf16[256,128]{1,0:T(8,128)(2,1)}, u32[]{:S(2)}) copy-start(bf16[256,128]{1,0:T(8,128)(2,1)} %param.20) | copy-start | bytes 196612
  54.2 44.5 %collective-permute-start.5 = (bf16[512,256]{1,0:T(8,128)(2,1)S(1)}, bf16[512,256]{1,0:T(8,128)(2,1)S(1)}, u32[]{:S(2)}, u32[]{:S(2)}) collective-permute-start(bf16[512,256]{1,0:T(8,128)(2,1)S(1)} %get-tuple-element.67), channel_id=1, source_target_pairs={{0,12},{1,13},{2,14},{3,15},{4,0},{5,1},{6,2},{7,3},{8,4},{9,5},{1... | collective-permute-start | bytes 786440 | tf_op jit(solution)/shard_map/ppermute | solution.py:41
  56.5 42.3 %collective-permute-start.3 = (bf16[512,256]{1,0:T(8,128)(2,1)S(1)}, bf16[512,256]{1,0:T(8,128)(2,1)S(1)}, u32[]{:S(2)}, u32[]{:S(2)}) collective-permute-start(bf16[512,256]{1,0:T(8,128)(2,1)S(1)} %get-tuple-element.69), channel_id=1, source_target_pairs={{0,4},{1,5},{2,6},{3,7},{4,8},{5,9},{6,10},{7,11},{8,12},{9,13},{1... | collective-permute-start | bytes 786440 | tf_op jit(solution)/shard_map/ppermute | solution.py:41
  62.2 36.6 %collective-permute-start.4 = (bf16[512,256]{1,0:T(8,128)(2,1)S(1)}, bf16[512,256]{1,0:T(8,128)(2,1)S(1)}, u32[]{:S(2)}, u32[]{:S(2)}) collective-permute-start(bf16[512,256]{1,0:T(8,128)(2,1)S(1)} %get-tuple-element.70), channel_id=1, source_target_pairs={{0,8},{1,9},{2,10},{3,11},{4,12},{5,13},{6,14},{7,15},{8,0},{9,1},... | collective-permute-start | bytes 786440 | tf_op jit(solution)/shard_map/ppermute | solution.py:41
  97.7 6.8 %copy-start.5 = (bf16[256,128]{1,0:T(8,128)(2,1)}, bf16[256,128]{1,0:T(8,128)(2,1)S(1)}, u32[]{:S(2)}) copy-start(bf16[256,128]{1,0:T(8,128)(2,1)S(1)} %fusion.10) | copy-start | bytes 196612
  98.8 18.5 %all-to-all-start.2 = ((bf16[32,32,128]{2,1,0:T(8,128)(2,1)}), bf16[32,32,128]{2,1,0:T(8,128)(2,1)S(1)}, u32[]{:S(2)}, u32[]{:S(2)}) async-start(bf16[32,32,128]{2,1,0:T(8,128)(2,1)} %bitcast.31), calls=%async_computation.2 | async-start | bytes 524288 | tf_op jit(solution)/shard_map/all_to_all | solution.py:27
  103.7 1.3 copy-start.2
  103.7 1.6 copy-start.3
  105.3 0.7 copy-start.10
  117.2 9.6 %collective-permute-start.8 = (bf16[1024,128]{1,0:T(8,128)(2,1)S(1)}, bf16[1024,128]{1,0:T(8,128)(2,1)S(1)}, u32[]{:S(2)}, u32[]{:S(2)}) collective-permute-start(bf16[1024,128]{1,0:T(8,128)(2,1)S(1)} %bitcast.144), channel_id=1, source_target_pairs={{0,14},{1,15},{2,0},{3,1},{4,2},{5,3},{6,4},{7,5},{8,6},{9,7},{10,... | collective-permute-start | bytes 786440 | tf_op jit(solution)/shard_map/ppermute | solution.py:41
  120.3 8.3 %collective-permute-start.7 = (bf16[1024,128]{1,0:T(8,128)(2,1)S(1)}, bf16[1024,128]{1,0:T(8,128)(2,1)S(1)}, u32[]{:S(2)}, u32[]{:S(2)}) collective-permute-start(bf16[1024,128]{1,0:T(8,128)(2,1)S(1)} %bitcast.145), channel_id=1, source_target_pairs={{0,2},{1,3},{2,4},{3,5},{4,6},{5,7},{6,8},{7,9},{8,10},{9,11},{10,... | collective-permute-start | bytes 786440 | tf_op jit(solution)/shard_map/ppermute | solution.py:41
  124.3 13.6 %collective-permute-start.6 = (bf16[1024,128]{1,0:T(8,128)(2,1)S(1)}, bf16[1024,128]{1,0:T(8,128)(2,1)S(1)}, u32[]{:S(2)}, u32[]{:S(2)}) collective-permute-start(bf16[1024,128]{1,0:T(8,128)(2,1)S(1)} %bitcast.146), channel_id=1, source_target_pairs={{0,1},{1,0},{2,3},{3,2},{4,5},{5,4},{6,7},{7,6},{8,9},{9,8},{10,11... | collective-permute-start | bytes 786440 | tf_op jit(solution)/shard_map/ppermute | solution.py:33
  128.6 39.5 %collective-permute-start.9 = (bf16[1024,256]{1,0:T(8,128)(2,1)S(1)}, bf16[1024,256]{1,0:T(8,128)(2,1)S(1)}, u32[]{:S(2)}, u32[]{:S(2)}) collective-permute-start(bf16[1024,256]{1,0:T(8,128)(2,1)S(1)} %pad_maximum_fusion.2), channel_id=1, source_target_pairs={{0,1},{1,0},{2,3},{3,2},{4,5},{5,4},{6,7},{7,6},{8,9},{9,8},{10,11... | collective-permute-start | bytes 1572872 | tf_op jit(solution)/shard_map/ppermute | solution.py:33
  130.6 12.1 %collective-permute-start.11 = (bf16[1024,128]{1,0:T(8,128)(2,1)S(1)}, bf16[1024,128]{1,0:T(8,128)(2,1)S(1)}, u32[]{:S(2)}, u32[]{:S(2)}) collective-permute-start(bf16[1024,128]{1,0:T(8,128)(2,1)S(1)} %collective-permute-done.8), channel_id=1, source_target_pairs={{0,14},{1,15},{2,0},{3,1},{4,2},{5,3},{6,4},{7,5},{8,6},{9,7},{10,... | collective-permute-start | bytes 786440 | tf_op jit(solution)/shard_map/ppermute | solution.py:41
  133.7 10.6 %collective-permute-start.10 = (bf16[1024,128]{1,0:T(8,128)(2,1)S(1)}, bf16[1024,128]{1,0:T(8,128)(2,1)S(1)}, u32[]{:S(2)}, u32[]{:S(2)}) collective-permute-start(bf16[1024,128]{1,0:T(8,128)(2,1)S(1)} %collective-permute-done.7), channel_id=1, source_target_pairs={{0,2},{1,3},{2,4},{3,5},{4,6},{5,7},{6,8},{7,9},{8,10},{9,11},{10,... | collective-permute-start | bytes 786440 | tf_op jit(solution)/shard_map/ppermute | solution.py:41
  144.4 27.6 %collective-permute-start.12 = (bf16[1024,256]{1,0:T(8,128)(2,1)S(1)}, bf16[1024,256]{1,0:T(8,128)(2,1)S(1)}, u32[]{:S(2)}, u32[]{:S(2)}) collective-permute-start(bf16[1024,256]{1,0:T(8,128)(2,1)S(1)} %pad_maximum_fusion.3), channel_id=1, source_target_pairs={{0,1},{1,0},{2,3},{3,2},{4,5},{5,4},{6,7},{7,6},{8,9},{9,8},{10,11... | collective-permute-start | bytes 1572872 | tf_op jit(solution)/shard_map/ppermute | solution.py:33
  146.3 12.1 %collective-permute-start.14 = (bf16[1024,128]{1,0:T(8,128)(2,1)S(1)}, bf16[1024,128]{1,0:T(8,128)(2,1)S(1)}, u32[]{:S(2)}, u32[]{:S(2)}) collective-permute-start(bf16[1024,128]{1,0:T(8,128)(2,1)S(1)} %collective-permute-done.11), channel_id=1, source_target_pairs={{0,14},{1,15},{2,0},{3,1},{4,2},{5,3},{6,4},{7,5},{8,6},{9,7},{10,... | collective-permute-start | bytes 786440 | tf_op jit(solution)/shard_map/ppermute | solution.py:41
  149.9 10.6 %collective-permute-start.13 = (bf16[1024,128]{1,0:T(8,128)(2,1)S(1)}, bf16[1024,128]{1,0:T(8,128)(2,1)S(1)}, u32[]{:S(2)}, u32[]{:S(2)}) collective-permute-start(bf16[1024,128]{1,0:T(8,128)(2,1)S(1)} %collective-permute-done.10), channel_id=1, source_target_pairs={{0,2},{1,3},{2,4},{3,5},{4,6},{5,7},{6,8},{7,9},{8,10},{9,11},{10,... | collective-permute-start | bytes 786440 | tf_op jit(solution)/shard_map/ppermute | solution.py:41
  158.5 10.9 %collective-permute-start.17 = (bf16[512,128]{1,0:T(8,128)(2,1)S(1)}, bf16[512,128]{1,0:T(8,128)(2,1)S(1)}, u32[]{:S(2)}, u32[]{:S(2)}) collective-permute-start(bf16[512,128]{1,0:T(8,128)(2,1)S(1)} %slice.225), channel_id=1, source_target_pairs={{0,14},{1,15},{2,0},{3,1},{4,2},{5,3},{6,4},{7,5},{8,6},{9,7},{10,... | collective-permute-start | bytes 393224 | tf_op jit(solution)/shard_map/ppermute | solution.py:41
  160.6 8.7 %collective-permute-start.16 = (bf16[512,128]{1,0:T(8,128)(2,1)S(1)}, bf16[512,128]{1,0:T(8,128)(2,1)S(1)}, u32[]{:S(2)}, u32[]{:S(2)}) collective-permute-start(bf16[512,128]{1,0:T(8,128)(2,1)S(1)} %slice.224), channel_id=1, source_target_pairs={{0,2},{1,3},{2,4},{3,5},{4,6},{5,7},{6,8},{7,9},{8,10},{9,11},{10,... | collective-permute-start | bytes 393224 | tf_op jit(solution)/shard_map/ppermute | solution.py:41
  165.8 7.6 %collective-permute-start.15 = (bf16[1024,256]{1,0:T(8,128)(2,1)S(1)}, bf16[1024,256]{1,0:T(8,128)(2,1)S(1)}, u32[]{:S(2)}, u32[]{:S(2)}) collective-permute-start(bf16[1024,256]{1,0:T(8,128)(2,1)S(1)} %pad_maximum_fusion.4), channel_id=1, source_target_pairs={{0,1},{1,0},{2,3},{3,2},{4,5},{5,4},{6,7},{7,6},{8,9},{9,8},{10,11... | collective-permute-start | bytes 1572872 | tf_op jit(solution)/shard_map/ppermute | solution.py:33
  169.4 3.8 %collective-permute-start.18 = (bf16[1024,128]{1,0:T(8,128)(2,1)S(1)}, bf16[1024,128]{1,0:T(8,128)(2,1)S(1)}, u32[]{:S(2)}, u32[]{:S(2)}) collective-permute-start(bf16[1024,128]{1,0:T(8,128)(2,1)S(1)} %constant_dynamic-update-slice_fusion), channel_id=1, source_target_pairs={{0,1},{1,0},{2,3},{3,2},{4,5},{5,4},{6,7},{7,6},{8,9},{9,8},{10,11... | collective-permute-start | bytes 786440 | tf_op jit(solution)/shard_map/ppermute | solution.py:33
  175.2 4.6 %copy-start.4 = (bf16[512,128]{1,0:T(8,128)(2,1)S(1)}, bf16[512,128]{1,0:T(8,128)(2,1)}, u32[]{:S(2)}) copy-start(bf16[512,128]{1,0:T(8,128)(2,1)} %get-tuple-element.39) | copy-start | bytes 393220
  175.6 3.8 %collective-permute-start.19 = (bf16[1024,256]{0,1:T(8,128)(2,1)S(1)}, bf16[1024,256]{0,1:T(8,128)(2,1)S(1)}, u32[]{:S(2)}, u32[]{:S(2)}) collective-permute-start(bf16[1024,256]{0,1:T(8,128)(2,1)S(1)} %fusion.13), channel_id=1, source_target_pairs={{0,1},{1,0},{2,3},{3,2},{4,5},{5,4},{6,7},{7,6},{8,9},{9,8},{10,11... | collective-permute-start | bytes 1572872 | tf_op jit(solution)/shard_map/ppermute | solution.py:33
  180.4 7.4 %collective-permute-start.20 = (bf16[512,128]{1,0:T(8,128)(2,1)S(1)}, bf16[512,128]{1,0:T(8,128)(2,1)S(1)}, u32[]{:S(2)}, u32[]{:S(2)}) collective-permute-start(bf16[512,128]{1,0:T(8,128)(2,1)S(1)} %get-tuple-element.81), channel_id=1, source_target_pairs={{0,2},{1,3},{2,4},{3,5},{4,6},{5,7},{6,8},{7,9},{8,10},{9,11},{10,... | collective-permute-start | bytes 393224 | tf_op jit(solution)/shard_map/ppermute | solution.py:41
  184.4 9.7 %collective-permute-start.24 = (bf16[512,128]{1,0:T(8,128)(2,1)S(1)}, bf16[512,128]{1,0:T(8,128)(2,1)S(1)}, u32[]{:S(2)}, u32[]{:S(2)}) collective-permute-start(bf16[512,128]{1,0:T(8,128)(2,1)S(1)} %get-tuple-element.82), channel_id=1, source_target_pairs={{0,14},{1,15},{2,0},{3,1},{4,2},{5,3},{6,4},{7,5},{8,6},{9,7},{10,... | collective-permute-start | bytes 393224 | tf_op jit(solution)/shard_map/ppermute | solution.py:41
  187.9 10.7 %collective-permute-start.21 = (bf16[1024,128]{1,0:T(8,128)(2,1)S(1)}, bf16[1024,128]{1,0:T(8,128)(2,1)S(1)}, u32[]{:S(2)}, u32[]{:S(2)}) collective-permute-start(bf16[1024,128]{1,0:T(8,128)(2,1)S(1)} %fusion.78), channel_id=1, source_target_pairs={{0,2},{1,3},{2,4},{3,5},{4,6},{5,7},{6,8},{7,9},{8,10},{9,11},{10,... | collective-permute-start | bytes 786440 | tf_op jit(solution)/shard_map/ppermute | solution.py:41
  194.2 10.5 %collective-permute-start.25 = (bf16[1024,128]{1,0:T(8,128)(2,1)S(1)}, bf16[1024,128]{1,0:T(8,128)(2,1)S(1)}, u32[]{:S(2)}, u32[]{:S(2)}) collective-permute-start(bf16[1024,128]{1,0:T(8,128)(2,1)S(1)} %fusion.75), channel_id=1, source_target_pairs={{0,14},{1,15},{2,0},{3,1},{4,2},{5,3},{6,4},{7,5},{8,6},{9,7},{10,... | collective-permute-start | bytes 786440 | tf_op jit(solution)/shard_map/ppermute | solution.py:41
  198.6 10.0 %collective-permute-start.22 = (bf16[1024,128]{1,0:T(8,128)(2,1)S(1)}, bf16[1024,128]{1,0:T(8,128)(2,1)S(1)}, u32[]{:S(2)}, u32[]{:S(2)}) collective-permute-start(bf16[1024,128]{1,0:T(8,128)(2,1)S(1)} %fusion.77), channel_id=1, source_target_pairs={{0,2},{1,3},{2,4},{3,5},{4,6},{5,7},{6,8},{7,9},{8,10},{9,11},{10,... | collective-permute-start | bytes 786440 | tf_op jit(solution)/shard_map/ppermute | solution.py:41
  204.8 24.8 %copy-start.8 = (f32[256,2]{0,1:T(2,128)S(1)}, f32[256,2]{0,1:T(2,128)}, u32[]{:S(2)}) copy-start(f32[256,2]{0,1:T(2,128)} %param.23) | copy-start | bytes 6148
  204.8 24.8 %copy-start.11 = (f32[256]{0:T(256)S(1)}, f32[256]{0:T(256)}, u32[]{:S(2)}) copy-start(f32[256]{0:T(256)} %param.24) | copy-start | bytes 3076
  204.8 36.2 %copy-start.6 = (bf16[256,128]{1,0:T(8,128)(2,1)S(1)}, bf16[256,128]{1,0:T(8,128)(2,1)}, u32[]{:S(2)}) copy-start(bf16[256,128]{1,0:T(8,128)(2,1)} %copy-done.5) | copy-start | bytes 196612
  204.8 9.8 %collective-permute-start.26 = (bf16[1024,128]{1,0:T(8,128)(2,1)S(1)}, bf16[1024,128]{1,0:T(8,128)(2,1)S(1)}, u32[]{:S(2)}, u32[]{:S(2)}) collective-permute-start(bf16[1024,128]{1,0:T(8,128)(2,1)S(1)} %fusion.74), channel_id=1, source_target_pairs={{0,14},{1,15},{2,0},{3,1},{4,2},{5,3},{6,4},{7,5},{8,6},{9,7},{10,... | collective-permute-start | bytes 786440 | tf_op jit(solution)/shard_map/ppermute | solution.py:41
  208.6 9.5 %collective-permute-start.23 = (bf16[1024,128]{1,0:T(8,128)(2,1)S(1)}, bf16[1024,128]{1,0:T(8,128)(2,1)S(1)}, u32[]{:S(2)}, u32[]{:S(2)}) collective-permute-start(bf16[1024,128]{1,0:T(8,128)(2,1)S(1)} %fusion.76), channel_id=1, source_target_pairs={{0,2},{1,3},{2,4},{3,5},{4,6},{5,7},{6,8},{7,9},{8,10},{9,11},{10,... | collective-permute-start | bytes 786440 | tf_op jit(solution)/shard_map/ppermute | solution.py:41
  214.7 9.5 %collective-permute-start.27 = (bf16[1024,128]{1,0:T(8,128)(2,1)S(1)}, bf16[1024,128]{1,0:T(8,128)(2,1)S(1)}, u32[]{:S(2)}, u32[]{:S(2)}) collective-permute-start(bf16[1024,128]{1,0:T(8,128)(2,1)S(1)} %fusion.73), channel_id=1, source_target_pairs={{0,14},{1,15},{2,0},{3,1},{4,2},{5,3},{6,4},{7,5},{8,6},{9,7},{10,... | collective-permute-start | bytes 786440 | tf_op jit(solution)/shard_map/ppermute | solution.py:41
  225.0 16.0 %all-to-all-start.3 = ((bf16[32,32,128]{2,1,0:T(8,128)(2,1)}), bf16[32,32,128]{2,1,0:T(8,128)(2,1)S(1)}, u32[]{:S(2)}, u32[]{:S(2)}) async-start(bf16[32,32,128]{2,1,0:T(8,128)(2,1)} %bitcast.68), calls=%async_computation.3 | async-start | bytes 524288 | tf_op jit(solution)/shard_map/all_to_all | solution.py:27

commit v7 on v6

--- a/solution.py
+++ b/solution.py
@@ -110,14 +110,12 @@
 
     down = down_weight.reshape(Y // 2, 2, 2 * ff, width)
     odd = y % 2
-    parity = lambda one: lax.dynamic_index_in_dim(down, one, 1, keepdims=False)
-    kept = parity(odd)
-    got = lax.ppermute(parity(1 - odd), "tp", [(t, t ^ 2) for t in range(TP)])
-    both = [jnp.where(odd == 0, kept, got), jnp.where(odd == 0, got, kept)]
-    both = jnp.concatenate(both, axis=2)
-    down = [at(both, y // 2)]
+    parts = [at(down, y // 2)]
     for by in (1, 2, 3):
-        down.append(y_step(at(both, (y // 2 + by) % (Y // 2)), 2 * by))
+        parts.append(y_step(at(down, (y // 2 + by) % (Y // 2)), 2 * by))
+    kept = [at(part, odd) for part in parts]
+    given = jnp.stack([at(part, 1 - odd) for part in parts])
+    got = lax.ppermute(given, "tp", [(t, t ^ 2) for t in range(TP)])
 
     experts = SP
     capacity = 2 * tokens * TOP // experts
@@ -166,8 +164,8 @@
     mixed = (residual.astype(f32) + projected).astype(bf16)
 
     sent = lax.dot_general(placed, mixed, (((0,), (0,)), ((), ())), preferred_element_type=f32)
-    sent, gate_weight, up_weight, ffn_gain, down = lax.optimization_barrier(
-        (sent.astype(bf16), gate_weight, up_weight, ffn_gain, down)
+    sent, gate_weight, up_weight, ffn_gain, kept, got = lax.optimization_barrier(
+        (sent.astype(bf16), gate_weight, up_weight, ffn_gain, kept, got)
     )
     arrived = exchange(sent.reshape(SP, capacity, width), "sp")
     gate_up_weight = jnp.concatenate(
@@ -178,14 +176,12 @@
     def features(steps):
         parts = []
         for by in steps:
-            for r in range(Y // 2):
-                for h in range(2):
-                    columns = down[r][:, h * width : (h + 1) * width]
-                    if (h - 2 * r - by) % Y == 0:
-                        even_part = columns
-                    if (h - 2 * r - 1 - by) % Y == 0:
-                        odd_part = columns
-            parts.append(jnp.where(odd == 0, even_part, odd_part))
+            if by % 2 == 0:
+                parts.append(kept[-by // 2 % (Y // 2)])
+            else:
+                even_part = got[(1 - by) // 2 % (Y // 2)]
+                odd_part = got[(-1 - by) // 2 % (Y // 2)]
+                parts.append(jnp.where(odd == 0, even_part, odd_part))
         return jnp.concatenate(parts, axis=1)
 
     down_first, down_above, down_below = features([4]), features([3, 2, 1]), features([-3, -2, -1, 0])

time: 244 us -> 242 us (level)
  the two profiles are of different devices: /device:TPU:24 before, /device:TPU:56 now
where the time goes in v7:
time: 242 us; the launch traced here: 240 us
  starting transfers between devices  128 us (53%)
  waiting for transfers between devices  53.8 us (22%)
  blocking collectives  22.5 us (9%)
  other arithmetic  14.3 us (6%)
  matrix products  13.2 us (5%)
  local copies, waits for them, and re-layouts  6.69 us (3%)
    ppermute x19, starting transfers between devices, y_step(): lax.ppermute(value, 'tp', [(t, (t + 2 * by) % TP) for t in range(TP)])  70.3 us
    all_to_all x4, starting transfers between devices, exchange(): lax.all_to_all(value, axis, split_axis=0, concat_axis=0, tiled=True, axis...  28.9 us
    ppermute x19, waiting for transfers between devices, y_step(): lax.ppermute(value, 'tp', [(t, (t + 2 * by) % TP) for t in range(TP)])  26.1 us
    all_to_all x4, waiting for transfers between devices, exchange(): lax.all_to_all(value, axis, split_axis=0, concat_axis=0, tiled=True, axis...  22.9 us
    all_gather x1, blocking collectives, body(): attended_all = lax.all_gather(attended, 'tp', axis=0, tiled=True)  22.5 us
    ppermute x6, starting transfers between devices, swap(): return lax.ppermute(value, 'tp', [(t, t ^ 1) for t in range(TP)])  12.3 us
    ppermute x1, starting transfers between devices, body(): got = lax.ppermute(given, 'tp', [(t, t ^ 2) for t in range(TP)])  8.58 us
    ppermute x2, starting transfers between devices, x_swap(): return lax.ppermute(value, 'sp', [(s, s ^ bit) for s in range(SP)])  8.04 us
  transfers between devices with their start and end apart: 32, of which 16 were waited for; matrix products, arithmetic and copies ran while one was open for 10% of the time, Pallas kernels for 0%

profile of v7, /device:TPU:56, one launch (start us, length us, event | category | flops | bytes accessed | tf_op | source)
XLA Modules:
  0.0 240.0 jit_solution(10011152983823476352)
XLA Ops:
  5.6 3.4 %collective-permute-start = (bf16[256,96]{0,1:T(8,128)(2,1)S(1)}, bf16[256,96]{0,1:T(8,128)(2,1)S(1)}, u32[]{:S(2)}, u32[]{:S(2)}) collective-permute-start(bf16[256,96]{0,1:T(8,128)(2,1)S(1)} %get-tuple-element.121), channel_id=1, source_target_pairs={{0,16},{16,0},{32,48},{48,32},{64,80},{80,64},{96,112},{112,96},{1... | collective-permute-start | bytes 147464 | tf_op jit(solution)/shard_map/ppermute | solution.py:37
  9.9 10.3 %all-to-all-start = ((bf16[8,160,256]{2,1,0:T(8,128)(2,1)}), bf16[8,160,256]{2,1,0:T(8,128)(2,1)S(1)}, u32[]{:S(2)}, u32[]{:S(2)}) async-start(bf16[8,160,256]{2,1,0:T(8,128)(2,1)} %broadcast_in_dim.9), calls=%async_computation | async-start | bytes 1310720 | tf_op jit(solution)/shard_map/all_to_all | solution.py:27
  21.0 4.0 %collective-permute-start.4 = (bf16[2,512,128]{2,1,0:T(8,128)(2,1)}, bf16[2,512,128]{2,1,0:T(8,128)(2,1)}, u32[]{:S(2)}, u32[]{:S(2)}) collective-permute-start(bf16[2,512,128]{2,1,0:T(8,128)(2,1)} %get-tuple-element.69), channel_id=1, source_target_pairs={{0,12},{1,13},{2,14},{3,15},{4,0},{5,1},{6,2},{7,3},{8,4},{9,5},{1... | collective-permute-start | bytes 786440 | tf_op jit(solution)/shard_map/ppermute | solution.py:41
  25.0 2.9 %collective-permute-start.3 = (bf16[2,512,128]{2,1,0:T(8,128)(2,1)S(1)}, bf16[2,512,128]{2,1,0:T(8,128)(2,1)}, u32[]{:S(2)}, u32[]{:S(2)}) collective-permute-start(bf16[2,512,128]{2,1,0:T(8,128)(2,1)S(1)} %get-tuple-element.70), channel_id=1, source_target_pairs={{0,8},{1,9},{2,10},{3,11},{4,12},{5,13},{6,14},{7,15},{8,0},{9,1},... | collective-permute-start | bytes 786440 | tf_op jit(solution)/shard_map/ppermute | solution.py:41
  27.9 5.7 %collective-permute-start.2 = (bf16[2,512,128]{2,1,0:T(8,128)(2,1)S(1)}, bf16[2,512,128]{2,1,0:T(8,128)(2,1)}, u32[]{:S(2)}, u32[]{:S(2)}) collective-permute-start(bf16[2,512,128]{2,1,0:T(8,128)(2,1)S(1)} %get-tuple-element.71), channel_id=1, source_target_pairs={{0,4},{1,5},{2,6},{3,7},{4,8},{5,9},{6,10},{7,11},{8,12},{9,13},{1... | collective-permute-start | bytes 786440 | tf_op jit(solution)/shard_map/ppermute | solution.py:41
  34.4 4.6 %collective-permute-start.1 = (bf16[2,256,96]{1,2,0:T(8,128)(2,1)S(1)}, bf16[2,256,96]{1,2,0:T(8,128)(2,1)S(1)}, u32[]{:S(2)}, u32[]{:S(2)}) collective-permute-start(bf16[2,256,96]{1,2,0:T(8,128)(2,1)S(1)} %pad_maximum_fusion.9), channel_id=1, source_target_pairs={{0,32},{16,48},{32,0},{48,16},{64,96},{80,112},{96,64},{112,80},{1... | collective-permute-start | bytes 294920 | tf_op jit(solution)/shard_map/ppermute | solution.py:37
  39.4 3.0 %collective-permute-done.1 = bf16[2,256,96]{1,2,0:T(8,128)(2,1)S(1)} collective-permute-done((bf16[2,256,96]{1,2,0:T(8,128)(2,1)S(1)}, bf16[2,256,96]{1,2,0:T(8,128)(2,1)S(1)}, u32[]{:S(2)}, u32[]{:S(2)}) %collective-permute-start.1) | collective-permute-done | bytes 98336 | tf_op jit(solution)/shard_map/ppermute | solution.py:37
  42.5 1.8 collective-permute-done.4
  45.3 1.6 constant_dynamic-slice_fusion.17
  46.9 1.5 fusion.2
  48.4 2.1 fusion
  50.5 2.2 fusion.5
  53.6 4.0 %all-to-all-start.1 = ((f32[4,72,256]{2,1,0:T(8,128)}), f32[4,72,256]{2,1,0:T(8,128)S(1)}, u32[]{:S(2)}, u32[]{:S(2)}) async-start(f32[4,72,256]{2,1,0:T(8,128)} %pad_maximum_fusion.7), calls=%async_computation.1 | async-start | bytes 589824 | tf_op jit(solution)/shard_map/all_to_all | solution.py:27
  58.6 8.6 %collective-permute-start.5 = (bf16[4,512,128]{2,1,0:T(8,128)(2,1)S(1)}, bf16[4,512,128]{2,1,0:T(8,128)(2,1)S(1)}, u32[]{:S(2)}, u32[]{:S(2)}) collective-permute-start(bf16[4,512,128]{2,1,0:T(8,128)(2,1)S(1)} %pad_maximum_fusion.1), channel_id=1, source_target_pairs={{0,2},{1,3},{2,0},{3,1},{4,6},{5,7},{6,4},{7,5},{8,10},{9,11},{10,... | collective-permute-start | bytes 1572872 | tf_op jit(solution)/shard_map/ppermute | solution.py:118
  67.4 22.5 %all_gather.3 = bf16[1024,256]{1,0:T(8,128)(2,1)S(1)} all-gather(bf16[64,256]{1,0:T(8,128)(2,1)S(1)} %fusion.133), channel_id=1, replica_groups=mesh['sp'=32,'tp'=16] {'tp'}, dimensions={0}, use_global_device_ids=true | all-gather | bytes 557056 | tf_op jit(solution)/shard_map/all_gather | solution.py:160
  91.3 10.1 %all-to-all-start.2 = ((bf16[32,32,128]{2,1,0:T(8,128)(2,1)}), bf16[32,32,128]{2,1,0:T(8,128)(2,1)S(1)}, u32[]{:S(2)}, u32[]{:S(2)}) async-start(bf16[32,32,128]{2,1,0:T(8,128)(2,1)} %bitcast.33), calls=%async_computation.2 | async-start | bytes 524288 | tf_op jit(solution)/shard_map/all_to_all | solution.py:27
  101.6 1.7 pad_maximum_fusion
  103.3 11.6 %all-to-all-done.2 = bf16[32,32,128]{2,1,0:T(8,128)(2,1)S(1)} async-done(((bf16[32,32,128]{2,1,0:T(8,128)(2,1)}), bf16[32,32,128]{2,1,0:T(8,128)(2,1)S(1)}, u32[]{:S(2)}, u32[]{:S(2)}) %all-to-all-start.2) | async-done | bytes 262176 | tf_op jit(solution)/shard_map/all_to_all | solution.py:27
  114.9 1.9 collective-permute-start.8
  116.8 5.1 %collective-permute-start.7 = (bf16[1024,128]{1,0:T(8,128)(2,1)S(1)}, bf16[1024,128]{1,0:T(8,128)(2,1)S(1)}, u32[]{:S(2)}, u32[]{:S(2)}) collective-permute-start(bf16[1024,128]{1,0:T(8,128)(2,1)S(1)} %bitcast.158), channel_id=1, source_target_pairs={{0,2},{1,3},{2,4},{3,5},{4,6},{5,7},{6,8},{7,9},{8,10},{9,11},{10,... | collective-permute-start | bytes 786440 | tf_op jit(solution)/shard_map/ppermute | solution.py:41
  122.0 1.9 collective-permute-start.6
  125.9 1.9 collective-permute-start.9
  127.8 3.2 %collective-permute-start.11 = (bf16[1024,128]{1,0:T(8,128)(2,1)S(1)}, bf16[1024,128]{1,0:T(8,128)(2,1)S(1)}, u32[]{:S(2)}, u32[]{:S(2)}) collective-permute-start(bf16[1024,128]{1,0:T(8,128)(2,1)S(1)} %collective-permute-done.8), channel_id=1, source_target_pairs={{0,14},{1,15},{2,0},{3,1},{4,2},{5,3},{6,4},{7,5},{8,6},{9,7},{10,... | collective-permute-start | bytes 786440 | tf_op jit(solution)/shard_map/ppermute | solution.py:41
  131.0 4.3 %collective-permute-start.10 = (bf16[1024,128]{1,0:T(8,128)(2,1)S(1)}, bf16[1024,128]{1,0:T(8,128)(2,1)S(1)}, u32[]{:S(2)}, u32[]{:S(2)}) collective-permute-start(bf16[1024,128]{1,0:T(8,128)(2,1)S(1)} %collective-permute-done.7), channel_id=1, source_target_pairs={{0,2},{1,3},{2,4},{3,5},{4,6},{5,7},{6,8},{7,9},{8,10},{9,11},{10,... | collective-permute-start | bytes 786440 | tf_op jit(solution)/shard_map/ppermute | solution.py:41
  136.5 3.9 %collective-permute-done.11 = bf16[1024,128]{1,0:T(8,128)(2,1)S(1)} collective-permute-done((bf16[1024,128]{1,0:T(8,128)(2,1)S(1)}, bf16[1024,128]{1,0:T(8,128)(2,1)S(1)}, u32[]{:S(2)}, u32[]{:S(2)}) %collective-permute-start.11) | collective-permute-done | bytes 262176 | tf_op jit(solution)/shard_map/ppermute | solution.py:41
  141.6 1.9 collective-permute-start.12
  143.6 2.0 collective-permute-start.14
  145.5 5.5 %collective-permute-start.13 = (bf16[1024,128]{1,0:T(8,128)(2,1)S(1)}, bf16[1024,128]{1,0:T(8,128)(2,1)S(1)}, u32[]{:S(2)}, u32[]{:S(2)}) collective-permute-start(bf16[1024,128]{1,0:T(8,128)(2,1)S(1)} %collective-permute-done.10), channel_id=1, source_target_pairs={{0,2},{1,3},{2,4},{3,5},{4,6},{5,7},{6,8},{7,9},{8,10},{9,11},{10,... | collective-permute-start | bytes 786440 | tf_op jit(solution)/shard_map/ppermute | solution.py:41
  151.5 4.6 %collective-permute-done.14 = bf16[1024,128]{1,0:T(8,128)(2,1)S(1)} collective-permute-done((bf16[1024,128]{1,0:T(8,128)(2,1)S(1)}, bf16[1024,128]{1,0:T(8,128)(2,1)S(1)}, u32[]{:S(2)}, u32[]{:S(2)}) %collective-permute-start.14) | collective-permute-done | bytes 262176 | tf_op jit(solution)/shard_map/ppermute | solution.py:41
  156.1 1.9 collective-permute-start.17
  158.1 5.1 %collective-permute-start.16 = (bf16[512,128]{1,0:T(8,128)(2,1)S(1)}, bf16[512,128]{1,0:T(8,128)(2,1)S(1)}, u32[]{:S(2)}, u32[]{:S(2)}) collective-permute-start(bf16[512,128]{1,0:T(8,128)(2,1)S(1)} %slice.204), channel_id=1, source_target_pairs={{0,2},{1,3},{2,4},{3,5},{4,6},{5,7},{6,8},{7,9},{8,10},{9,11},{10,... | collective-permute-start | bytes 393224 | tf_op jit(solution)/shard_map/ppermute | solution.py:41
  163.3 2.1 collective-permute-start.15
  167.0 2.4 %collective-permute-start.18 = (bf16[1024,128]{1,0:T(8,128)(2,1)S(1)}, bf16[1024,128]{1,0:T(8,128)(2,1)S(1)}, u32[]{:S(2)}, u32[]{:S(2)}) collective-permute-start(bf16[1024,128]{1,0:T(8,128)(2,1)S(1)} %constant_dynamic-update-slice_fusion), channel_id=1, source_target_pairs={{0,1},{1,0},{2,3},{3,2},{4,5},{5,4},{6,7},{7,6},{8,9},{9,8},{10,11... | collective-permute-start | bytes 786440 | tf_op jit(solution)/shard_map/ppermute | solution.py:33
  173.2 2.1 collective-permute-start.19
  175.3 1.7 collective-permute-done.19
  178.1 4.0 %collective-permute-start.20 = (bf16[512,128]{1,0:T(8,128)(2,1)S(1)}, bf16[512,128]{1,0:T(8,128)(2,1)S(1)}, u32[]{:S(2)}, u32[]{:S(2)}) collective-permute-start(bf16[512,128]{1,0:T(8,128)(2,1)S(1)} %get-tuple-element.86), channel_id=1, source_target_pairs={{0,2},{1,3},{2,4},{3,5},{4,6},{5,7},{6,8},{7,9},{8,10},{9,11},{10,... | collective-permute-start | bytes 393224 | tf_op jit(solution)/shard_map/ppermute | solution.py:41
  182.1 1.9 collective-permute-start.24
  185.6 5.4 %collective-permute-start.21 = (bf16[1024,128]{1,0:T(8,128)(2,1)S(1)}, bf16[1024,128]{1,0:T(8,128)(2,1)S(1)}, u32[]{:S(2)}, u32[]{:S(2)}) collective-permute-start(bf16[1024,128]{1,0:T(8,128)(2,1)S(1)} %fusion.78), channel_id=1, source_target_pairs={{0,2},{1,3},{2,4},{3,5},{4,6},{5,7},{6,8},{7,9},{8,10},{9,11},{10,... | collective-permute-start | bytes 786440 | tf_op jit(solution)/shard_map/ppermute | solution.py:41
  191.9 1.9 collective-permute-start.25
  193.8 2.4 %collective-permute-done.21 = bf16[1024,128]{1,0:T(8,128)(2,1)S(1)} collective-permute-done((bf16[1024,128]{1,0:T(8,128)(2,1)S(1)}, bf16[1024,128]{1,0:T(8,128)(2,1)S(1)}, u32[]{:S(2)}, u32[]{:S(2)}) %collective-permute-start.21) | collective-permute-done | bytes 262176 | tf_op jit(solution)/shard_map/ppermute | solution.py:41
  196.3 5.6 %collective-permute-start.22 = (bf16[1024,128]{1,0:T(8,128)(2,1)S(1)}, bf16[1024,128]{1,0:T(8,128)(2,1)S(1)}, u32[]{:S(2)}, u32[]{:S(2)}) collective-permute-start(bf16[1024,128]{1,0:T(8,128)(2,1)S(1)} %fusion.77), channel_id=1, source_target_pairs={{0,2},{1,3},{2,4},{3,5},{4,6},{5,7},{6,8},{7,9},{8,10},{9,11},{10,... | collective-permute-start | bytes 786440 | tf_op jit(solution)/shard_map/ppermute | solution.py:41
  202.5 2.1 collective-permute-start.26
  204.6 1.7 collective-permute-done.22
  206.3 5.6 %collective-permute-start.23 = (bf16[1024,128]{1,0:T(8,128)(2,1)S(1)}, bf16[1024,128]{1,0:T(8,128)(2,1)S(1)}, u32[]{:S(2)}, u32[]{:S(2)}) collective-permute-start(bf16[1024,128]{1,0:T(8,128)(2,1)S(1)} %fusion.76), channel_id=1, source_target_pairs={{0,2},{1,3},{2,4},{3,5},{4,6},{5,7},{6,8},{7,9},{8,10},{9,11},{10,... | collective-permute-start | bytes 786440 | tf_op jit(solution)/shard_map/ppermute | solution.py:41
  212.4 1.9 collective-permute-start.27
  215.8 6.1 %collective-permute-done.27 = bf16[1024,128]{1,0:T(8,128)(2,1)S(1)} collective-permute-done((bf16[1024,128]{1,0:T(8,128)(2,1)S(1)}, bf16[1024,128]{1,0:T(8,128)(2,1)S(1)}, u32[]{:S(2)}, u32[]{:S(2)}) %collective-permute-start.27) | collective-permute-done | bytes 262176 | tf_op jit(solution)/shard_map/ppermute | solution.py:41
  222.7 4.6 %all-to-all-start.3 = ((bf16[32,32,128]{2,1,0:T(8,128)(2,1)}), bf16[32,32,128]{2,1,0:T(8,128)(2,1)S(1)}, u32[]{:S(2)}, u32[]{:S(2)}) async-start(bf16[32,32,128]{2,1,0:T(8,128)(2,1)} %bitcast.74), calls=%async_computation.3 | async-start | bytes 524288 | tf_op jit(solution)/shard_map/all_to_all | solution.py:27
  227.3 11.3 %all-to-all-done.3 = bf16[32,32,128]{2,1,0:T(8,128)(2,1)S(1)} async-done(((bf16[32,32,128]{2,1,0:T(8,128)(2,1)}), bf16[32,32,128]{2,1,0:T(8,128)(2,1)S(1)}, u32[]{:S(2)}, u32[]{:S(2)}) %all-to-all-start.3) | async-done | bytes 262176 | tf_op jit(solution)/shard_map/all_to_all | solution.py:27
  (139 shorter events, 30.7 us)
Async XLA Ops:
  0.0 89.9 %copy-start = (bf16[1024,128]{1,0:T(8,128)(2,1)S(1)}, bf16[1024,128]{1,0:T(8,128)(2,1)}, u32[]{:S(2)}) copy-start(bf16[1024,128]{1,0:T(8,128)(2,1)} %param.19) | copy-start | bytes 786436
  0.0 20.2 %copy-start.1 = (bf16[1,4096,128]{2,1,0:T(8,128)(2,1)S(1)}, bf16[1,4096,128]{2,1,0:T(8,128)(2,1)}, u32[]{:S(2)}) copy-start(bf16[1,4096,128]{2,1,0:T(8,128)(2,1)} %param.27) | copy-start | bytes 3145732
  3.9 29.8 %copy-start.7 = (s32[256,2]{0,1:T(2,128)S(1)}, s32[256,2]{0,1:T(2,128)}, u32[]{:S(2)}) copy-start(s32[256,2]{0,1:T(2,128)} %param.22) | copy-start | bytes 6148
  5.6 28.8 %collective-permute-start = (bf16[256,96]{0,1:T(8,128)(2,1)S(1)}, bf16[256,96]{0,1:T(8,128)(2,1)S(1)}, u32[]{:S(2)}, u32[]{:S(2)}) collective-permute-start(bf16[256,96]{0,1:T(8,128)(2,1)S(1)} %get-tuple-element.121), channel_id=1, source_target_pairs={{0,16},{16,0},{32,48},{48,32},{64,80},{80,64},{96,112},{112,96},{1... | collective-permute-start | bytes 147464 | tf_op jit(solution)/shard_map/ppermute | solution.py:37
  9.9 37.1 %all-to-all-start = ((bf16[8,160,256]{2,1,0:T(8,128)(2,1)}), bf16[8,160,256]{2,1,0:T(8,128)(2,1)S(1)}, u32[]{:S(2)}, u32[]{:S(2)}) async-start(bf16[8,160,256]{2,1,0:T(8,128)(2,1)} %broadcast_in_dim.9), calls=%async_computation | async-start | bytes 1310720 | tf_op jit(solution)/shard_map/all_to_all | solution.py:27
  21.0 23.3 %collective-permute-start.4 = (bf16[2,512,128]{2,1,0:T(8,128)(2,1)}, bf16[2,512,128]{2,1,0:T(8,128)(2,1)}, u32[]{:S(2)}, u32[]{:S(2)}) collective-permute-start(bf16[2,512,128]{2,1,0:T(8,128)(2,1)} %get-tuple-element.69), channel_id=1, source_target_pairs={{0,12},{1,13},{2,14},{3,15},{4,0},{5,1},{6,2},{7,3},{8,4},{9,5},{1... | collective-permute-start | bytes 786440 | tf_op jit(solution)/shard_map/ppermute | solution.py:41
  25.0 20.3 %collective-permute-start.3 = (bf16[2,512,128]{2,1,0:T(8,128)(2,1)S(1)}, bf16[2,512,128]{2,1,0:T(8,128)(2,1)}, u32[]{:S(2)}, u32[]{:S(2)}) collective-permute-start(bf16[2,512,128]{2,1,0:T(8,128)(2,1)S(1)} %get-tuple-element.70), channel_id=1, source_target_pairs={{0,8},{1,9},{2,10},{3,11},{4,12},{5,13},{6,14},{7,15},{8,0},{9,1},... | collective-permute-start | bytes 786440 | tf_op jit(solution)/shard_map/ppermute | solution.py:41
  27.9 29.6 %collective-permute-start.2 = (bf16[2,512,128]{2,1,0:T(8,128)(2,1)S(1)}, bf16[2,512,128]{2,1,0:T(8,128)(2,1)}, u32[]{:S(2)}, u32[]{:S(2)}) collective-permute-start(bf16[2,512,128]{2,1,0:T(8,128)(2,1)S(1)} %get-tuple-element.71), channel_id=1, source_target_pairs={{0,4},{1,5},{2,6},{3,7},{4,8},{5,9},{6,10},{7,11},{8,12},{9,13},{1... | collective-permute-start | bytes 786440 | tf_op jit(solution)/shard_map/ppermute | solution.py:41
  34.4 8.0 %collective-permute-start.1 = (bf16[2,256,96]{1,2,0:T(8,128)(2,1)S(1)}, bf16[2,256,96]{1,2,0:T(8,128)(2,1)S(1)}, u32[]{:S(2)}, u32[]{:S(2)}) collective-permute-start(bf16[2,256,96]{1,2,0:T(8,128)(2,1)S(1)} %pad_maximum_fusion.9), channel_id=1, source_target_pairs={{0,32},{16,48},{32,0},{48,16},{64,96},{80,112},{96,64},{112,80},{1... | collective-permute-start | bytes 294920 | tf_op jit(solution)/shard_map/ppermute | solution.py:37
  52.8 37.1 %copy-start.5 = (bf16[256,128]{1,0:T(8,128)(2,1)S(1)}, bf16[256,128]{1,0:T(8,128)(2,1)}, u32[]{:S(2)}) copy-start(bf16[256,128]{1,0:T(8,128)(2,1)} %param.20) | copy-start | bytes 196612
  53.6 13.7 %all-to-all-start.1 = ((f32[4,72,256]{2,1,0:T(8,128)}), f32[4,72,256]{2,1,0:T(8,128)S(1)}, u32[]{:S(2)}, u32[]{:S(2)}) async-start(f32[4,72,256]{2,1,0:T(8,128)} %pad_maximum_fusion.7), calls=%async_computation.1 | async-start | bytes 589824 | tf_op jit(solution)/shard_map/all_to_all | solution.py:27
  58.6 32.6 %collective-permute-start.5 = (bf16[4,512,128]{2,1,0:T(8,128)(2,1)S(1)}, bf16[4,512,128]{2,1,0:T(8,128)(2,1)S(1)}, u32[]{:S(2)}, u32[]{:S(2)}) collective-permute-start(bf16[4,512,128]{2,1,0:T(8,128)(2,1)S(1)} %pad_maximum_fusion.1), channel_id=1, source_target_pairs={{0,2},{1,3},{2,0},{3,1},{4,6},{5,7},{6,4},{7,5},{8,10},{9,11},{10,... | collective-permute-start | bytes 1572872 | tf_op jit(solution)/shard_map/ppermute | solution.py:118
  90.2 1.1 copy-start.3
  91.3 23.6 %all-to-all-start.2 = ((bf16[32,32,128]{2,1,0:T(8,128)(2,1)}), bf16[32,32,128]{2,1,0:T(8,128)(2,1)S(1)}, u32[]{:S(2)}, u32[]{:S(2)}) async-start(bf16[32,32,128]{2,1,0:T(8,128)(2,1)} %bitcast.33), calls=%async_computation.2 | async-start | bytes 524288 | tf_op jit(solution)/shard_map/all_to_all | solution.py:27
  101.5 1.8 copy-start.8
  114.9 9.6 %collective-permute-start.8 = (bf16[1024,128]{1,0:T(8,128)(2,1)S(1)}, bf16[1024,128]{1,0:T(8,128)(2,1)S(1)}, u32[]{:S(2)}, u32[]{:S(2)}) collective-permute-start(bf16[1024,128]{1,0:T(8,128)(2,1)S(1)} %bitcast.157), channel_id=1, source_target_pairs={{0,14},{1,15},{2,0},{3,1},{4,2},{5,3},{6,4},{7,5},{8,6},{9,7},{10,... | collective-permute-start | bytes 786440 | tf_op jit(solution)/shard_map/ppermute | solution.py:41
  116.8 9.0 %collective-permute-start.7 = (bf16[1024,128]{1,0:T(8,128)(2,1)S(1)}, bf16[1024,128]{1,0:T(8,128)(2,1)S(1)}, u32[]{:S(2)}, u32[]{:S(2)}) collective-permute-start(bf16[1024,128]{1,0:T(8,128)(2,1)S(1)} %bitcast.158), channel_id=1, source_target_pairs={{0,2},{1,3},{2,4},{3,5},{4,6},{5,7},{6,8},{7,9},{8,10},{9,11},{10,... | collective-permute-start | bytes 786440 | tf_op jit(solution)/shard_map/ppermute | solution.py:41
  122.0 13.6 %collective-permute-start.6 = (bf16[1024,128]{1,0:T(8,128)(2,1)S(1)}, bf16[1024,128]{1,0:T(8,128)(2,1)S(1)}, u32[]{:S(2)}, u32[]{:S(2)}) collective-permute-start(bf16[1024,128]{1,0:T(8,128)(2,1)S(1)} %bitcast.159), channel_id=1, source_target_pairs={{0,1},{1,0},{2,3},{3,2},{4,5},{5,4},{6,7},{7,6},{8,9},{9,8},{10,11... | collective-permute-start | bytes 786440 | tf_op jit(solution)/shard_map/ppermute | solution.py:33
  125.9 39.9 %collective-permute-start.9 = (bf16[1024,256]{1,0:T(8,128)(2,1)S(1)}, bf16[1024,256]{1,0:T(8,128)(2,1)S(1)}, u32[]{:S(2)}, u32[]{:S(2)}) collective-permute-start(bf16[1024,256]{1,0:T(8,128)(2,1)S(1)} %pad_maximum_fusion.3), channel_id=1, source_target_pairs={{0,1},{1,0},{2,3},{3,2},{4,5},{5,4},{6,7},{7,6},{8,9},{9,8},{10,11... | collective-permute-start | bytes 1572872 | tf_op jit(solution)/shard_map/ppermute | solution.py:33
  127.8 12.6 %collective-permute-start.11 = (bf16[1024,128]{1,0:T(8,128)(2,1)S(1)}, bf16[1024,128]{1,0:T(8,128)(2,1)S(1)}, u32[]{:S(2)}, u32[]{:S(2)}) collective-permute-start(bf16[1024,128]{1,0:T(8,128)(2,1)S(1)} %collective-permute-done.8), channel_id=1, source_target_pairs={{0,14},{1,15},{2,0},{3,1},{4,2},{5,3},{6,4},{7,5},{8,6},{9,7},{10,... | collective-permute-start | bytes 786440 | tf_op jit(solution)/shard_map/ppermute | solution.py:41
  131.0 10.6 %collective-permute-start.10 = (bf16[1024,128]{1,0:T(8,128)(2,1)S(1)}, bf16[1024,128]{1,0:T(8,128)(2,1)S(1)}, u32[]{:S(2)}, u32[]{:S(2)}) collective-permute-start(bf16[1024,128]{1,0:T(8,128)(2,1)S(1)} %collective-permute-done.7), channel_id=1, source_target_pairs={{0,2},{1,3},{2,4},{3,5},{4,6},{5,7},{6,8},{7,9},{8,10},{9,11},{10,... | collective-permute-start | bytes 786440 | tf_op jit(solution)/shard_map/ppermute | solution.py:41
  141.6 28.1 %collective-permute-start.12 = (bf16[1024,256]{1,0:T(8,128)(2,1)S(1)}, bf16[1024,256]{1,0:T(8,128)(2,1)S(1)}, u32[]{:S(2)}, u32[]{:S(2)}) collective-permute-start(bf16[1024,256]{1,0:T(8,128)(2,1)S(1)} %pad_maximum_fusion.4), channel_id=1, source_target_pairs={{0,1},{1,0},{2,3},{3,2},{4,5},{5,4},{6,7},{7,6},{8,9},{9,8},{10,11... | collective-permute-start | bytes 1572872 | tf_op jit(solution)/shard_map/ppermute | solution.py:33
  143.6 12.6 %collective-permute-start.14 = (bf16[1024,128]{1,0:T(8,128)(2,1)S(1)}, bf16[1024,128]{1,0:T(8,128)(2,1)S(1)}, u32[]{:S(2)}, u32[]{:S(2)}) collective-permute-start(bf16[1024,128]{1,0:T(8,128)(2,1)S(1)} %collective-permute-done.11), channel_id=1, source_target_pairs={{0,14},{1,15},{2,0},{3,1},{4,2},{5,3},{6,4},{7,5},{8,6},{9,7},{10,... | collective-permute-start | bytes 786440 | tf_op jit(solution)/shard_map/ppermute | solution.py:41
  145.5 12.5 %collective-permute-start.13 = (bf16[1024,128]{1,0:T(8,128)(2,1)S(1)}, bf16[1024,128]{1,0:T(8,128)(2,1)S(1)}, u32[]{:S(2)}, u32[]{:S(2)}) collective-permute-start(bf16[1024,128]{1,0:T(8,128)(2,1)S(1)} %collective-permute-done.10), channel_id=1, source_target_pairs={{0,2},{1,3},{2,4},{3,5},{4,6},{5,7},{6,8},{7,9},{8,10},{9,11},{10,... | collective-permute-start | bytes 786440 | tf_op jit(solution)/shard_map/ppermute | solution.py:41
  156.1 10.9 %collective-permute-start.17 = (bf16[512,128]{1,0:T(8,128)(2,1)S(1)}, bf16[512,128]{1,0:T(8,128)(2,1)S(1)}, u32[]{:S(2)}, u32[]{:S(2)}) collective-permute-start(bf16[512,128]{1,0:T(8,128)(2,1)S(1)} %slice.205), channel_id=1, source_target_pairs={{0,14},{1,15},{2,0},{3,1},{4,2},{5,3},{6,4},{7,5},{8,6},{9,7},{10,... | collective-permute-start | bytes 393224 | tf_op jit(solution)/shard_map/ppermute | solution.py:41
  158.1 8.9 %collective-permute-start.16 = (bf16[512,128]{1,0:T(8,128)(2,1)S(1)}, bf16[512,128]{1,0:T(8,128)(2,1)S(1)}, u32[]{:S(2)}, u32[]{:S(2)}) collective-permute-start(bf16[512,128]{1,0:T(8,128)(2,1)S(1)} %slice.204), channel_id=1, source_target_pairs={{0,2},{1,3},{2,4},{3,5},{4,6},{5,7},{6,8},{7,9},{8,10},{9,11},{10,... | collective-permute-start | bytes 393224 | tf_op jit(solution)/shard_map/ppermute | solution.py:41
  163.3 7.8 %collective-permute-start.15 = (bf16[1024,256]{1,0:T(8,128)(2,1)S(1)}, bf16[1024,256]{1,0:T(8,128)(2,1)S(1)}, u32[]{:S(2)}, u32[]{:S(2)}) collective-permute-start(bf16[1024,256]{1,0:T(8,128)(2,1)S(1)} %pad_maximum_fusion.5), channel_id=1, source_target_pairs={{0,1},{1,0},{2,3},{3,2},{4,5},{5,4},{6,7},{7,6},{8,9},{9,8},{10,11... | collective-permute-start | bytes 1572872 | tf_op jit(solution)/shard_map/ppermute | solution.py:33
  167.0 3.8 %collective-permute-start.18 = (bf16[1024,128]{1,0:T(8,128)(2,1)S(1)}, bf16[1024,128]{1,0:T(8,128)(2,1)S(1)}, u32[]{:S(2)}, u32[]{:S(2)}) collective-permute-start(bf16[1024,128]{1,0:T(8,128)(2,1)S(1)} %constant_dynamic-update-slice_fusion), channel_id=1, source_target_pairs={{0,1},{1,0},{2,3},{3,2},{4,5},{5,4},{6,7},{7,6},{8,9},{9,8},{10,11... | collective-permute-start | bytes 786440 | tf_op jit(solution)/shard_map/ppermute | solution.py:33
  172.9 4.6 %copy-start.2 = (bf16[512,128]{1,0:T(8,128)(2,1)S(1)}, bf16[512,128]{1,0:T(8,128)(2,1)}, u32[]{:S(2)}) copy-start(bf16[512,128]{1,0:T(8,128)(2,1)} %get-tuple-element.41) | copy-start | bytes 393220
  173.2 3.8 %collective-permute-start.19 = (bf16[1024,256]{0,1:T(8,128)(2,1)S(1)}, bf16[1024,256]{0,1:T(8,128)(2,1)S(1)}, u32[]{:S(2)}, u32[]{:S(2)}) collective-permute-start(bf16[1024,256]{0,1:T(8,128)(2,1)S(1)} %fusion.13), channel_id=1, source_target_pairs={{0,1},{1,0},{2,3},{3,2},{4,5},{5,4},{6,7},{7,6},{8,9},{9,8},{10,11... | collective-permute-start | bytes 1572872 | tf_op jit(solution)/shard_map/ppermute | solution.py:33
  178.1 7.4 %collective-permute-start.20 = (bf16[512,128]{1,0:T(8,128)(2,1)S(1)}, bf16[512,128]{1,0:T(8,128)(2,1)S(1)}, u32[]{:S(2)}, u32[]{:S(2)}) collective-permute-start(bf16[512,128]{1,0:T(8,128)(2,1)S(1)} %get-tuple-element.86), channel_id=1, source_target_pairs={{0,2},{1,3},{2,4},{3,5},{4,6},{5,7},{6,8},{7,9},{8,10},{9,11},{10,... | collective-permute-start | bytes 393224 | tf_op jit(solution)/shard_map/ppermute | solution.py:41
  182.1 9.7 %collective-permute-start.24 = (bf16[512,128]{1,0:T(8,128)(2,1)S(1)}, bf16[512,128]{1,0:T(8,128)(2,1)S(1)}, u32[]{:S(2)}, u32[]{:S(2)}) collective-permute-start(bf16[512,128]{1,0:T(8,128)(2,1)S(1)} %get-tuple-element.87), channel_id=1, source_target_pairs={{0,14},{1,15},{2,0},{3,1},{4,2},{5,3},{6,4},{7,5},{8,6},{9,7},{10,... | collective-permute-start | bytes 393224 | tf_op jit(solution)/shard_map/ppermute | solution.py:41
  185.6 10.7 %collective-permute-start.21 = (bf16[1024,128]{1,0:T(8,128)(2,1)S(1)}, bf16[1024,128]{1,0:T(8,128)(2,1)S(1)}, u32[]{:S(2)}, u32[]{:S(2)}) collective-permute-start(bf16[1024,128]{1,0:T(8,128)(2,1)S(1)} %fusion.78), channel_id=1, source_target_pairs={{0,2},{1,3},{2,4},{3,5},{4,6},{5,7},{6,8},{7,9},{8,10},{9,11},{10,... | collective-permute-start | bytes 786440 | tf_op jit(solution)/shard_map/ppermute | solution.py:41
  191.9 10.5 %collective-permute-start.25 = (bf16[1024,128]{1,0:T(8,128)(2,1)S(1)}, bf16[1024,128]{1,0:T(8,128)(2,1)S(1)}, u32[]{:S(2)}, u32[]{:S(2)}) collective-permute-start(bf16[1024,128]{1,0:T(8,128)(2,1)S(1)} %fusion.75), channel_id=1, source_target_pairs={{0,14},{1,15},{2,0},{3,1},{4,2},{5,3},{6,4},{7,5},{8,6},{9,7},{10,... | collective-permute-start | bytes 786440 | tf_op jit(solution)/shard_map/ppermute | solution.py:41
  196.3 10.0 %collective-permute-start.22 = (bf16[1024,128]{1,0:T(8,128)(2,1)S(1)}, bf16[1024,128]{1,0:T(8,128)(2,1)S(1)}, u32[]{:S(2)}, u32[]{:S(2)}) collective-permute-start(bf16[1024,128]{1,0:T(8,128)(2,1)S(1)} %fusion.77), channel_id=1, source_target_pairs={{0,2},{1,3},{2,4},{3,5},{4,6},{5,7},{6,8},{7,9},{8,10},{9,11},{10,... | collective-permute-start | bytes 786440 | tf_op jit(solution)/shard_map/ppermute | solution.py:41
  202.5 24.8 %copy-start.6 = (f32[256,2]{0,1:T(2,128)S(1)}, f32[256,2]{0,1:T(2,128)}, u32[]{:S(2)}) copy-start(f32[256,2]{0,1:T(2,128)} %param.23) | copy-start | bytes 6148
  202.5 24.8 %copy-start.9 = (f32[256]{0:T(256)S(1)}, f32[256]{0:T(256)}, u32[]{:S(2)}) copy-start(f32[256]{0:T(256)} %param.24) | copy-start | bytes 3076
  202.5 36.1 %copy-start.4 = (bf16[256,128]{1,0:T(8,128)(2,1)S(1)}, bf16[256,128]{1,0:T(8,128)(2,1)}, u32[]{:S(2)}) copy-start(bf16[256,128]{1,0:T(8,128)(2,1)} %copy-done.3) | copy-start | bytes 196612
  202.5 9.8 %collective-permute-start.26 = (bf16[1024,128]{1,0:T(8,128)(2,1)S(1)}, bf16[1024,128]{1,0:T(8,128)(2,1)S(1)}, u32[]{:S(2)}, u32[]{:S(2)}) collective-permute-start(bf16[1024,128]{1,0:T(8,128)(2,1)S(1)} %fusion.74), channel_id=1, source_target_pairs={{0,14},{1,15},{2,0},{3,1},{4,2},{5,3},{6,4},{7,5},{8,6},{9,7},{10,... | collective-permute-start | bytes 786440 | tf_op jit(solution)/shard_map/ppermute | solution.py:41
  206.3 9.5 %collective-permute-start.23 = (bf16[1024,128]{1,0:T(8,128)(2,1)S(1)}, bf16[1024,128]{1,0:T(8,128)(2,1)S(1)}, u32[]{:S(2)}, u32[]{:S(2)}) collective-permute-start(bf16[1024,128]{1,0:T(8,128)(2,1)S(1)} %fusion.76), channel_id=1, source_target_pairs={{0,2},{1,3},{2,4},{3,5},{4,6},{5,7},{6,8},{7,9},{8,10},{9,11},{10,... | collective-permute-start | bytes 786440 | tf_op jit(solution)/shard_map/ppermute | solution.py:41
  212.4 9.5 %collective-permute-start.27 = (bf16[1024,128]{1,0:T(8,128)(2,1)S(1)}, bf16[1024,128]{1,0:T(8,128)(2,1)S(1)}, u32[]{:S(2)}, u32[]{:S(2)}) collective-permute-start(bf16[1024,128]{1,0:T(8,128)(2,1)S(1)} %fusion.73), channel_id=1, source_target_pairs={{0,14},{1,15},{2,0},{3,1},{4,2},{5,3},{6,4},{7,5},{8,6},{9,7},{10,... | collective-permute-start | bytes 786440 | tf_op jit(solution)/shard_map/ppermute | solution.py:41
  222.7 15.9 %all-to-all-start.3 = ((bf16[32,32,128]{2,1,0:T(8,128)(2,1)}), bf16[32,32,128]{2,1,0:T(8,128)(2,1)S(1)}, u32[]{:S(2)}, u32[]{:S(2)}) async-start(bf16[32,32,128]{2,1,0:T(8,128)(2,1)} %bitcast.74), calls=%async_computation.3 | async-start | bytes 524288 | tf_op jit(solution)/shard_map/all_to_all | solution.py:27
